TPU v7x, 128 devices: a whole 4x4x4 slice. The times are simulated.
128 devices in a mesh: sp: 64 (over z, y, x), tp: 2 (over core).
Axes of the slice: x: 4, y: 4, z: 4, core: 2. Of those that a mesh axis runs over, the one named last changes fastest.
Arguments:
- tokens: bfloat16 [24576, 2048], P(('sp', 'tp')), may hold values from -6 to 6
- norm_gain: float32 [2048], replicated, may hold values from 0.1 to 1.9
- w_query: bfloat16 [2048, 1024], P(None, 'tp'), may hold values from -0.125 to 0.125
- w_key: bfloat16 [2048, 1024], P(None, 'tp'), may hold values from -0.125 to 0.125
- w_value: bfloat16 [2048, 2048], P(None, 'tp'), may hold values from -0.125 to 0.125
- w_ogate: bfloat16 [2048, 2048], P(None, 'tp'), may hold values from -0.125 to 0.125
- w_igate: bfloat16 [2048, 8], replicated, may hold values from -0.125 to 0.125
- w_fgate: bfloat16 [2048, 8], replicated, may hold values from -0.125 to 0.125
- conv_query: bfloat16 [4, 1024], replicated, may hold values from -3 to 3
- conv_key: bfloat16 [4, 1024], replicated, may hold values from -3 to 3
- gate_offset: float32 [2, 192, 8], P(None, 'sp', 'tp'), may hold values from -60 to 140, as said below
- head_gain: float32 [2048], replicated, may hold values from 0.1 to 1.9
- w_out: bfloat16 [2048, 2048], P('tp'), may hold values from -0.125 to 0.125
Outputs:
- mixed: bfloat16 [24576, 2048], P(('sp', 'tp'))
Inputs may be any that keep to these rules, and one draw needn't show every extreme that they name: `gate_offset`: row 0 is added to the input gate's pre-activation and row 1 to the forget gate's; each entry holds for one block of 128 positions and one head.
All inputs are finite; a program needn't handle non-finite values.
Results may differ from a plain program's by a relative error of at most 0.011.
Values may be sent and summed in bfloat16 or wider, within the bound.
No kernel may reach another device: no remote copies, remote signals or barrier semaphores. Data moves between devices by JAX's collectives and lax.ppermute only.
A program may use at most 128 MiB of HBM per device.

v0:
```python
import jax
import jax.numpy as jnp
import numpy as np
from jax import lax
from jax.experimental import pallas as pl
from jax.experimental.pallas import tpu as pltpu
from jax.sharding import Mesh
from jax.sharding import PartitionSpec as P


SPAN = 128
SP = ("sp_0", "sp_1", "sp_2")
SP_TP = ("sp_0", "sp_1", "sp_2", "tp")
EPS = 1e-06
EMPTY = -1e30
TAIL = 16
HEADS = 4
DQK = 128
DV = 256
WIDTH = DV + 128
BLOCKS = 3
ROWS = BLOCKS * SPAN
HALF = ROWS // 2
HIGHEST = lax.Precision.HIGHEST
BF = jnp.bfloat16
F32 = jnp.float32
MIB = 1 << 20


def call(kernel, outs, out_spaces, spaces, scratch=(), flops=0, limit=8):
    def spec(space):
        return pl.BlockSpec(memory_space=pltpu.VMEM if space is None else space)

    def placed(like, space):
        return like if space is None else space(like.shape, like.dtype)

    several = isinstance(outs, tuple)
    run = pl.pallas_call(
        kernel,
        out_shape=tuple(map(placed, outs, out_spaces)) if several else placed(outs, out_spaces),
        in_specs=[spec(space) for space in spaces],
        out_specs=tuple(map(spec, out_spaces)) if several else spec(out_spaces),
        scratch_shapes=list(scratch),
        cost_estimate=pl.CostEstimate(flops=flops, transcendentals=0, bytes_accessed=1 << 20),
        compiler_params=pltpu.CompilerParams(vmem_limit_bytes=limit * MIB),
    )

    def kept(x, space):
        return x if space is None else pltpu.with_memory_space_constraint(x, space)

    return lambda *args: run(*map(kept, args, spaces))


def started(pairs, sems):
    copies = [pltpu.make_async_copy(src, dst, sems.at[n]) for n, (src, dst) in enumerate(pairs)]
    for copy in copies:
        copy.start()
    return copies


def by_rows(src, dst, parts):
    rows = src.shape[0] // parts
    return [(src.at[pl.ds(c * rows, rows)], dst.at[pl.ds(c * rows, rows)]) for c in range(parts)]


def wait_all(copies):
    for copy in copies:
        copy.wait()


def thirds(x):
    hi = x.astype(BF).astype(F32)
    rest = x - hi
    mid = rest.astype(BF).astype(F32)
    return hi, mid, (rest - mid).astype(BF).astype(F32)


def lane_of(shape):
    return lax.broadcasted_iota(jnp.int32, shape, len(shape) - 1)


def mixed_rows(pre_ref, taps, lanes, first, rows):
    acc = None
    for j in range(4):
        term = taps[j : j + 1, lanes] * pre_ref[pl.ds(first + TAIL - 3 + j, rows), lanes]
        acc = term if acc is None else acc + term
    return acc * (1.0 / (1.0 + jnp.exp(-acc)))


def row_scale(x):
    return lax.rsqrt(jnp.mean(x * x, axis=-1, keepdims=True) + EPS)


def normalized(x, gain):
    x = x.astype(F32)
    return (x * row_scale(x) * gain).astype(BF)


def fetch_kernel(own_hbm, gain_hbm, wk_hbm, wv_hbm, rows_ref, wk_ref, wv_ref, own_ref, gain_ref, sems):
    copies = started(
        [(own_hbm, own_ref), (gain_hbm, gain_ref)] + by_rows(wk_hbm, wk_ref, 4) + by_rows(wv_hbm, wv_ref, 8), sems
    )
    copies[0].wait()
    parts = [slice(at, at + 48) for at in range(0, HALF, 48)]
    scales = [row_scale(own_ref[part, :].astype(F32)) for part in parts]
    copies[1].wait()
    gain = gain_ref[...]
    for part, scale in zip(parts, scales):
        rows_ref[part, :] = (own_ref[part, :].astype(F32) * scale * gain).astype(BF)
    wait_all(copies[2:])


def summary_kernel(own_ref, oth_ref, one_ref, two_ref, gain_ref, wk_ref, wv_ref, wi_ref, wf_ref, taps_ref, offs_ref,
                   key_out, value_out, logs_out, piece_ref, rows_out,
                   rows_ref, pre_ref, key_ref, value_ref, logs_ref, wg_ref, sems):
    outs = [
        pltpu.make_async_copy(src, dst, sems.at[n])
        for n, (src, dst) in enumerate(
            [(logs_ref, logs_out), (key_ref, key_out), (value_ref, value_out), (rows_ref, rows_out)]
        )
    ]
    tp = lax.axis_index("tp")
    gain = gain_ref[...]
    rows_ref[0:TAIL, :] = normalized(one_ref[...] + two_ref[...], gain)
    mine = pl.multiple_of(TAIL + tp * HALF, 16)
    rows_ref[pl.ds(mine, HALF), :] = own_ref[...]
    for part in range(HALF // 48):
        to = pl.multiple_of(TAIL + (1 - tp) * HALF + part * 48, 16)
        rows_ref[pl.ds(to, 48), :] = normalized(oth_ref[part * 48 : part * 48 + 48, :], gain)
    outs[3].start()
    all_heads = wi_ref.shape[0]
    wg_ref[...] = jnp.zeros_like(wg_ref)
    wg_ref[0:all_heads, :] = wi_ref[...]
    wg_ref[all_heads : 2 * all_heads, :] = wf_ref[...]
    own = pl.ds(TAIL, ROWS)
    gates = lax.dot_general(rows_ref[own, :], wg_ref[...], (((1,), (1,)), ((), ())), preferred_element_type=F32)
    gates = jnp.where(tp == 0, gates, pltpu.roll(gates, 128 - HEADS, 1))
    pre_ref[...] = jnp.dot(rows_ref[...], wk_ref[...], preferred_element_type=F32).astype(BF).astype(F32)

    lane = lane_of((SPAN, 128))
    tri = (lax.broadcasted_iota(jnp.int32, (SPAN, SPAN), 0) >= lax.broadcasted_iota(jnp.int32, (SPAN, SPAN), 1)).astype(F32)
    gate, inside, totals = [], [], []
    for b in range(BLOCKS):
        offs = jnp.zeros((1, 128), F32)
        for h in range(HEADS):
            for row, at in ((0, h), (1, 2 * HEADS + h)):
                offs = jnp.where(lane_of((1, 128)) == at, offs_ref[b, row : row + 1, h : h + 1], offs)
        g = gates[b * SPAN : (b + 1) * SPAN] + offs
        soft = jnp.minimum(g, 0.0) - jnp.log1p(jnp.exp(-jnp.abs(g)))
        total = jnp.dot(tri, soft, precision=HIGHEST, preferred_element_type=F32)
        logs_ref[b * SPAN : (b + 1) * SPAN, :] = jnp.where(lane < HEADS, g, pltpu.roll(total, 128 - HEADS, 1))
        total = pltpu.roll(total, 128 - 2 * HEADS, 1)
        gate.append(g)
        inside.append(total)
        totals.append(total[SPAN - 1 : SPAN, :])
    outs[0].start()
    write, level = [], None
    later = jnp.zeros_like(totals[0])
    for b in reversed(range(BLOCKS)):
        w = (totals[b] - inside[b]) + later + gate[b]
        later = later + totals[b]
        write.insert(0, w)
        top = jnp.max(w, axis=0, keepdims=True)
        level = top if level is None else jnp.maximum(level, top)
    weight = [jnp.exp(w - level) for w in write]
    numbers = thirds(later) + thirds(level)

    taps = taps_ref[:, pl.ds(pl.multiple_of(tp * (HEADS * DQK), 128), HEADS * DQK)].astype(F32)
    for h in range(HEADS):
        lanes = slice(h * DQK, (h + 1) * DQK)
        for b in range(BLOCKS):
            rows = slice(b * SPAN, (b + 1) * SPAN)
            key_ref[rows, lanes] = (mixed_rows(pre_ref, taps, lanes, b * SPAN, SPAN) * DQK**-0.5).astype(BF)
    outs[1].start()
    value_ref[...] = jnp.dot(rows_ref[own, :], wv_ref[...], preferred_element_type=F32).astype(BF)
    outs[2].start()
    ones = jnp.ones((ROWS, 128), BF)
    dims = (((0,), (0,)), ((), ()))
    for h in range(HEADS):
        lanes = slice(h * DQK, (h + 1) * DQK)
        weighted = jnp.concatenate(
            [
                (key_ref[b * SPAN : (b + 1) * SPAN, lanes].astype(F32) * weight[b][:, h : h + 1]).astype(BF)
                for b in range(BLOCKS)
            ],
            axis=0,
        )
        memory = lax.dot_general(weighted, value_ref[:, h * DV : (h + 1) * DV], dims, preferred_element_type=F32)
        extra = lax.dot_general(weighted, ones, dims, preferred_element_type=F32)
        for n, number in enumerate(numbers):
            extra = jnp.where(lane == n + 1, number[:, h : h + 1], extra)
        out = slice(h * DQK, (h + 1) * DQK)
        piece_ref[out, :DV] = memory.astype(BF)
        piece_ref[out, DV:] = extra.astype(BF)
    for copy in outs:
        copy.wait()


def prefix_kernel(piece_ref, place_ref, wout_hbm, out_ref, wout_ref, sems):
    copies = started(by_rows(wout_hbm.at[pl.ds(0, wout_ref.shape[0])], wout_ref, 4), sems)
    count = piece_ref.shape[0] // 8
    tall = piece_ref.shape[0]

    def iota(shape, dim):
        return lax.broadcasted_iota(jnp.int32, shape, dim)

    def ones_where(test):
        return jnp.where(test, 1.0, 0.0).astype(BF)

    first = ones_where(iota((count, tall), 1) == 8 * iota((count, tall), 0))
    down = iota((tall, count), 0) - 8 * iota((tall, count), 1)
    spread = ones_where((down >= 0) & (down < 8))
    over = iota((count, tall), 1) - 8 * iota((count, tall), 0)
    spread_over = ones_where((over >= 0) & (over < 8))
    extra = jnp.dot(first, piece_ref[:, DV:], preferred_element_type=F32)
    lane = lane_of((count, 128))

    def number(at):
        return jnp.sum(jnp.where((lane >= at) & (lane < at + 3), extra, 0.0), axis=1, keepdims=True)

    forget, level = number(1), number(4)
    down, over = place_ref[0], place_ref[1]
    steps = jnp.where(down > over, forget, jnp.where(down == over, level, 0.0))
    earlier = over < down
    logs = jnp.dot(jnp.where(earlier, 1.0, 0.0), steps, precision=HIGHEST, preferred_element_type=F32)
    logs = jnp.where(earlier, logs, EMPTY)
    top = jnp.max(logs, axis=1, keepdims=True)
    weight = jnp.where(earlier, jnp.exp(logs - top), 0.0).astype(BF)
    weight = jnp.dot(weight, spread_over, preferred_element_type=F32).astype(BF)
    weight = jnp.dot(spread, weight, preferred_element_type=F32)
    same = (iota((tall, tall), 0) & 7) == (iota((tall, tall), 1) & 7)
    weight = jnp.where(same, weight, 0.0).astype(BF)
    marks = jnp.zeros((count, 128), F32)
    for n, mark in enumerate(thirds(top)):
        marks = jnp.where(lane == n + 1, mark, marks)
    marks = jnp.dot(spread, marks.astype(BF), preferred_element_type=F32)
    state = jnp.dot(weight, piece_ref[...], preferred_element_type=F32)
    lane = lane_of((tall, 128))
    out_ref[:, :DV] = state[:, :DV].astype(BF)
    out_ref[:, DV:] = jnp.where((lane >= 1) & (lane < 4), marks, state[:, DV:]).astype(BF)
    wait_all(copies)


def local_kernel(rows_hbm, wq_hbm, key_hbm, value_hbm, logs_hbm, wo_hbm, taps_ref, gain_ref,
                 query_ref, numer_ref, stats_ref, ogate_ref,
                 rows_ref, wq_ref, pre_ref, key_ref, value_ref, logs_ref, wo_ref, sems):
    copies = started(
        by_rows(rows_hbm, rows_ref, 5)
        + by_rows(wq_hbm, wq_ref, 4)
        + [(logs_hbm, logs_ref), (key_hbm, key_ref), (value_hbm, value_ref)]
        + by_rows(wo_hbm, wo_ref, 8),
        sems,
    )
    tp = lax.axis_index("tp")
    taps = taps_ref[:, pl.ds(pl.multiple_of(tp * (HEADS * DQK), 128), HEADS * DQK)].astype(F32)
    wait_all(copies[:9])
    pre_ref[...] = jnp.dot(rows_ref[...], wq_ref[...], preferred_element_type=F32).astype(BF).astype(F32)
    for h in range(HEADS):
        lanes = slice(h * DQK, (h + 1) * DQK)
        for b in range(BLOCKS):
            rows = slice(b * SPAN, (b + 1) * SPAN)
            query_ref[rows, lanes] = mixed_rows(pre_ref, taps, lanes, b * SPAN, SPAN).astype(BF)
    wait_all(copies[9:12])
    lane = lane_of((SPAN, 128))
    cols = [logs_ref[b * SPAN : (b + 1) * SPAN, :] for b in range(BLOCKS)]
    flat = [c.T for c in cols]
    ends = [c[SPAN - 1 : SPAN, :] for c in cols]
    causal = lax.broadcasted_iota(jnp.int32, (SPAN, SPAN), 0) >= lax.broadcasted_iota(jnp.int32, (SPAN, SPAN), 1)
    stats = []
    before = jnp.zeros_like(ends[0])
    for b in range(BLOCKS):
        carried = pltpu.roll(cols[b] + before, HEADS, 1)
        before = before + ends[b]
        stats.append(jnp.where((lane >= 2 * HEADS) & (lane < 3 * HEADS), carried, 0.0))
    nt = (((1,), (1,)), ((), ()))
    for h in range(HEADS):
        head = slice(h * DQK, (h + 1) * DQK)
        wide = slice(h * DV, (h + 1) * DV)
        for t in range(BLOCKS):
            rows = slice(t * SPAN, (t + 1) * SPAN)
            seen = (t + 1) * SPAN
            now = cols[t][:, HEADS + h : HEADS + h + 1]
            logs = []
            for s in range(t + 1):
                gate = flat[s][h : h + 1, :]
                past = flat[s][HEADS + h : HEADS + h + 1, :]
                if s == t:
                    logs.append(jnp.where(causal, (now - past) + gate, EMPTY))
                else:
                    rest = ends[s][:, HEADS + h : HEADS + h + 1] - past
                    for c in range(s + 1, t):
                        rest = rest + ends[c][:, HEADS + h : HEADS + h + 1]
                    logs.append(now + (rest + gate))
            top = None
            for x in logs:
                peak = jnp.max(x, axis=1, keepdims=True)
                top = peak if top is None else jnp.maximum(top, peak)
            weight = jnp.concatenate([jnp.exp(x - top) for x in logs], axis=1)
            scores = (
                lax.dot_general(query_ref[rows, head], key_ref[:seen, head], nt, preferred_element_type=F32) * weight
            )
            denom = jnp.sum(scores, axis=1, keepdims=True)
            numer = jnp.dot(scores.astype(BF), value_ref[:seen, wide], preferred_element_type=F32)
            numer_ref[rows, wide] = numer.astype(BF)
            stats[t] = jnp.where(lane == h, denom, jnp.where(lane == HEADS + h, top, stats[t]))
    for t in range(BLOCKS):
        stats_ref[t * SPAN : (t + 1) * SPAN, :] = stats[t]
    wait_all(copies[12:])
    gain = gain_ref[:, pl.ds(pl.multiple_of(tp * (HEADS * DV), 128), HEADS * DV)]
    for c in range(2):
        cols = slice(c * HEADS * DV // 2, (c + 1) * HEADS * DV // 2)
        pre = jnp.dot(rows_ref[pl.ds(TAIL, ROWS), :], wo_ref[:, cols], preferred_element_type=F32).astype(BF).astype(F32)
        ogate_ref[:, cols] = (gain[:, cols] / (1.0 + jnp.exp(-pre))).astype(BF)


def hidden_rows(first, query_ref, ogate_ref, state_ref, numer_ref, stats_ref, hidden_ref):
    rows = pl.ds(pl.multiple_of(first, 16), HALF)
    lane = lane_of((HALF, 128))
    stats = stats_ref[rows, :]
    place = lane_of((DQK, 128))
    norms, level = [], jnp.zeros((1, 128), F32)
    for h in range(HEADS):
        extra = state_ref[h * DQK : (h + 1) * DQK, DV:].astype(F32)
        norms.append(jnp.where(place == h, extra[:, 0:1], 0.0).astype(BF))
        mark = extra[0:1, 1:2] + extra[0:1, 2:3] + extra[0:1, 3:4]
        level = jnp.where(lane_of((1, 128)) == h, mark, level)
    norms = jnp.concatenate(norms, axis=0)
    query = query_ref[rows, :]
    read_norm = jnp.dot(query, norms, preferred_element_type=F32)
    top = pltpu.roll(stats, 128 - HEADS, 1)
    carried = pltpu.roll(stats, 128 - 2 * HEADS, 1) + level
    peak = jnp.maximum(carried, top)
    one = jnp.exp(carried - peak)
    two = jnp.exp(top - peak)
    denom = one * read_norm + two * stats
    denom = jnp.maximum(jnp.abs(denom), jnp.exp(-peak))
    one = one / denom
    two = two / denom
    for h in range(HEADS):
        wide = slice(h * DV, (h + 1) * DV)
        read = jnp.dot(
            query[:, h * DQK : (h + 1) * DQK], state_ref[h * DQK : (h + 1) * DQK, :DV], preferred_element_type=F32
        )
        cell = one[:, h : h + 1] * read + two[:, h : h + 1] * numer_ref[rows, wide].astype(F32)
        scale = lax.rsqrt(jnp.mean(cell * cell, axis=-1, keepdims=True) + EPS)
        hidden_ref[:, wide] = (cell * scale * ogate_ref[rows, wide].astype(F32)).astype(BF)


def sent_kernel(query_ref, ogate_ref, state_ref, numer_ref, stats_ref, upper_ref, wout_hbm, out_ref, lower_ref, hidden_ref, sems):
    deep = upper_ref.shape[0]
    copies = started(by_rows(wout_hbm.at[pl.ds(deep, deep)], lower_ref, 4), sems)
    first = (1 - lax.axis_index("tp")) * HALF
    hidden_rows(first, query_ref, ogate_ref, state_ref, numer_ref, stats_ref, hidden_ref)
    part = jnp.dot(hidden_ref[:, :deep], upper_ref[...], preferred_element_type=F32)
    wait_all(copies)
    out_ref[...] = (part + jnp.dot(hidden_ref[:, deep:], lower_ref[...], preferred_element_type=F32)).astype(BF)


def kept_kernel(query_ref, ogate_ref, state_ref, numer_ref, stats_ref, upper_ref, lower_ref, out_ref, hidden_ref):
    deep = upper_ref.shape[0]
    first = lax.axis_index("tp") * HALF
    hidden_rows(first, query_ref, ogate_ref, state_ref, numer_ref, stats_ref, hidden_ref)
    part = jnp.dot(hidden_ref[:, :deep], upper_ref[...], preferred_element_type=F32)
    out_ref[...] = part + jnp.dot(hidden_ref[:, deep:], lower_ref[...], preferred_element_type=F32)


def far_first(stretches):
    at = np.arange(stretches)
    hops = sum(np.minimum(c, 4 - c) for c in (at // 16, at // 4 % 4, at % 4))
    return np.lexsort((at, -hops))


def body(
    tokens, norm_gain, w_query, w_key, w_value, w_ogate, w_igate, w_fgate, conv_query, conv_key, gate_offset, head_gain, w_out
):
    width = tokens.shape[1]
    stretches = lax.axis_size(SP)
    shape = jax.ShapeDtypeStruct
    other = lax.ppermute(tokens, "tp", [(0, 1), (1, 0)])
    last = tokens[HALF - TAIL :]
    to_second = lax.ppermute(last, SP_TP, [(2 * i + 1, 2 * i + 3) for i in range(stretches - 1)])
    to_first = lax.ppermute(last, SP_TP, [(2 * i + 1, 2 * i + 2) for i in range(stretches - 1)])
    gain = norm_gain.reshape(1, -1)
    head_gain = head_gain.reshape(1, -1)
    order = far_first(stretches)
    groups = [[2 * int(i) + t for i in order] for t in range(2)]
    place = np.stack([np.broadcast_to(order[:, None], (stretches, stretches)), np.broadcast_to(order, (stretches, stretches))])
    place = jnp.asarray(place.astype(np.int32))
    v, m, n = pltpu.VMEM, pltpu.HBM, None
    dma = pltpu.SemaphoreType.DMA
    key_shape, value_shape = shape((ROWS, HEADS * DQK), BF), shape((ROWS, HEADS * DV), BF)
    logs_shape = shape((ROWS, 128), F32)
    rows_shape, pre_shape = shape((TAIL + ROWS, width), BF), shape((TAIL + ROWS, HEADS * DQK), F32)

    def room(like):
        return pltpu.VMEM(like.shape, like.dtype)

    own, wk, wv = call(
        fetch_kernel,
        (shape(tokens.shape, BF), shape(w_key.shape, BF), shape(w_value.shape, BF)),
        (v, v, v),
        [m, m, m, m],
        [room(tokens), room(gain), dma((14,))],
        flops=1_000_000_000,
    )(tokens, gain, w_key, w_value)
    key, value, logs, pieces, rows = call(
        summary_kernel,
        (key_shape, value_shape, logs_shape, shape((HEADS * DQK, WIDTH), BF), rows_shape),
        (m, m, m, n, m),
        [v, n, n, n, n, v, v, n, n, n, n],
        [room(rows_shape), room(pre_shape), room(key_shape), room(value_shape), room(logs_shape), pltpu.VMEM((128, width), BF), dma((4,))],
        flops=3_000_000_000,
        limit=12,
    )(own, other, to_first, to_second, gain, wk, wv, w_igate.T, w_fgate.T, conv_key, gate_offset.transpose(1, 0, 2))
    pieces = lax.all_to_all(pieces.reshape(stretches, 8, WIDTH), SP_TP, 0, 0, axis_index_groups=groups, tiled=True)
    query, numer, stats, ogate = call(
        local_kernel,
        (key_shape, value_shape, logs_shape, value_shape),
        (v, v, v, v),
        [m, m, m, m, m, m, n, n],
        [room(rows_shape), room(w_query), room(pre_shape), room(key_shape), room(value_shape), room(logs_shape), room(w_ogate), dma((20,))],
        flops=6_000_000_000,
        limit=16,
    )(rows, w_query, key, value, logs, w_ogate, conv_query, head_gain)
    pieces, query, numer, stats, ogate = lax.optimization_barrier((pieces, query, numer, stats, ogate))
    piece_shape = shape((stretches * 8, WIDTH), BF)
    half_shape = shape((w_out.shape[0] // 2, width), BF)
    state, upper = call(
        prefix_kernel, (piece_shape, half_shape), (n, v), [n, n, m], [dma((4,))], flops=100_000_000
    )(pieces.reshape(piece_shape.shape), place, w_out)
    state = lax.all_to_all(state.reshape(stretches, 8, WIDTH), SP_TP, 0, 0, axis_index_groups=groups, tiled=True)
    state = state.reshape(HEADS * DQK, WIDTH)
    hidden = pltpu.VMEM((HALF, HEADS * DV), BF)
    sent, lower = call(
        sent_kernel,
        (shape((HALF, width), BF), half_shape),
        (n, v),
        [v, v, n, v, v, v, m],
        [hidden, dma((4,))],
        flops=1_000_000_000,
    )(query, ogate, state, numer, stats, upper, w_out)
    got = lax.ppermute(sent, "tp", [(0, 1), (1, 0)])
    kept = call(kept_kernel, shape((HALF, width), F32), n, [v, v, n, v, v, v, v], [hidden], flops=1_000_000_000)(
        query, ogate, state, numer, stats, upper, lower
    )
    return (kept + got.astype(F32)).astype(BF)


def solution(mesh):
    split = Mesh(mesh.devices.reshape(4, 4, 4, mesh.shape["tp"]), ("sp_0", "sp_1", "sp_2", "tp"))
    placed = (
        P(SP_TP, None),
        P(),
        P(None, "tp"),
        P(None, "tp"),
        P(None, "tp"),
        P(None, "tp"),
        P(),
        P(),
        P(),
        P(),
        P(None, SP, "tp"),
        P(),
        P("tp", None),
    )
    return jax.shard_map(body, mesh=split, in_specs=placed, out_specs=P(SP_TP, None), check_vma=False)
```

profile of v0, /device:TPU:1, one launch (start us, length us, event | category | flops | bytes accessed | tf_op | source)
XLA Modules:
  0.0 62.3 jit_solution(7938628118066211346)
XLA Ops:
  0.0 1.4 %collective-permute-start = (bf16[192,2048]{1,0:T(8,128)(2,1)}, bf16[192,2048]{1,0:T(8,128)(2,1)S(1)}, u32[]{:S(2)}, u32[]{:S(2)}) collective-permute-start(bf16[192,2048]{1,0:T(8,128)(2,1)} %own_hbm.1), channel_id=1, source_target_pairs={{0,1},{1,0},{2,3},{3,2},{4,5},{5,4},{6,7},{7,6},{8,9},{9,8},{10,11... | collective-permute-start | bytes 2359304 | tf_op jit(solution)/shard_map/ppermute | solution.py:379
  1.4 0.8 %slice.3 = bf16[16,2048]{1,0:T(8,128)(2,1)S(1)} slice(bf16[192,2048]{1,0:T(8,128)(2,1)} %own_hbm.1), slice={[176:192], [0:2048]} | slice | bytes 131072 | tf_op jit(solution)/shard_map/slice | solution.py:380
  2.2 3.2 %collective-permute-start.2 = (bf16[16,2048]{1,0:T(8,128)(2,1)S(1)}, bf16[16,2048]{1,0:T(8,128)(2,1)S(1)}, u32[]{:S(2)}, u32[]{:S(2)}) collective-permute-start(bf16[16,2048]{1,0:T(8,128)(2,1)S(1)} %slice.3), channel_id=1, source_target_pairs={{1,3},{3,5},{5,7},{7,9},{9,11},{11,13},{13,15},{15,17},{17,19},{19... | collective-permute-start | bytes 196616 | tf_op jit(solution)/shard_map/ppermute | solution.py:381
  5.5 1.3 %collective-permute-start.1 = (bf16[16,2048]{1,0:T(8,128)(2,1)S(1)}, bf16[16,2048]{1,0:T(8,128)(2,1)S(1)}, u32[]{:S(2)}, u32[]{:S(2)}) collective-permute-start(bf16[16,2048]{1,0:T(8,128)(2,1)S(1)} %slice.3), channel_id=1, source_target_pairs={{1,2},{3,4},{5,6},{7,8},{9,10},{11,12},{13,14},{15,16},{17,18},{19... | collective-permute-start | bytes 196616 | tf_op jit(solution)/shard_map/ppermute | solution.py:382
  6.8 0.0 copy-start.1
  6.8 0.0 copy-start.2
  6.8 0.0 copy-start.3
  6.8 0.0 copy-start.4
  6.8 0.0 copy-start.7
  6.8 3.2 %shard_map.136 = (bf16[192,2048]{1,0:T(8,128)(2,1)S(1)}, bf16[2048,512]{1,0:T(8,128)(2,1)S(1)}, bf16[2048,1024]{1,0:T(8,128)(2,1)S(1)}) custom-call(bf16[192,2048]{1,0:T(8,128)(2,1)} %own_hbm.1, f32[1,2048]{1,0:T(1,128)} %bitcast.13, bf16[2048,512]{1,0:T(8,128)(2,1)} %wk_hbm.1, bf16[2048,1024]{1,0:T(8,128)(2,1)} %wv_hbm.1), custom_call_target="tpu_custom_call" | custom-call | flops 1000000000 | bytes 1048576 | tf_op jit(solution)/shard_map/pallas_call | solution.py:51
  10.0 0.0 collective-permute-done.2.two_ref
  10.0 0.0 collective-permute-done.1.one_ref
  10.0 0.0 collective-permute-done.oth_ref
  10.0 0.0 copy-done.1
  10.0 0.0 copy-done.2
  10.0 0.0 copy-done.3
  10.0 0.0 copy-done.4
  10.0 0.0 copy-done.7
  10.1 0.0 copy-start.5
  10.1 0.0 copy-start.6
  10.1 6.0 %shard_map.137 = (bf16[384,512]{1,0:T(8,128)(2,1)}, bf16[384,1024]{1,0:T(8,128)(2,1)}, f32[384,128]{1,0:T(8,128)}, bf16[512,384]{1,0:T(8,128)(2,1)}, bf16[400,2048]{1,0:T(8,128)(2,1)}) custom-call(bf16[192,2048]{1,0:T(8,128)(2,1)S(1)} %get-tuple-element.26.own_ref, bf16[192,2048]{1,0:T(8,128)(2,1)S(1)} %collective-permute-done.oth_ref, ...), custom_call_target="tpu_custom_call" | custom-call | flops 3000000000 | bytes 1048576 | tf_op jit(solution)/shard_map/pallas_call | solution.py:51
  16.1 13.4 %all-to-all-start = ((bf16[64,8,384]{2,1,0:T(8,128)(2,1)}), bf16[64,8,384]{2,1,0:T(8,128)(2,1)S(1)}, u32[]{:S(2)}, u32[]{:S(2)}) async-start(bf16[64,8,384]{2,1,0:T(8,128)(2,1)} %bitcast.4), calls=%async_computation | async-start | bytes 786432 | tf_op jit(solution)/shard_map/all_to_all | solution.py:415
  29.5 0.0 copy-done.5
  29.5 0.0 copy-done.6
  29.5 0.0 copy-start
  29.5 8.0 %shard_map.138 = (bf16[384,512]{1,0:T(8,128)(2,1)S(1)}, bf16[384,1024]{1,0:T(8,128)(2,1)S(1)}, f32[384,128]{1,0:T(8,128)S(1)}, bf16[384,1024]{1,0:T(8,128)(2,1)S(1)}) custom-call(bf16[400,2048]{1,0:T(8,128)(2,1)} %get-tuple-element.30.rows_hbm, bf16[2048,512]{1,0:T(8,128)(2,1)} %wq_hbm.1, bf16[384,512]{1,0:T(8,128)(2,1)} %get-tuple-element.31.key_hbm, ...), custom_call_target="tpu_custom_call" | custom-call | flops 6000000000 | bytes 1048576 | tf_op jit(solution)/shard_map/pallas_call | solution.py:51
  37.6 0.0 all-to-all-done
  37.6 0.0 copy-done
  37.6 1.6 %shard_map.139 = (bf16[512,384]{1,0:T(8,128)(2,1)S(1)}, bf16[512,2048]{1,0:T(8,128)(2,1)S(1)}) custom-call(bf16[512,384]{1,0:T(8,128)(2,1)S(1)} %bitcast.11, s32[2,64,64]{2,1,0:T(8,128)S(1)} %copy-done, bf16[1024,2048]{1,0:T(8,128)(2,1)} %wout_hbm.3), custom_call_target="tpu_custom_call" | custom-call | flops 100000000 | bytes 1048576 | tf_op jit(solution)/shard_map/pallas_call | solution.py:51
  39.2 13.1 %all_to_all.10 = bf16[64,8,384]{2,1,0:T(8,128)(2,1)S(1)} all-to-all(bf16[64,8,384]{2,1,0:T(8,128)(2,1)S(1)} %bitcast.12), channel_id=1, replica_groups={{84,52,76,82,86,92,116,20,44,50,54,60,68,74,78,80,90,94,108,114,118,124..., dimensions={0} | all-to-all | bytes 786432 | tf_op jit(solution)/shard_map/all_to_all | solution.py:431
  52.3 3.3 %shard_map.140 = (bf16[192,2048]{1,0:T(8,128)(2,1)S(1)}, bf16[512,2048]{1,0:T(8,128)(2,1)S(1)}) custom-call(bf16[384,512]{1,0:T(8,128)(2,1)S(1)} %get-tuple-element.38.query_ref, bf16[384,1024]{1,0:T(8,128)(2,1)S(1)} %get-tuple-element.39.ogate_ref, bf16[512,384]{1,0:T(8,128)(2,1)S(1)} %bitcast.9, bf16[384,1024]{1,0:T(8,128)(2,1)S(1)} %get-tuple-element.42.numer_ref, ...), custom_call_target="tpu_custom_call" | custom-call | flops 1000000000 | bytes 1048576 | tf_op jit(solution)/shard_map/pallas_call | solution.py:51
  55.6 3.8 %collective-permute-start.3 = (bf16[192,2048]{1,0:T(8,128)(2,1)S(1)}, bf16[192,2048]{1,0:T(8,128)(2,1)S(1)}, u32[]{:S(2)}, u32[]{:S(2)}) collective-permute-start(bf16[192,2048]{1,0:T(8,128)(2,1)S(1)} %get-tuple-element.46), channel_id=1, source_target_pairs={{0,1},{1,0},{2,3},{3,2},{4,5},{5,4},{6,7},{7,6},{8,9},{9,8},{10,11... | collective-permute-start | bytes 2359304 | tf_op jit(solution)/shard_map/ppermute | solution.py:442
  59.3 1.7 %shard_map.141 = f32[192,2048]{1,0:T(8,128)S(1)} custom-call(bf16[384,512]{1,0:T(8,128)(2,1)S(1)} %get-tuple-element.38.query_ref, bf16[384,1024]{1,0:T(8,128)(2,1)S(1)} %get-tuple-element.39.ogate_ref, bf16[512,384]{1,0:T(8,128)(2,1)S(1)} %bitcast.10, bf16[384,1024]{1,0:T(8,128)(2,1)S(1)} %get-tuple-element.42.numer_ref, ...), custom_call_target="tpu_custom_call" | custom-call | flops 1000000000 | bytes 1048576 | tf_op jit(solution)/shard_map/pallas_call | solution.py:51
  61.0 0.2 collective-permute-done.3
  61.2 1.1 %add_convert_fusion = bf16[192,2048]{1,0:T(8,128)(2,1)} fusion(f32[192,2048]{1,0:T(8,128)S(1)} %shard_map.141, bf16[192,2048]{1,0:T(8,128)(2,1)S(1)} %collective-permute-done.3), kind=kLoop, calls=%fused_computation | loop fusion | flops 1179648 | bytes 3145728 | tf_op jit(solution)/shard_map/convert_element_type | solution.py:446
Async XLA Ops:
  0.0 10.0 %collective-permute-start = (bf16[192,2048]{1,0:T(8,128)(2,1)}, bf16[192,2048]{1,0:T(8,128)(2,1)S(1)}, u32[]{:S(2)}, u32[]{:S(2)}) collective-permute-start(bf16[192,2048]{1,0:T(8,128)(2,1)} %own_hbm.1), channel_id=1, source_target_pairs={{0,1},{1,0},{2,3},{3,2},{4,5},{5,4},{6,7},{7,6},{8,9},{9,8},{10,11... | collective-permute-start | bytes 2359304 | tf_op jit(solution)/shard_map/ppermute | solution.py:379
  2.2 7.8 %collective-permute-start.2 = (bf16[16,2048]{1,0:T(8,128)(2,1)S(1)}, bf16[16,2048]{1,0:T(8,128)(2,1)S(1)}, u32[]{:S(2)}, u32[]{:S(2)}) collective-permute-start(bf16[16,2048]{1,0:T(8,128)(2,1)S(1)} %slice.3), channel_id=1, source_target_pairs={{1,3},{3,5},{5,7},{7,9},{9,11},{11,13},{13,15},{15,17},{17,19},{19... | collective-permute-start | bytes 196616 | tf_op jit(solution)/shard_map/ppermute | solution.py:381
  5.5 4.5 %collective-permute-start.1 = (bf16[16,2048]{1,0:T(8,128)(2,1)S(1)}, bf16[16,2048]{1,0:T(8,128)(2,1)S(1)}, u32[]{:S(2)}, u32[]{:S(2)}) collective-permute-start(bf16[16,2048]{1,0:T(8,128)(2,1)S(1)} %slice.3), channel_id=1, source_target_pairs={{1,2},{3,4},{5,6},{7,8},{9,10},{11,12},{13,14},{15,16},{17,18},{19... | collective-permute-start | bytes 196616 | tf_op jit(solution)/shard_map/ppermute | solution.py:382
  6.8 3.3 %copy-start.1 = (f32[2048]{0:T(1024)S(1)}, f32[2048]{0:T(1024)}, u32[]{:S(2)}) copy-start(f32[2048]{0:T(1024)} %param.15) | copy-start | bytes 24580
  6.8 3.3 %copy-start.2 = (bf16[2048,8]{0,1:T(8,128)(2,1)S(1)}, bf16[2048,8]{0,1:T(8,128)(2,1)}, u32[]{:S(2)}) copy-start(bf16[2048,8]{0,1:T(8,128)(2,1)} %param.20) | copy-start | bytes 98308
  6.8 3.3 %copy-start.3 = (bf16[2048,8]{0,1:T(8,128)(2,1)S(1)}, bf16[2048,8]{0,1:T(8,128)(2,1)}, u32[]{:S(2)}) copy-start(bf16[2048,8]{0,1:T(8,128)(2,1)} %param.21) | copy-start | bytes 98308
  6.8 3.2 %copy-start.4 = (bf16[4,1024]{1,0:T(4,128)(2,1)S(1)}, bf16[4,1024]{1,0:T(4,128)(2,1)}, u32[]{:S(2)}) copy-start(bf16[4,1024]{1,0:T(4,128)(2,1)} %taps_ref.2) | copy-start | bytes 24580
  6.8 3.2 %copy-start.7 = (f32[2,3,4]{2,0,1:T(2,128)S(1)}, f32[2,3,4]{2,0,1:T(2,128)}, u32[]{:S(2)}) copy-start(f32[2,3,4]{2,0,1:T(2,128)} %param.24) | copy-start | bytes 292
  10.1 19.5 %copy-start.5 = (bf16[4,1024]{1,0:T(4,128)(2,1)S(1)}, bf16[4,1024]{1,0:T(4,128)(2,1)}, u32[]{:S(2)}) copy-start(bf16[4,1024]{1,0:T(4,128)(2,1)} %taps_ref.3) | copy-start | bytes 24580
  10.1 19.5 %copy-start.6 = (f32[2048]{0:T(1024)S(1)}, f32[2048]{0:T(1024)}, u32[]{:S(2)}) copy-start(f32[2048]{0:T(1024)} %param.25) | copy-start | bytes 24580
  16.1 21.5 %all-to-all-start = ((bf16[64,8,384]{2,1,0:T(8,128)(2,1)}), bf16[64,8,384]{2,1,0:T(8,128)(2,1)S(1)}, u32[]{:S(2)}, u32[]{:S(2)}) async-start(bf16[64,8,384]{2,1,0:T(8,128)(2,1)} %bitcast.4), calls=%async_computation | async-start | bytes 786432 | tf_op jit(solution)/shard_map/all_to_all | solution.py:415
  29.5 8.1 %copy-start = (s32[2,64,64]{2,1,0:T(8,128)S(1)}, s32[2,64,64]{2,1,0:T(8,128)}, u32[]{:S(2)}) copy-start(s32[2,64,64]{2,1,0:T(8,128)} %constant.2.clone.place_ref) | copy-start | bytes 98308
  55.6 5.7 %collective-permute-start.3 = (bf16[192,2048]{1,0:T(8,128)(2,1)S(1)}, bf16[192,2048]{1,0:T(8,128)(2,1)S(1)}, u32[]{:S(2)}, u32[]{:S(2)}) collective-permute-start(bf16[192,2048]{1,0:T(8,128)(2,1)S(1)} %get-tuple-element.46), channel_id=1, source_target_pairs={{0,1},{1,0},{2,3},{3,2},{4,5},{5,4},{6,7},{7,6},{8,9},{9,8},{10,11... | collective-permute-start | bytes 2359304 | tf_op jit(solution)/shard_map/ppermute | solution.py:442
where the time goes:
time: 62.7 us; the launch traced here: 62.3 us
  Pallas kernels  23.7 us (38%)
  starting transfers between devices  23.1 us (37%)
  blocking collectives  13.1 us (21%)
  other arithmetic  1.07 us (2%)
  local copies, waits for them, and re-layouts  0.89 us (1%)
    pallas_call x6, Pallas kernels, call(): return lambda *args: run(*map(kept, args, spaces))  23.7 us
    all_to_all x1, starting transfers between devices, body(): lax.all_to_all(pieces.reshape(stretches, 8, WIDTH), SP_TP, 0, 0, axis_ind...  13.4 us
    all_to_all x1, blocking collectives, body(): lax.all_to_all(state.reshape(stretches, 8, WIDTH), SP_TP, 0, 0, axis_inde...  13.1 us
    ppermute x1, starting transfers between devices, body(): got = lax.ppermute(sent, 'tp', [(0, 1), (1, 0)])  3.76 us
    ppermute x1, starting transfers between devices, body(): lax.ppermute(last, SP_TP, [(2 * i + 1, 2 * i + 3) for i in range(stretche...  3.22 us
    ppermute x1, starting transfers between devices, body(): other = lax.ppermute(tokens, 'tp', [(0, 1), (1, 0)])  1.38 us
    ppermute x1, starting transfers between devices, body(): lax.ppermute(last, SP_TP, [(2 * i + 1, 2 * i + 2) for i in range(stretche...  1.29 us
  transfers between devices with their start and end apart: 5, of which 1 were waited for; matrix products, arithmetic and copies ran while one was open for 1% of the time, Pallas kernels for 21%

commit v1 on v0

--- a/solution.py
+++ b/solution.py
@@ -196,8 +196,7 @@
         copy.wait()
 
 
-def prefix_kernel(piece_ref, place_ref, wout_hbm, out_ref, wout_ref, sems):
-    copies = started(by_rows(wout_hbm.at[pl.ds(0, wout_ref.shape[0])], wout_ref, 4), sems)
+def prefix_kernel(piece_ref, place_ref, out_ref):
     count = piece_ref.shape[0] // 8
     tall = piece_ref.shape[0]
 
@@ -238,7 +237,6 @@
     lane = lane_of((tall, 128))
     out_ref[:, :DV] = state[:, :DV].astype(BF)
     out_ref[:, DV:] = jnp.where((lane >= 1) & (lane < 4), marks, state[:, DV:]).astype(BF)
-    wait_all(copies)
 
 
 def local_kernel(rows_hbm, wq_hbm, key_hbm, value_hbm, logs_hbm, wo_hbm, taps_ref, gain_ref,
@@ -346,22 +344,21 @@
         hidden_ref[:, wide] = (cell * scale * ogate_ref[rows, wide].astype(F32)).astype(BF)
 
 
-def sent_kernel(query_ref, ogate_ref, state_ref, numer_ref, stats_ref, upper_ref, wout_hbm, out_ref, lower_ref, hidden_ref, sems):
-    deep = upper_ref.shape[0]
-    copies = started(by_rows(wout_hbm.at[pl.ds(deep, deep)], lower_ref, 4), sems)
+def sent_kernel(query_ref, ogate_ref, state_ref, numer_ref, stats_ref, wout_hbm, out_ref, wout_ref, hidden_ref, sems):
+    deep = HEADS * DV // 2
+    copies = started(by_rows(wout_hbm, wout_ref, 8), sems)
     first = (1 - lax.axis_index("tp")) * HALF
     hidden_rows(first, query_ref, ogate_ref, state_ref, numer_ref, stats_ref, hidden_ref)
-    part = jnp.dot(hidden_ref[:, :deep], upper_ref[...], preferred_element_type=F32)
-    wait_all(copies)
-    out_ref[...] = (part + jnp.dot(hidden_ref[:, deep:], lower_ref[...], preferred_element_type=F32)).astype(BF)
-
-
-def kept_kernel(query_ref, ogate_ref, state_ref, numer_ref, stats_ref, upper_ref, lower_ref, out_ref, hidden_ref):
-    deep = upper_ref.shape[0]
+    wait_all(copies[:4])
+    part = jnp.dot(hidden_ref[:, :deep], wout_ref[:deep, :], preferred_element_type=F32)
+    wait_all(copies[4:])
+    out_ref[...] = (part + jnp.dot(hidden_ref[:, deep:], wout_ref[deep:, :], preferred_element_type=F32)).astype(BF)
+
+
+def kept_kernel(query_ref, ogate_ref, state_ref, numer_ref, stats_ref, wout_ref, out_ref, hidden_ref):
     first = lax.axis_index("tp") * HALF
     hidden_rows(first, query_ref, ogate_ref, state_ref, numer_ref, stats_ref, hidden_ref)
-    part = jnp.dot(hidden_ref[:, :deep], upper_ref[...], preferred_element_type=F32)
-    out_ref[...] = part + jnp.dot(hidden_ref[:, deep:], lower_ref[...], preferred_element_type=F32)
+    out_ref[...] = jnp.dot(hidden_ref[...], wout_ref[...], preferred_element_type=F32)
 
 
 def far_first(stretches):
@@ -413,6 +410,11 @@
         limit=12,
     )(own, other, to_first, to_second, gain, wk, wv, w_igate.T, w_fgate.T, conv_key, gate_offset.transpose(1, 0, 2))
     pieces = lax.all_to_all(pieces.reshape(stretches, 8, WIDTH), SP_TP, 0, 0, axis_index_groups=groups, tiled=True)
+    piece_shape = shape((stretches * 8, WIDTH), BF)
+    state = call(prefix_kernel, piece_shape, n, [n, n], flops=100_000_000)(pieces.reshape(piece_shape.shape), place)
+    state, rows = lax.optimization_barrier((state, rows))
+    state = lax.all_to_all(state.reshape(stretches, 8, WIDTH), SP_TP, 0, 0, axis_index_groups=groups, tiled=True)
+    state = state.reshape(HEADS * DQK, WIDTH)
     query, numer, stats, ogate = call(
         local_kernel,
         (key_shape, value_shape, logs_shape, value_shape),
@@ -422,26 +424,18 @@
         flops=6_000_000_000,
         limit=16,
     )(rows, w_query, key, value, logs, w_ogate, conv_query, head_gain)
-    pieces, query, numer, stats, ogate = lax.optimization_barrier((pieces, query, numer, stats, ogate))
-    piece_shape = shape((stretches * 8, WIDTH), BF)
-    half_shape = shape((w_out.shape[0] // 2, width), BF)
-    state, upper = call(
-        prefix_kernel, (piece_shape, half_shape), (n, v), [n, n, m], [dma((4,))], flops=100_000_000
-    )(pieces.reshape(piece_shape.shape), place, w_out)
-    state = lax.all_to_all(state.reshape(stretches, 8, WIDTH), SP_TP, 0, 0, axis_index_groups=groups, tiled=True)
-    state = state.reshape(HEADS * DQK, WIDTH)
     hidden = pltpu.VMEM((HALF, HEADS * DV), BF)
-    sent, lower = call(
+    sent, wout = call(
         sent_kernel,
-        (shape((HALF, width), BF), half_shape),
+        (shape((HALF, width), BF), shape(w_out.shape, BF)),
         (n, v),
-        [v, v, n, v, v, v, m],
-        [hidden, dma((4,))],
+        [v, v, n, v, v, m],
+        [hidden, dma((8,))],
         flops=1_000_000_000,
-    )(query, ogate, state, numer, stats, upper, w_out)
+    )(query, ogate, state, numer, stats, w_out)
     got = lax.ppermute(sent, "tp", [(0, 1), (1, 0)])
-    kept = call(kept_kernel, shape((HALF, width), F32), n, [v, v, n, v, v, v, v], [hidden], flops=1_000_000_000)(
-        query, ogate, state, numer, stats, upper, lower
+    kept = call(kept_kernel, shape((HALF, width), F32), n, [v, v, n, v, v, v], [hidden], flops=1_000_000_000)(
+        query, ogate, state, numer, stats, wout
     )
     return (kept + got.astype(F32)).astype(BF)
 

time: 62.7 us -> 64.9 us (1.035)
  blocking collectives: 13.1 us -> 16.7 us
  starting transfers between devices: 23.1 us -> 20.9 us
  Pallas kernels: 23.7 us -> 24.9 us
    all_to_all x1, blocking collectives: 13.1 us -> 16.7 us  [body(): lax.all_to_all(pieces.reshape(stretches, 8, WIDTH), SP_TP, 0, 0, axis_ind...]
    all_to_all x1, starting transfers between devices: 13.4 us -> 11.2 us  [body(): lax.all_to_all(state.reshape(stretches, 8, WIDTH), SP_TP, 0, 0, axis_inde...]
    pallas_call x6, Pallas kernels: 23.7 us -> 24.9 us  [call(): return lambda *args: run(*map(kept, args, spaces))]
  transfers between devices with their start and end apart: 5 -> 5, of which waited for: 1 -> 0; matrix products, arithmetic and copies ran while one was open for 1% -> 1% of each run, Pallas kernels for 21% -> 20%
where the time goes in v1:
time: 64.9 us; the launch traced here: 64.6 us
  Pallas kernels  24.9 us (38%)
  starting transfers between devices  20.9 us (32%)
  blocking collectives  16.7 us (26%)
  other arithmetic  1.09 us (2%)
  local copies, waits for them, and re-layouts  0.89 us (1%)
    pallas_call x6, Pallas kernels, call(): return lambda *args: run(*map(kept, args, spaces))  24.9 us
    all_to_all x1, blocking collectives, body(): lax.all_to_all(pieces.reshape(stretches, 8, WIDTH), SP_TP, 0, 0, axis_ind...  16.7 us
    all_to_all x1, starting transfers between devices, body(): lax.all_to_all(state.reshape(stretches, 8, WIDTH), SP_TP, 0, 0, axis_inde...  11.2 us
    ppermute x1, starting transfers between devices, body(): got = lax.ppermute(sent, 'tp', [(0, 1), (1, 0)])  3.76 us
    ppermute x1, starting transfers between devices, body(): lax.ppermute(last, SP_TP, [(2 * i + 1, 2 * i + 3) for i in range(stretche...  3.22 us
    ppermute x1, starting transfers between devices, body(): other = lax.ppermute(tokens, 'tp', [(0, 1), (1, 0)])  1.38 us
  transfers between devices with their start and end apart: 5, of which 0 were waited for; matrix products, arithmetic and copies ran while one was open for 1% of the time, Pallas kernels for 20%

profile of v1, /device:TPU:1, one launch (start us, length us, event | category | flops | bytes accessed | tf_op | source)
XLA Modules:
  0.0 64.6 jit_solution(1874826408374262689)
XLA Ops:
  0.0 1.4 %collective-permute-start = (bf16[192,2048]{1,0:T(8,128)(2,1)}, bf16[192,2048]{1,0:T(8,128)(2,1)S(1)}, u32[]{:S(2)}, u32[]{:S(2)}) collective-permute-start(bf16[192,2048]{1,0:T(8,128)(2,1)} %own_hbm.1), channel_id=1, source_target_pairs={{0,1},{1,0},{2,3},{3,2},{4,5},{5,4},{6,7},{7,6},{8,9},{9,8},{10,11... | collective-permute-start | bytes 2359304 | tf_op jit(solution)/shard_map/ppermute | solution.py:376
  1.4 0.8 %slice.3 = bf16[16,2048]{1,0:T(8,128)(2,1)S(1)} slice(bf16[192,2048]{1,0:T(8,128)(2,1)} %own_hbm.1), slice={[176:192], [0:2048]} | slice | bytes 131072 | tf_op jit(solution)/shard_map/slice | solution.py:377
  2.2 3.2 %collective-permute-start.2 = (bf16[16,2048]{1,0:T(8,128)(2,1)S(1)}, bf16[16,2048]{1,0:T(8,128)(2,1)S(1)}, u32[]{:S(2)}, u32[]{:S(2)}) collective-permute-start(bf16[16,2048]{1,0:T(8,128)(2,1)S(1)} %slice.3), channel_id=1, source_target_pairs={{1,3},{3,5},{5,7},{7,9},{9,11},{11,13},{13,15},{15,17},{17,19},{19... | collective-permute-start | bytes 196616 | tf_op jit(solution)/shard_map/ppermute | solution.py:378
  5.5 1.3 %collective-permute-start.1 = (bf16[16,2048]{1,0:T(8,128)(2,1)S(1)}, bf16[16,2048]{1,0:T(8,128)(2,1)S(1)}, u32[]{:S(2)}, u32[]{:S(2)}) collective-permute-start(bf16[16,2048]{1,0:T(8,128)(2,1)S(1)} %slice.3), channel_id=1, source_target_pairs={{1,2},{3,4},{5,6},{7,8},{9,10},{11,12},{13,14},{15,16},{17,18},{19... | collective-permute-start | bytes 196616 | tf_op jit(solution)/shard_map/ppermute | solution.py:379
  6.8 0.0 copy-start.1
  6.8 0.0 copy-start.2
  6.8 0.0 copy-start.3
  6.8 0.0 copy-start.4
  6.8 0.0 copy-start.7
  6.8 3.2 %shard_map.136 = (bf16[192,2048]{1,0:T(8,128)(2,1)S(1)}, bf16[2048,512]{1,0:T(8,128)(2,1)S(1)}, bf16[2048,1024]{1,0:T(8,128)(2,1)S(1)}) custom-call(bf16[192,2048]{1,0:T(8,128)(2,1)} %own_hbm.1, f32[1,2048]{1,0:T(1,128)} %bitcast.13, bf16[2048,512]{1,0:T(8,128)(2,1)} %wk_hbm.1, bf16[2048,1024]{1,0:T(8,128)(2,1)} %wv_hbm.1), custom_call_target="tpu_custom_call" | custom-call | flops 1000000000 | bytes 1048576 | tf_op jit(solution)/shard_map/pallas_call | solution.py:51
  10.0 0.0 collective-permute-done.2.two_ref
  10.0 0.0 collective-permute-done.1.one_ref
  10.0 0.0 collective-permute-done.oth_ref
  10.0 0.0 copy-done.1
  10.0 0.0 copy-done.2
  10.0 0.0 copy-done.3
  10.0 0.0 copy-done.4
  10.0 0.0 copy-done.7
  10.1 0.0 copy-start
  10.1 5.8 %shard_map.137 = (bf16[384,512]{1,0:T(8,128)(2,1)}, bf16[384,1024]{1,0:T(8,128)(2,1)}, f32[384,128]{1,0:T(8,128)}, bf16[512,384]{1,0:T(8,128)(2,1)S(1)}, bf16[400,2048]{1,0:T(8,128)(2,1)}) custom-call(bf16[192,2048]{1,0:T(8,128)(2,1)S(1)} %get-tuple-element.21.own_ref, bf16[192,2048]{1,0:T(8,128)(2,1)S(1)} %collective-permute-done.oth_ref, ...), custom_call_target="tpu_custom_call" | custom-call | flops 3000000000 | bytes 1048576 | tf_op jit(solution)/shard_map/pallas_call | solution.py:51
  15.9 0.0 copy-start.5
  15.9 0.0 copy-start.6
  15.9 16.7 %all_to_all.10 = bf16[64,8,384]{2,1,0:T(8,128)(2,1)S(1)} all-to-all(bf16[64,8,384]{2,1,0:T(8,128)(2,1)S(1)} %bitcast.12), channel_id=1, replica_groups={{84,52,76,82,86,92,116,20,44,50,54,60,68,74,78,80,90,94,108,114,118,124..., dimensions={0} | all-to-all | bytes 786432 | tf_op jit(solution)/shard_map/all_to_all | solution.py:412
  32.6 0.0 copy-done
  32.6 2.0 %shard_map.138 = bf16[512,384]{1,0:T(8,128)(2,1)} custom-call(bf16[512,384]{1,0:T(8,128)(2,1)S(1)} %bitcast.11, s32[2,64,64]{2,1,0:T(8,128)S(1)} %copy-done), custom_call_target="tpu_custom_call" | custom-call | flops 100000000 | bytes 1048576 | tf_op jit(solution)/shard_map/pallas_call | solution.py:51
  34.5 11.2 %all-to-all-start.1 = ((bf16[64,8,384]{2,1,0:T(8,128)(2,1)}), bf16[64,8,384]{2,1,0:T(8,128)(2,1)S(1)}, u32[]{:S(2)}, u32[]{:S(2)}) async-start(bf16[64,8,384]{2,1,0:T(8,128)(2,1)} %bitcast.7), calls=%async_computation.1 | async-start | bytes 786432 | tf_op jit(solution)/shard_map/all_to_all | solution.py:416
  45.7 0.0 copy-done.5
  45.8 0.0 copy-done.6
  45.8 8.0 %shard_map.139 = (bf16[384,512]{1,0:T(8,128)(2,1)S(1)}, bf16[384,1024]{1,0:T(8,128)(2,1)S(1)}, f32[384,128]{1,0:T(8,128)S(1)}, bf16[384,1024]{1,0:T(8,128)(2,1)S(1)}) custom-call(bf16[400,2048]{1,0:T(8,128)(2,1)} %get-tuple-element.26.rows_hbm, bf16[2048,512]{1,0:T(8,128)(2,1)} %wq_hbm.1, bf16[384,512]{1,0:T(8,128)(2,1)} %get-tuple-element.27.key_hbm, ...), custom_call_target="tpu_custom_call" | custom-call | flops 6000000000 | bytes 1048576 | tf_op jit(solution)/shard_map/pallas_call | solution.py:51
  53.8 0.0 all-to-all-done.1
  53.8 3.9 %shard_map.140 = (bf16[192,2048]{1,0:T(8,128)(2,1)S(1)}, bf16[1024,2048]{1,0:T(8,128)(2,1)S(1)}) custom-call(bf16[384,512]{1,0:T(8,128)(2,1)S(1)} %get-tuple-element.30.query_ref, bf16[384,1024]{1,0:T(8,128)(2,1)S(1)} %get-tuple-element.31.ogate_ref, bf16[512,384]{1,0:T(8,128)(2,1)S(1)} %bitcast.9, bf16[384,1024]{1,0:T(8,128)(2,1)S(1)} %get-tuple-element.33.numer_ref, ...), custom_call_target="tpu_custom_call" | custom-call | flops 1000000000 | bytes 1048576 | tf_op jit(solution)/shard_map/pallas_call | solution.py:51
  57.7 3.8 %collective-permute-start.3 = (bf16[192,2048]{1,0:T(8,128)(2,1)S(1)}, bf16[192,2048]{1,0:T(8,128)(2,1)S(1)}, u32[]{:S(2)}, u32[]{:S(2)}) collective-permute-start(bf16[192,2048]{1,0:T(8,128)(2,1)S(1)} %get-tuple-element.36), channel_id=1, source_target_pairs={{0,1},{1,0},{2,3},{3,2},{4,5},{5,4},{6,7},{7,6},{8,9},{9,8},{10,11... | collective-permute-start | bytes 2359304 | tf_op jit(solution)/shard_map/ppermute | solution.py:436
  61.5 2.0 %shard_map.141 = f32[192,2048]{1,0:T(8,128)S(1)} custom-call(bf16[384,512]{1,0:T(8,128)(2,1)S(1)} %get-tuple-element.30.query_ref, bf16[384,1024]{1,0:T(8,128)(2,1)S(1)} %get-tuple-element.31.ogate_ref, bf16[512,384]{1,0:T(8,128)(2,1)S(1)} %bitcast.10, bf16[384,1024]{1,0:T(8,128)(2,1)S(1)} %get-tuple-element.33.numer_ref, ...), custom_call_target="tpu_custom_call" | custom-call | flops 1000000000 | bytes 1048576 | tf_op jit(solution)/shard_map/pallas_call | solution.py:51
  63.5 0.0 collective-permute-done.3
  63.5 1.1 %add_convert_fusion = bf16[192,2048]{1,0:T(8,128)(2,1)} fusion(f32[192,2048]{1,0:T(8,128)S(1)} %shard_map.141, bf16[192,2048]{1,0:T(8,128)(2,1)S(1)} %collective-permute-done.3), kind=kLoop, calls=%fused_computation | loop fusion | flops 1179648 | bytes 3145728 | tf_op jit(solution)/shard_map/convert_element_type | solution.py:440
Async XLA Ops:
  0.0 10.0 %collective-permute-start = (bf16[192,2048]{1,0:T(8,128)(2,1)}, bf16[192,2048]{1,0:T(8,128)(2,1)S(1)}, u32[]{:S(2)}, u32[]{:S(2)}) collective-permute-start(bf16[192,2048]{1,0:T(8,128)(2,1)} %own_hbm.1), channel_id=1, source_target_pairs={{0,1},{1,0},{2,3},{3,2},{4,5},{5,4},{6,7},{7,6},{8,9},{9,8},{10,11... | collective-permute-start | bytes 2359304 | tf_op jit(solution)/shard_map/ppermute | solution.py:376
  2.2 7.8 %collective-permute-start.2 = (bf16[16,2048]{1,0:T(8,128)(2,1)S(1)}, bf16[16,2048]{1,0:T(8,128)(2,1)S(1)}, u32[]{:S(2)}, u32[]{:S(2)}) collective-permute-start(bf16[16,2048]{1,0:T(8,128)(2,1)S(1)} %slice.3), channel_id=1, source_target_pairs={{1,3},{3,5},{5,7},{7,9},{9,11},{11,13},{13,15},{15,17},{17,19},{19... | collective-permute-start | bytes 196616 | tf_op jit(solution)/shard_map/ppermute | solution.py:378
  5.5 4.5 %collective-permute-start.1 = (bf16[16,2048]{1,0:T(8,128)(2,1)S(1)}, bf16[16,2048]{1,0:T(8,128)(2,1)S(1)}, u32[]{:S(2)}, u32[]{:S(2)}) collective-permute-start(bf16[16,2048]{1,0:T(8,128)(2,1)S(1)} %slice.3), channel_id=1, source_target_pairs={{1,2},{3,4},{5,6},{7,8},{9,10},{11,12},{13,14},{15,16},{17,18},{19... | collective-permute-start | bytes 196616 | tf_op jit(solution)/shard_map/ppermute | solution.py:379
  6.8 3.3 %copy-start.1 = (f32[2048]{0:T(1024)S(1)}, f32[2048]{0:T(1024)}, u32[]{:S(2)}) copy-start(f32[2048]{0:T(1024)} %param.15) | copy-start | bytes 24580
  6.8 3.3 %copy-start.2 = (bf16[2048,8]{0,1:T(8,128)(2,1)S(1)}, bf16[2048,8]{0,1:T(8,128)(2,1)}, u32[]{:S(2)}) copy-start(bf16[2048,8]{0,1:T(8,128)(2,1)} %param.20) | copy-start | bytes 98308
  6.8 3.3 %copy-start.3 = (bf16[2048,8]{0,1:T(8,128)(2,1)S(1)}, bf16[2048,8]{0,1:T(8,128)(2,1)}, u32[]{:S(2)}) copy-start(bf16[2048,8]{0,1:T(8,128)(2,1)} %param.21) | copy-start | bytes 98308
  6.8 3.2 %copy-start.4 = (bf16[4,1024]{1,0:T(4,128)(2,1)S(1)}, bf16[4,1024]{1,0:T(4,128)(2,1)}, u32[]{:S(2)}) copy-start(bf16[4,1024]{1,0:T(4,128)(2,1)} %taps_ref.2) | copy-start | bytes 24580
  6.8 3.2 %copy-start.7 = (f32[2,3,4]{2,0,1:T(2,128)S(1)}, f32[2,3,4]{2,0,1:T(2,128)}, u32[]{:S(2)}) copy-start(f32[2,3,4]{2,0,1:T(2,128)} %param.24) | copy-start | bytes 292
  10.1 22.5 %copy-start = (s32[2,64,64]{2,1,0:T(8,128)S(1)}, s32[2,64,64]{2,1,0:T(8,128)}, u32[]{:S(2)}) copy-start(s32[2,64,64]{2,1,0:T(8,128)} %constant.2.clone.place_ref) | copy-start | bytes 98308
  15.9 29.9 %copy-start.5 = (bf16[4,1024]{1,0:T(4,128)(2,1)S(1)}, bf16[4,1024]{1,0:T(4,128)(2,1)}, u32[]{:S(2)}) copy-start(bf16[4,1024]{1,0:T(4,128)(2,1)} %taps_ref.3) | copy-start | bytes 24580
  15.9 29.9 %copy-start.6 = (f32[2048]{0:T(1024)S(1)}, f32[2048]{0:T(1024)}, u32[]{:S(2)}) copy-start(f32[2048]{0:T(1024)} %param.25) | copy-start | bytes 24580
  34.5 19.2 %all-to-all-start.1 = ((bf16[64,8,384]{2,1,0:T(8,128)(2,1)}), bf16[64,8,384]{2,1,0:T(8,128)(2,1)S(1)}, u32[]{:S(2)}, u32[]{:S(2)}) async-start(bf16[64,8,384]{2,1,0:T(8,128)(2,1)} %bitcast.7), calls=%async_computation.1 | async-start | bytes 786432 | tf_op jit(solution)/shard_map/all_to_all | solution.py:416
  57.7 5.8 %collective-permute-start.3 = (bf16[192,2048]{1,0:T(8,128)(2,1)S(1)}, bf16[192,2048]{1,0:T(8,128)(2,1)S(1)}, u32[]{:S(2)}, u32[]{:S(2)}) collective-permute-start(bf16[192,2048]{1,0:T(8,128)(2,1)S(1)} %get-tuple-element.36), channel_id=1, source_target_pairs={{0,1},{1,0},{2,3},{3,2},{4,5},{5,4},{6,7},{7,6},{8,9},{9,8},{10,11... | collective-permute-start | bytes 2359304 | tf_op jit(solution)/shard_map/ppermute | solution.py:436

commit v2 on v0

--- a/solution.py
+++ b/solution.py
@@ -96,10 +96,8 @@
     return (x * row_scale(x) * gain).astype(BF)
 
 
-def fetch_kernel(own_hbm, gain_hbm, wk_hbm, wv_hbm, rows_ref, wk_ref, wv_ref, own_ref, gain_ref, sems):
-    copies = started(
-        [(own_hbm, own_ref), (gain_hbm, gain_ref)] + by_rows(wk_hbm, wk_ref, 4) + by_rows(wv_hbm, wv_ref, 8), sems
-    )
+def fetch_kernel(own_hbm, gain_hbm, wk_hbm, rows_ref, wk_ref, own_ref, gain_ref, sems):
+    copies = started([(own_hbm, own_ref), (gain_hbm, gain_ref)] + by_rows(wk_hbm, wk_ref, 4), sems)
     copies[0].wait()
     parts = [slice(at, at + 48) for at in range(0, HALF, 48)]
     scales = [row_scale(own_ref[part, :].astype(F32)) for part in parts]
@@ -110,9 +108,10 @@
     wait_all(copies[2:])
 
 
-def summary_kernel(own_ref, oth_ref, one_ref, two_ref, gain_ref, wk_ref, wv_ref, wi_ref, wf_ref, taps_ref, offs_ref,
+def summary_kernel(own_ref, oth_ref, one_ref, two_ref, gain_ref, wk_ref, wv_hbm, wi_ref, wf_ref, taps_ref, offs_ref,
                    key_out, value_out, logs_out, piece_ref, rows_out,
-                   rows_ref, pre_ref, key_ref, value_ref, logs_ref, wg_ref, sems):
+                   rows_ref, pre_ref, key_ref, value_ref, logs_ref, wg_ref, wv_ref, sems, in_sems):
+    copies = started(by_rows(wv_hbm, wv_ref, 8), in_sems)
     outs = [
         pltpu.make_async_copy(src, dst, sems.at[n])
         for n, (src, dst) in enumerate(
@@ -136,6 +135,7 @@
     gates = lax.dot_general(rows_ref[own, :], wg_ref[...], (((1,), (1,)), ((), ())), preferred_element_type=F32)
     gates = jnp.where(tp == 0, gates, pltpu.roll(gates, 128 - HEADS, 1))
     pre_ref[...] = jnp.dot(rows_ref[...], wk_ref[...], preferred_element_type=F32).astype(BF).astype(F32)
+    wait_all(copies)
 
     lane = lane_of((SPAN, 128))
     tri = (lax.broadcasted_iota(jnp.int32, (SPAN, SPAN), 0) >= lax.broadcasted_iota(jnp.int32, (SPAN, SPAN), 1)).astype(F32)
@@ -395,23 +395,23 @@
     def room(like):
         return pltpu.VMEM(like.shape, like.dtype)
 
-    own, wk, wv = call(
+    own, wk = call(
         fetch_kernel,
-        (shape(tokens.shape, BF), shape(w_key.shape, BF), shape(w_value.shape, BF)),
-        (v, v, v),
-        [m, m, m, m],
-        [room(tokens), room(gain), dma((14,))],
+        (shape(tokens.shape, BF), shape(w_key.shape, BF)),
+        (v, v),
+        [m, m, m],
+        [room(tokens), room(gain), dma((6,))],
         flops=1_000_000_000,
-    )(tokens, gain, w_key, w_value)
+    )(tokens, gain, w_key)
     key, value, logs, pieces, rows = call(
         summary_kernel,
         (key_shape, value_shape, logs_shape, shape((HEADS * DQK, WIDTH), BF), rows_shape),
         (m, m, m, n, m),
-        [v, n, n, n, n, v, v, n, n, n, n],
-        [room(rows_shape), room(pre_shape), room(key_shape), room(value_shape), room(logs_shape), pltpu.VMEM((128, width), BF), dma((4,))],
+        [v, n, n, n, n, v, m, n, n, n, n],
+        [room(rows_shape), room(pre_shape), room(key_shape), room(value_shape), room(logs_shape), pltpu.VMEM((128, width), BF), room(w_value), dma((4,)), dma((8,))],
         flops=3_000_000_000,
-        limit=12,
-    )(own, other, to_first, to_second, gain, wk, wv, w_igate.T, w_fgate.T, conv_key, gate_offset.transpose(1, 0, 2))
+        limit=16,
+    )(own, other, to_first, to_second, gain, wk, w_value, w_igate.T, w_fgate.T, conv_key, gate_offset.transpose(1, 0, 2))
     pieces = lax.all_to_all(pieces.reshape(stretches, 8, WIDTH), SP_TP, 0, 0, axis_index_groups=groups, tiled=True)
     query, numer, stats, ogate = call(
         local_kernel,

time: 62.7 us -> 66 us (1.053)
  Pallas kernels: 23.7 us -> 25.6 us
  starting transfers between devices: 23.1 us -> 24.6 us
    pallas_call x6, Pallas kernels: 23.7 us -> 25.6 us  [call(): return lambda *args: run(*map(kept, args, spaces))]
    all_to_all x1, starting transfers between devices: 13.4 us -> 14.8 us  [body(): lax.all_to_all(pieces.reshape(stretches, 8, WIDTH), SP_TP, 0, 0, axis_ind...]
  transfers between devices with their start and end apart: 5 -> 5, of which waited for: 1 -> 1; matrix products, arithmetic and copies ran while one was open for 1% -> 1% of each run, Pallas kernels for 21% -> 18%
where the time goes in v2:
time: 66 us; the launch traced here: 65.7 us
  Pallas kernels  25.6 us (39%)
  starting transfers between devices  24.6 us (37%)
  blocking collectives  13.1 us (20%)
  other arithmetic  1.07 us (2%)
  local copies, waits for them, and re-layouts  0.88 us (1%)
    pallas_call x6, Pallas kernels, call(): return lambda *args: run(*map(kept, args, spaces))  25.6 us
    all_to_all x1, starting transfers between devices, body(): lax.all_to_all(pieces.reshape(stretches, 8, WIDTH), SP_TP, 0, 0, axis_ind...  14.8 us
    all_to_all x1, blocking collectives, body(): lax.all_to_all(state.reshape(stretches, 8, WIDTH), SP_TP, 0, 0, axis_inde...  13.1 us
    ppermute x1, starting transfers between devices, body(): got = lax.ppermute(sent, 'tp', [(0, 1), (1, 0)])  3.76 us
    ppermute x1, starting transfers between devices, body(): lax.ppermute(last, SP_TP, [(2 * i + 1, 2 * i + 3) for i in range(stretche...  3.23 us
    ppermute x1, starting transfers between devices, body(): other = lax.ppermute(tokens, 'tp', [(0, 1), (1, 0)])  1.45 us
  transfers between devices with their start and end apart: 5, of which 1 were waited for; matrix products, arithmetic and copies ran while one was open for 1% of the time, Pallas kernels for 18%

profile of v2, /device:TPU:1, one launch (start us, length us, event | category | flops | bytes accessed | tf_op | source)
XLA Modules:
  0.0 65.7 jit_solution(4375326784058966021)
XLA Ops:
  0.0 0.0 copy-start.3
  0.0 0.0 copy-start.7
  0.0 0.0 copy-start.4
  0.0 0.0 copy-start.2
  0.0 0.0 copy-start.1
  0.0 1.4 %collective-permute-start = (bf16[192,2048]{1,0:T(8,128)(2,1)}, bf16[192,2048]{1,0:T(8,128)(2,1)S(1)}, u32[]{:S(2)}, u32[]{:S(2)}) collective-permute-start(bf16[192,2048]{1,0:T(8,128)(2,1)} %own_hbm.1), channel_id=1, source_target_pairs={{0,1},{1,0},{2,3},{3,2},{4,5},{5,4},{6,7},{7,6},{8,9},{9,8},{10,11... | collective-permute-start | bytes 2359304 | tf_op jit(solution)/shard_map/ppermute | solution.py:379
  1.5 0.8 %slice.3 = bf16[16,2048]{1,0:T(8,128)(2,1)S(1)} slice(bf16[192,2048]{1,0:T(8,128)(2,1)} %own_hbm.1), slice={[176:192], [0:2048]} | slice | bytes 131072 | tf_op jit(solution)/shard_map/slice | solution.py:380
  2.3 3.2 %collective-permute-start.2 = (bf16[16,2048]{1,0:T(8,128)(2,1)S(1)}, bf16[16,2048]{1,0:T(8,128)(2,1)S(1)}, u32[]{:S(2)}, u32[]{:S(2)}) collective-permute-start(bf16[16,2048]{1,0:T(8,128)(2,1)S(1)} %slice.3), channel_id=1, source_target_pairs={{1,3},{3,5},{5,7},{7,9},{9,11},{11,13},{13,15},{15,17},{17,19},{19... | collective-permute-start | bytes 196616 | tf_op jit(solution)/shard_map/ppermute | solution.py:381
  5.6 1.3 %collective-permute-start.1 = (bf16[16,2048]{1,0:T(8,128)(2,1)S(1)}, bf16[16,2048]{1,0:T(8,128)(2,1)S(1)}, u32[]{:S(2)}, u32[]{:S(2)}) collective-permute-start(bf16[16,2048]{1,0:T(8,128)(2,1)S(1)} %slice.3), channel_id=1, source_target_pairs={{1,2},{3,4},{5,6},{7,8},{9,10},{11,12},{13,14},{15,16},{17,18},{19... | collective-permute-start | bytes 196616 | tf_op jit(solution)/shard_map/ppermute | solution.py:382
  6.9 1.8 %shard_map.136 = (bf16[192,2048]{1,0:T(8,128)(2,1)S(1)}, bf16[2048,512]{1,0:T(8,128)(2,1)S(1)}) custom-call(bf16[192,2048]{1,0:T(8,128)(2,1)} %own_hbm.1, f32[1,2048]{1,0:T(1,128)} %bitcast.15, bf16[2048,512]{1,0:T(8,128)(2,1)} %wk_hbm.1), custom_call_target="tpu_custom_call" | custom-call | flops 1000000000 | bytes 1048576 | tf_op jit(solution)/shard_map/pallas_call | solution.py:51
  8.7 0.0 collective-permute-done.2.two_ref
  8.7 0.0 collective-permute-done.1.one_ref
  8.7 0.0 collective-permute-done.oth_ref
  8.7 0.0 copy-done.3
  8.7 0.0 copy-done.7
  8.7 0.0 copy-done.4
  8.8 0.0 copy-done.2
  8.8 0.0 copy-done.1
  8.8 0.0 copy-start.5
  8.8 0.0 copy-start.6
  8.8 9.2 %shard_map.137 = (bf16[384,512]{1,0:T(8,128)(2,1)}, bf16[384,1024]{1,0:T(8,128)(2,1)}, f32[384,128]{1,0:T(8,128)}, bf16[512,384]{1,0:T(8,128)(2,1)}, bf16[400,2048]{1,0:T(8,128)(2,1)}) custom-call(bf16[192,2048]{1,0:T(8,128)(2,1)S(1)} %get-tuple-element.25.own_ref, bf16[192,2048]{1,0:T(8,128)(2,1)S(1)} %collective-permute-done.oth_ref, ...), custom_call_target="tpu_custom_call" | custom-call | flops 3000000000 | bytes 1048576 | tf_op jit(solution)/shard_map/pallas_call | solution.py:51
  18.0 14.8 %all-to-all-start = ((bf16[64,8,384]{2,1,0:T(8,128)(2,1)}), bf16[64,8,384]{2,1,0:T(8,128)(2,1)S(1)}, u32[]{:S(2)}, u32[]{:S(2)}) async-start(bf16[64,8,384]{2,1,0:T(8,128)(2,1)} %bitcast.4), calls=%async_computation | async-start | bytes 786432 | tf_op jit(solution)/shard_map/all_to_all | solution.py:415
  32.8 0.0 copy-done.5
  32.9 0.0 copy-done.6
  32.9 0.0 copy-start
  32.9 8.0 %shard_map.138 = (bf16[384,512]{1,0:T(8,128)(2,1)S(1)}, bf16[384,1024]{1,0:T(8,128)(2,1)S(1)}, f32[384,128]{1,0:T(8,128)S(1)}, bf16[384,1024]{1,0:T(8,128)(2,1)S(1)}) custom-call(bf16[400,2048]{1,0:T(8,128)(2,1)} %get-tuple-element.28.rows_hbm, bf16[2048,512]{1,0:T(8,128)(2,1)} %wq_hbm.1, bf16[384,512]{1,0:T(8,128)(2,1)} %get-tuple-element.29.key_hbm, ...), custom_call_target="tpu_custom_call" | custom-call | flops 6000000000 | bytes 1048576 | tf_op jit(solution)/shard_map/pallas_call | solution.py:51
  40.9 0.0 all-to-all-done
  40.9 0.0 copy-done
  40.9 1.6 %shard_map.139 = (bf16[512,384]{1,0:T(8,128)(2,1)S(1)}, bf16[512,2048]{1,0:T(8,128)(2,1)S(1)}) custom-call(bf16[512,384]{1,0:T(8,128)(2,1)S(1)} %bitcast.11, s32[2,64,64]{2,1,0:T(8,128)S(1)} %copy-done, bf16[1024,2048]{1,0:T(8,128)(2,1)} %wout_hbm.3), custom_call_target="tpu_custom_call" | custom-call | flops 100000000 | bytes 1048576 | tf_op jit(solution)/shard_map/pallas_call | solution.py:51
  42.5 13.1 %all_to_all.10 = bf16[64,8,384]{2,1,0:T(8,128)(2,1)S(1)} all-to-all(bf16[64,8,384]{2,1,0:T(8,128)(2,1)S(1)} %bitcast.12), channel_id=1, replica_groups={{84,52,76,82,86,92,116,20,44,50,54,60,68,74,78,80,90,94,108,114,118,124..., dimensions={0} | all-to-all | bytes 786432 | tf_op jit(solution)/shard_map/all_to_all | solution.py:431
  55.6 3.3 %shard_map.140 = (bf16[192,2048]{1,0:T(8,128)(2,1)S(1)}, bf16[512,2048]{1,0:T(8,128)(2,1)S(1)}) custom-call(bf16[384,512]{1,0:T(8,128)(2,1)S(1)} %get-tuple-element.36.query_ref, bf16[384,1024]{1,0:T(8,128)(2,1)S(1)} %get-tuple-element.37.ogate_ref, bf16[512,384]{1,0:T(8,128)(2,1)S(1)} %bitcast.9, bf16[384,1024]{1,0:T(8,128)(2,1)S(1)} %get-tuple-element.40.numer_ref, ...), custom_call_target="tpu_custom_call" | custom-call | flops 1000000000 | bytes 1048576 | tf_op jit(solution)/shard_map/pallas_call | solution.py:51
  58.9 3.8 %collective-permute-start.3 = (bf16[192,2048]{1,0:T(8,128)(2,1)S(1)}, bf16[192,2048]{1,0:T(8,128)(2,1)S(1)}, u32[]{:S(2)}, u32[]{:S(2)}) collective-permute-start(bf16[192,2048]{1,0:T(8,128)(2,1)S(1)} %get-tuple-element.44), channel_id=1, source_target_pairs={{0,1},{1,0},{2,3},{3,2},{4,5},{5,4},{6,7},{7,6},{8,9},{9,8},{10,11... | collective-permute-start | bytes 2359304 | tf_op jit(solution)/shard_map/ppermute | solution.py:442
  62.7 1.7 %shard_map.141 = f32[192,2048]{1,0:T(8,128)S(1)} custom-call(bf16[384,512]{1,0:T(8,128)(2,1)S(1)} %get-tuple-element.36.query_ref, bf16[384,1024]{1,0:T(8,128)(2,1)S(1)} %get-tuple-element.37.ogate_ref, bf16[512,384]{1,0:T(8,128)(2,1)S(1)} %bitcast.10, bf16[384,1024]{1,0:T(8,128)(2,1)S(1)} %get-tuple-element.40.numer_ref, ...), custom_call_target="tpu_custom_call" | custom-call | flops 1000000000 | bytes 1048576 | tf_op jit(solution)/shard_map/pallas_call | solution.py:51
  64.4 0.2 collective-permute-done.3
  64.6 1.1 %add_convert_fusion = bf16[192,2048]{1,0:T(8,128)(2,1)} fusion(f32[192,2048]{1,0:T(8,128)S(1)} %shard_map.141, bf16[192,2048]{1,0:T(8,128)(2,1)S(1)} %collective-permute-done.3), kind=kLoop, calls=%fused_computation | loop fusion | flops 1179648 | bytes 3145728 | tf_op jit(solution)/shard_map/convert_element_type | solution.py:446
Async XLA Ops:
  0.0 8.7 %copy-start.3 = (f32[2048]{0:T(1024)S(1)}, f32[2048]{0:T(1024)}, u32[]{:S(2)}) copy-start(f32[2048]{0:T(1024)} %param.15) | copy-start | bytes 24580
  0.0 8.7 %copy-start.7 = (f32[2,3,4]{2,0,1:T(2,128)S(1)}, f32[2,3,4]{2,0,1:T(2,128)}, u32[]{:S(2)}) copy-start(f32[2,3,4]{2,0,1:T(2,128)} %param.24) | copy-start | bytes 292
  0.0 8.7 %copy-start.4 = (bf16[4,1024]{1,0:T(4,128)(2,1)S(1)}, bf16[4,1024]{1,0:T(4,128)(2,1)}, u32[]{:S(2)}) copy-start(bf16[4,1024]{1,0:T(4,128)(2,1)} %taps_ref.2) | copy-start | bytes 24580
  0.0 8.7 %copy-start.2 = (bf16[2048,8]{0,1:T(8,128)(2,1)S(1)}, bf16[2048,8]{0,1:T(8,128)(2,1)}, u32[]{:S(2)}) copy-start(bf16[2048,8]{0,1:T(8,128)(2,1)} %param.21) | copy-start | bytes 98308
  0.0 8.7 %copy-start.1 = (bf16[2048,8]{0,1:T(8,128)(2,1)S(1)}, bf16[2048,8]{0,1:T(8,128)(2,1)}, u32[]{:S(2)}) copy-start(bf16[2048,8]{0,1:T(8,128)(2,1)} %param.20) | copy-start | bytes 98308
  0.0 8.7 %collective-permute-start = (bf16[192,2048]{1,0:T(8,128)(2,1)}, bf16[192,2048]{1,0:T(8,128)(2,1)S(1)}, u32[]{:S(2)}, u32[]{:S(2)}) collective-permute-start(bf16[192,2048]{1,0:T(8,128)(2,1)} %own_hbm.1), channel_id=1, source_target_pairs={{0,1},{1,0},{2,3},{3,2},{4,5},{5,4},{6,7},{7,6},{8,9},{9,8},{10,11... | collective-permute-start | bytes 2359304 | tf_op jit(solution)/shard_map/ppermute | solution.py:379
  2.3 6.4 %collective-permute-start.2 = (bf16[16,2048]{1,0:T(8,128)(2,1)S(1)}, bf16[16,2048]{1,0:T(8,128)(2,1)S(1)}, u32[]{:S(2)}, u32[]{:S(2)}) collective-permute-start(bf16[16,2048]{1,0:T(8,128)(2,1)S(1)} %slice.3), channel_id=1, source_target_pairs={{1,3},{3,5},{5,7},{7,9},{9,11},{11,13},{13,15},{15,17},{17,19},{19... | collective-permute-start | bytes 196616 | tf_op jit(solution)/shard_map/ppermute | solution.py:381
  5.6 3.1 %collective-permute-start.1 = (bf16[16,2048]{1,0:T(8,128)(2,1)S(1)}, bf16[16,2048]{1,0:T(8,128)(2,1)S(1)}, u32[]{:S(2)}, u32[]{:S(2)}) collective-permute-start(bf16[16,2048]{1,0:T(8,128)(2,1)S(1)} %slice.3), channel_id=1, source_target_pairs={{1,2},{3,4},{5,6},{7,8},{9,10},{11,12},{13,14},{15,16},{17,18},{19... | collective-permute-start | bytes 196616 | tf_op jit(solution)/shard_map/ppermute | solution.py:382
  8.8 24.1 %copy-start.5 = (bf16[4,1024]{1,0:T(4,128)(2,1)S(1)}, bf16[4,1024]{1,0:T(4,128)(2,1)}, u32[]{:S(2)}) copy-start(bf16[4,1024]{1,0:T(4,128)(2,1)} %taps_ref.3) | copy-start | bytes 24580
  8.8 24.1 %copy-start.6 = (f32[2048]{0:T(1024)S(1)}, f32[2048]{0:T(1024)}, u32[]{:S(2)}) copy-start(f32[2048]{0:T(1024)} %param.25) | copy-start | bytes 24580
  18.0 22.9 %all-to-all-start = ((bf16[64,8,384]{2,1,0:T(8,128)(2,1)}), bf16[64,8,384]{2,1,0:T(8,128)(2,1)S(1)}, u32[]{:S(2)}, u32[]{:S(2)}) async-start(bf16[64,8,384]{2,1,0:T(8,128)(2,1)} %bitcast.4), calls=%async_computation | async-start | bytes 786432 | tf_op jit(solution)/shard_map/all_to_all | solution.py:415
  32.9 8.1 %copy-start = (s32[2,64,64]{2,1,0:T(8,128)S(1)}, s32[2,64,64]{2,1,0:T(8,128)}, u32[]{:S(2)}) copy-start(s32[2,64,64]{2,1,0:T(8,128)} %constant.2.clone.place_ref) | copy-start | bytes 98308
  58.9 5.7 %collective-permute-start.3 = (bf16[192,2048]{1,0:T(8,128)(2,1)S(1)}, bf16[192,2048]{1,0:T(8,128)(2,1)S(1)}, u32[]{:S(2)}, u32[]{:S(2)}) collective-permute-start(bf16[192,2048]{1,0:T(8,128)(2,1)S(1)} %get-tuple-element.44), channel_id=1, source_target_pairs={{0,1},{1,0},{2,3},{3,2},{4,5},{5,4},{6,7},{7,6},{8,9},{9,8},{10,11... | collective-permute-start | bytes 2359304 | tf_op jit(solution)/shard_map/ppermute | solution.py:442

commit v3 on v0

--- a/solution.py
+++ b/solution.py
@@ -27,7 +27,7 @@
 MIB = 1 << 20
 
 
-def call(kernel, outs, out_spaces, spaces, scratch=(), flops=0, limit=8):
+def call(kernel, outs, out_spaces, spaces, scratch=(), flops=0, limit=8, aliases=None):
     def spec(space):
         return pl.BlockSpec(memory_space=pltpu.VMEM if space is None else space)
 
@@ -41,6 +41,7 @@
         in_specs=[spec(space) for space in spaces],
         out_specs=tuple(map(spec, out_spaces)) if several else spec(out_spaces),
         scratch_shapes=list(scratch),
+        input_output_aliases=aliases or {},
         cost_estimate=pl.CostEstimate(flops=flops, transcendentals=0, bytes_accessed=1 << 20),
         compiler_params=pltpu.CompilerParams(vmem_limit_bytes=limit * MIB),
     )
@@ -96,9 +97,13 @@
     return (x * row_scale(x) * gain).astype(BF)
 
 
-def fetch_kernel(own_hbm, gain_hbm, wk_hbm, wv_hbm, rows_ref, wk_ref, wv_ref, own_ref, gain_ref, sems):
+def fetch_kernel(own_hbm, gain_hbm, wk_hbm, wv_hbm, wi_hbm, wf_hbm,
+                 rows_ref, wk_ref, wv_ref, wg_ref, gates_ref, own_ref, gain_ref, wi_ref, wf_ref, flat_ref, sems):
     copies = started(
-        [(own_hbm, own_ref), (gain_hbm, gain_ref)] + by_rows(wk_hbm, wk_ref, 4) + by_rows(wv_hbm, wv_ref, 8), sems
+        [(own_hbm, own_ref), (gain_hbm, gain_ref), (wi_hbm, wi_ref), (wf_hbm, wf_ref)]
+        + by_rows(wk_hbm, wk_ref, 4)
+        + by_rows(wv_hbm, wv_ref, 8),
+        sems,
     )
     copies[0].wait()
     parts = [slice(at, at + 48) for at in range(0, HALF, 48)]
@@ -107,18 +112,19 @@
     gain = gain_ref[...]
     for part, scale in zip(parts, scales):
         rows_ref[part, :] = (own_ref[part, :].astype(F32) * scale * gain).astype(BF)
-    wait_all(copies[2:])
-
-
-def summary_kernel(own_ref, oth_ref, one_ref, two_ref, gain_ref, wk_ref, wv_ref, wi_ref, wf_ref, taps_ref, offs_ref,
-                   key_out, value_out, logs_out, piece_ref, rows_out,
-                   rows_ref, pre_ref, key_ref, value_ref, logs_ref, wg_ref, sems):
-    outs = [
-        pltpu.make_async_copy(src, dst, sems.at[n])
-        for n, (src, dst) in enumerate(
-            [(logs_ref, logs_out), (key_ref, key_out), (value_ref, value_out), (rows_ref, rows_out)]
-        )
-    ]
+    wait_all(copies[2:4])
+    all_heads = wi_ref.shape[0]
+    flat_ref[...] = jnp.zeros_like(flat_ref)
+    flat_ref[0:all_heads, :] = wi_ref[...].astype(F32)
+    flat_ref[all_heads : 2 * all_heads, :] = wf_ref[...].astype(F32)
+    for at in range(0, wg_ref.shape[0], 128):
+        wg_ref[at : at + 128, :] = flat_ref[:, at : at + 128].T.astype(BF)
+    gates_ref[...] = jnp.dot(rows_ref[...], wg_ref[...], preferred_element_type=F32)
+    wait_all(copies[4:])
+
+
+def summary_kernel(own_ref, oth_ref, one_ref, two_ref, gain_ref, wk_ref, wv_ref, wg_ref, gates_ref, taps_ref, offs_ref,
+                   key_ref, value_ref, logs_ref, piece_ref, rows_ref, pre_ref, both_ref):
     tp = lax.axis_index("tp")
     gain = gain_ref[...]
     rows_ref[0:TAIL, :] = normalized(one_ref[...] + two_ref[...], gain)
@@ -127,13 +133,13 @@
     for part in range(HALF // 48):
         to = pl.multiple_of(TAIL + (1 - tp) * HALF + part * 48, 16)
         rows_ref[pl.ds(to, 48), :] = normalized(oth_ref[part * 48 : part * 48 + 48, :], gain)
-    outs[3].start()
-    all_heads = wi_ref.shape[0]
-    wg_ref[...] = jnp.zeros_like(wg_ref)
-    wg_ref[0:all_heads, :] = wi_ref[...]
-    wg_ref[all_heads : 2 * all_heads, :] = wf_ref[...]
     own = pl.ds(TAIL, ROWS)
-    gates = lax.dot_general(rows_ref[own, :], wg_ref[...], (((1,), (1,)), ((), ())), preferred_element_type=F32)
+    theirs = pl.multiple_of((1 - tp) * HALF, 8)
+    both_ref[pl.ds(pl.multiple_of(tp * HALF, 8), HALF), :] = gates_ref[...]
+    both_ref[pl.ds(theirs, HALF), :] = jnp.dot(
+        rows_ref[pl.ds(pl.multiple_of(TAIL + (1 - tp) * HALF, 16), HALF), :], wg_ref[...], preferred_element_type=F32
+    )
+    gates = both_ref[...]
     gates = jnp.where(tp == 0, gates, pltpu.roll(gates, 128 - HEADS, 1))
     pre_ref[...] = jnp.dot(rows_ref[...], wk_ref[...], preferred_element_type=F32).astype(BF).astype(F32)
 
@@ -153,7 +159,6 @@
         gate.append(g)
         inside.append(total)
         totals.append(total[SPAN - 1 : SPAN, :])
-    outs[0].start()
     write, level = [], None
     later = jnp.zeros_like(totals[0])
     for b in reversed(range(BLOCKS)):
@@ -171,9 +176,7 @@
         for b in range(BLOCKS):
             rows = slice(b * SPAN, (b + 1) * SPAN)
             key_ref[rows, lanes] = (mixed_rows(pre_ref, taps, lanes, b * SPAN, SPAN) * DQK**-0.5).astype(BF)
-    outs[1].start()
     value_ref[...] = jnp.dot(rows_ref[own, :], wv_ref[...], preferred_element_type=F32).astype(BF)
-    outs[2].start()
     ones = jnp.ones((ROWS, 128), BF)
     dims = (((0,), (0,)), ((), ()))
     for h in range(HEADS):
@@ -192,8 +195,6 @@
         out = slice(h * DQK, (h + 1) * DQK)
         piece_ref[out, :DV] = memory.astype(BF)
         piece_ref[out, DV:] = extra.astype(BF)
-    for copy in outs:
-        copy.wait()
 
 
 def prefix_kernel(piece_ref, place_ref, wout_hbm, out_ref, wout_ref, sems):
@@ -241,26 +242,18 @@
     wait_all(copies)
 
 
-def local_kernel(rows_hbm, wq_hbm, key_hbm, value_hbm, logs_hbm, wo_hbm, taps_ref, gain_ref,
-                 query_ref, numer_ref, stats_ref, ogate_ref,
-                 rows_ref, wq_ref, pre_ref, key_ref, value_ref, logs_ref, wo_ref, sems):
-    copies = started(
-        by_rows(rows_hbm, rows_ref, 5)
-        + by_rows(wq_hbm, wq_ref, 4)
-        + [(logs_hbm, logs_ref), (key_hbm, key_ref), (value_hbm, value_ref)]
-        + by_rows(wo_hbm, wo_ref, 8),
-        sems,
-    )
+def local_kernel(rows_ref, wq_hbm, key_ref, value_ref, logs_ref, wo_hbm, taps_ref, gain_ref,
+                 query_out, wide_out, stats_ref, query_ref, numer_ref, ogate_ref, wq_ref, pre_ref, wo_ref, sems):
+    copies = started(by_rows(wq_hbm, wq_ref, 4) + by_rows(wo_hbm, wo_ref, 8), sems)
     tp = lax.axis_index("tp")
     taps = taps_ref[:, pl.ds(pl.multiple_of(tp * (HEADS * DQK), 128), HEADS * DQK)].astype(F32)
-    wait_all(copies[:9])
+    wait_all(copies[:4])
     pre_ref[...] = jnp.dot(rows_ref[...], wq_ref[...], preferred_element_type=F32).astype(BF).astype(F32)
     for h in range(HEADS):
         lanes = slice(h * DQK, (h + 1) * DQK)
         for b in range(BLOCKS):
             rows = slice(b * SPAN, (b + 1) * SPAN)
             query_ref[rows, lanes] = mixed_rows(pre_ref, taps, lanes, b * SPAN, SPAN).astype(BF)
-    wait_all(copies[9:12])
     lane = lane_of((SPAN, 128))
     cols = [logs_ref[b * SPAN : (b + 1) * SPAN, :] for b in range(BLOCKS)]
     flat = [c.T for c in cols]
@@ -305,15 +298,18 @@
             stats[t] = jnp.where(lane == h, denom, jnp.where(lane == HEADS + h, top, stats[t]))
     for t in range(BLOCKS):
         stats_ref[t * SPAN : (t + 1) * SPAN, :] = stats[t]
-    wait_all(copies[12:])
+    wait_all(copies[4:])
     gain = gain_ref[:, pl.ds(pl.multiple_of(tp * (HEADS * DV), 128), HEADS * DV)]
     for c in range(2):
         cols = slice(c * HEADS * DV // 2, (c + 1) * HEADS * DV // 2)
         pre = jnp.dot(rows_ref[pl.ds(TAIL, ROWS), :], wo_ref[:, cols], preferred_element_type=F32).astype(BF).astype(F32)
         ogate_ref[:, cols] = (gain[:, cols] / (1.0 + jnp.exp(-pre))).astype(BF)
-
-
-def hidden_rows(first, query_ref, ogate_ref, state_ref, numer_ref, stats_ref, hidden_ref):
+    query_out[...] = query_ref[...]
+    wide_out[0:ROWS, : HEADS * DV] = numer_ref[...]
+    wide_out[0:ROWS, HEADS * DV :] = ogate_ref[...]
+
+
+def hidden_rows(first, query_ref, wide_ref, state_ref, stats_ref, hidden_ref):
     rows = pl.ds(pl.multiple_of(first, 16), HALF)
     lane = lane_of((HALF, 128))
     stats = stats_ref[rows, :]
@@ -341,25 +337,25 @@
         read = jnp.dot(
             query[:, h * DQK : (h + 1) * DQK], state_ref[h * DQK : (h + 1) * DQK, :DV], preferred_element_type=F32
         )
-        cell = one[:, h : h + 1] * read + two[:, h : h + 1] * numer_ref[rows, wide].astype(F32)
+        cell = one[:, h : h + 1] * read + two[:, h : h + 1] * wide_ref[rows, wide].astype(F32)
         scale = lax.rsqrt(jnp.mean(cell * cell, axis=-1, keepdims=True) + EPS)
-        hidden_ref[:, wide] = (cell * scale * ogate_ref[rows, wide].astype(F32)).astype(BF)
-
-
-def sent_kernel(query_ref, ogate_ref, state_ref, numer_ref, stats_ref, upper_ref, wout_hbm, out_ref, lower_ref, hidden_ref, sems):
+        hidden_ref[:, wide] = (cell * scale * wide_ref[rows, HEADS * DV + h * DV : HEADS * DV + (h + 1) * DV].astype(F32)).astype(BF)
+
+
+def sent_kernel(query_ref, wide_ref, state_ref, stats_ref, upper_ref, wout_hbm, out_ref, lower_ref, hidden_ref, sems):
     deep = upper_ref.shape[0]
     copies = started(by_rows(wout_hbm.at[pl.ds(deep, deep)], lower_ref, 4), sems)
     first = (1 - lax.axis_index("tp")) * HALF
-    hidden_rows(first, query_ref, ogate_ref, state_ref, numer_ref, stats_ref, hidden_ref)
+    hidden_rows(first, query_ref, wide_ref, state_ref, stats_ref, hidden_ref)
     part = jnp.dot(hidden_ref[:, :deep], upper_ref[...], preferred_element_type=F32)
     wait_all(copies)
     out_ref[...] = (part + jnp.dot(hidden_ref[:, deep:], lower_ref[...], preferred_element_type=F32)).astype(BF)
 
 
-def kept_kernel(query_ref, ogate_ref, state_ref, numer_ref, stats_ref, upper_ref, lower_ref, out_ref, hidden_ref):
+def kept_kernel(query_ref, wide_ref, state_ref, stats_ref, upper_ref, lower_ref, out_ref, hidden_ref):
     deep = upper_ref.shape[0]
     first = lax.axis_index("tp") * HALF
-    hidden_rows(first, query_ref, ogate_ref, state_ref, numer_ref, stats_ref, hidden_ref)
+    hidden_rows(first, query_ref, wide_ref, state_ref, stats_ref, hidden_ref)
     part = jnp.dot(hidden_ref[:, :deep], upper_ref[...], preferred_element_type=F32)
     out_ref[...] = part + jnp.dot(hidden_ref[:, deep:], lower_ref[...], preferred_element_type=F32)
 
@@ -395,34 +391,35 @@
     def room(like):
         return pltpu.VMEM(like.shape, like.dtype)
 
-    own, wk, wv = call(
+    gates_shape = shape((width, 128), BF), shape((HALF, 128), F32)
+    own, wk, wv, wg, gates = call(
         fetch_kernel,
-        (shape(tokens.shape, BF), shape(w_key.shape, BF), shape(w_value.shape, BF)),
-        (v, v, v),
-        [m, m, m, m],
-        [room(tokens), room(gain), dma((14,))],
+        (shape(tokens.shape, BF), shape(w_key.shape, BF), shape(w_value.shape, BF), *gates_shape),
+        (v, v, v, v, v),
+        [m, m, m, m, m, m],
+        [room(tokens), room(gain), *[pltpu.VMEM((w_igate.shape[1], width), BF)] * 2, pltpu.VMEM((128, width), F32), dma((16,))],
         flops=1_000_000_000,
-    )(tokens, gain, w_key, w_value)
+    )(tokens, gain, w_key, w_value, w_igate.T, w_fgate.T)
     key, value, logs, pieces, rows = call(
         summary_kernel,
         (key_shape, value_shape, logs_shape, shape((HEADS * DQK, WIDTH), BF), rows_shape),
-        (m, m, m, n, m),
-        [v, n, n, n, n, v, v, n, n, n, n],
-        [room(rows_shape), room(pre_shape), room(key_shape), room(value_shape), room(logs_shape), pltpu.VMEM((128, width), BF), dma((4,))],
+        (v, v, v, n, v),
+        [v, n, n, n, n, v, v, v, v, n, n],
+        [room(pre_shape), room(logs_shape)],
         flops=3_000_000_000,
-        limit=12,
-    )(own, other, to_first, to_second, gain, wk, wv, w_igate.T, w_fgate.T, conv_key, gate_offset.transpose(1, 0, 2))
+    )(own, other, to_first, to_second, gain, wk, wv, wg, gates, conv_key, gate_offset.transpose(1, 0, 2))
     pieces = lax.all_to_all(pieces.reshape(stretches, 8, WIDTH), SP_TP, 0, 0, axis_index_groups=groups, tiled=True)
-    query, numer, stats, ogate = call(
+    query, wide, stats = call(
         local_kernel,
-        (key_shape, value_shape, logs_shape, value_shape),
-        (v, v, v, v),
-        [m, m, m, m, m, m, n, n],
-        [room(rows_shape), room(w_query), room(pre_shape), room(key_shape), room(value_shape), room(logs_shape), room(w_ogate), dma((20,))],
+        (key_shape, rows_shape, logs_shape),
+        (v, v, v),
+        [v, m, v, v, v, m, n, n],
+        [room(key_shape), room(value_shape), room(value_shape), room(w_query), room(pre_shape), room(w_ogate), dma((12,))],
         flops=6_000_000_000,
         limit=16,
+        aliases={2: 0, 0: 1, 4: 2},
     )(rows, w_query, key, value, logs, w_ogate, conv_query, head_gain)
-    pieces, query, numer, stats, ogate = lax.optimization_barrier((pieces, query, numer, stats, ogate))
+    pieces, query, wide, stats = lax.optimization_barrier((pieces, query, wide, stats))
     piece_shape = shape((stretches * 8, WIDTH), BF)
     half_shape = shape((w_out.shape[0] // 2, width), BF)
     state, upper = call(
@@ -435,13 +432,13 @@
         sent_kernel,
         (shape((HALF, width), BF), half_shape),
         (n, v),
-        [v, v, n, v, v, v, m],
+        [v, v, n, v, v, m],
         [hidden, dma((4,))],
         flops=1_000_000_000,
-    )(query, ogate, state, numer, stats, upper, w_out)
+    )(query, wide, state, stats, upper, w_out)
     got = lax.ppermute(sent, "tp", [(0, 1), (1, 0)])
-    kept = call(kept_kernel, shape((HALF, width), F32), n, [v, v, n, v, v, v, v], [hidden], flops=1_000_000_000)(
-        query, ogate, state, numer, stats, upper, lower
+    kept = call(kept_kernel, shape((HALF, width), F32), n, [v, v, n, v, v, v], [hidden], flops=1_000_000_000)(
+        query, wide, state, stats, upper, lower
     )
     return (kept + got.astype(F32)).astype(BF)
 

time: 62.7 us -> 60.1 us (0.959)
  Pallas kernels: 23.7 us -> 21.2 us
    pallas_call x6, Pallas kernels: 23.7 us -> 21.2 us  [call(): return lambda *args: run(*map(kept, args, spaces))]
  transfers between devices with their start and end apart: 5 -> 5, of which waited for: 1 -> 1; matrix products, arithmetic and copies ran while one was open for 1% -> 1% of each run, Pallas kernels for 21% -> 20%
where the time goes in v3:
time: 60.1 us; the launch traced here: 59.8 us
  starting transfers between devices  23.1 us (38%)
  Pallas kernels  21.2 us (35%)
  blocking collectives  13.1 us (22%)
  other arithmetic  1.07 us (2%)
  local copies, waits for them, and re-layouts  0.88 us (1%)
    pallas_call x6, Pallas kernels, call(): return lambda *args: run(*map(kept, args, spaces))  21.2 us
    all_to_all x1, starting transfers between devices, body(): lax.all_to_all(pieces.reshape(stretches, 8, WIDTH), SP_TP, 0, 0, axis_ind...  13.4 us
    all_to_all x1, blocking collectives, body(): lax.all_to_all(state.reshape(stretches, 8, WIDTH), SP_TP, 0, 0, axis_inde...  13.1 us
    ppermute x1, starting transfers between devices, body(): got = lax.ppermute(sent, 'tp', [(0, 1), (1, 0)])  3.75 us
    ppermute x1, starting transfers between devices, body(): lax.ppermute(last, SP_TP, [(2 * i + 1, 2 * i + 3) for i in range(stretche...  3.22 us
    ppermute x1, starting transfers between devices, body(): other = lax.ppermute(tokens, 'tp', [(0, 1), (1, 0)])  1.38 us
    ppermute x1, starting transfers between devices, body(): lax.ppermute(last, SP_TP, [(2 * i + 1, 2 * i + 2) for i in range(stretche...  1.29 us
  transfers between devices with their start and end apart: 5, of which 1 were waited for; matrix products, arithmetic and copies ran while one was open for 1% of the time, Pallas kernels for 20%

profile of v3, /device:TPU:1, one launch (start us, length us, event | category | flops | bytes accessed | tf_op | source)
XLA Modules:
  0.0 59.8 jit_solution(17688617791845033707)
XLA Ops:
  0.0 1.4 %collective-permute-start = (bf16[192,2048]{1,0:T(8,128)(2,1)}, bf16[192,2048]{1,0:T(8,128)(2,1)S(1)}, u32[]{:S(2)}, u32[]{:S(2)}) collective-permute-start(bf16[192,2048]{1,0:T(8,128)(2,1)} %own_hbm.1), channel_id=1, source_target_pairs={{0,1},{1,0},{2,3},{3,2},{4,5},{5,4},{6,7},{7,6},{8,9},{9,8},{10,11... | collective-permute-start | bytes 2359304 | tf_op jit(solution)/shard_map/ppermute | solution.py:375
  1.4 0.8 %slice.3 = bf16[16,2048]{1,0:T(8,128)(2,1)S(1)} slice(bf16[192,2048]{1,0:T(8,128)(2,1)} %own_hbm.1), slice={[176:192], [0:2048]} | slice | bytes 131072 | tf_op jit(solution)/shard_map/slice | solution.py:376
  2.2 3.2 %collective-permute-start.2 = (bf16[16,2048]{1,0:T(8,128)(2,1)S(1)}, bf16[16,2048]{1,0:T(8,128)(2,1)S(1)}, u32[]{:S(2)}, u32[]{:S(2)}) collective-permute-start(bf16[16,2048]{1,0:T(8,128)(2,1)S(1)} %slice.3), channel_id=1, source_target_pairs={{1,3},{3,5},{5,7},{7,9},{9,11},{11,13},{13,15},{15,17},{17,19},{19... | collective-permute-start | bytes 196616 | tf_op jit(solution)/shard_map/ppermute | solution.py:377
  5.5 1.3 %collective-permute-start.1 = (bf16[16,2048]{1,0:T(8,128)(2,1)S(1)}, bf16[16,2048]{1,0:T(8,128)(2,1)S(1)}, u32[]{:S(2)}, u32[]{:S(2)}) collective-permute-start(bf16[16,2048]{1,0:T(8,128)(2,1)S(1)} %slice.3), channel_id=1, source_target_pairs={{1,2},{3,4},{5,6},{7,8},{9,10},{11,12},{13,14},{15,16},{17,18},{19... | collective-permute-start | bytes 196616 | tf_op jit(solution)/shard_map/ppermute | solution.py:378
  6.8 0.0 copy-start.1
  6.8 0.0 copy-start.2
  6.8 0.0 copy-start.5
  6.8 3.2 %shard_map.136 = (bf16[192,2048]{1,0:T(8,128)(2,1)S(1)}, bf16[2048,512]{1,0:T(8,128)(2,1)S(1)}, bf16[2048,1024]{1,0:T(8,128)(2,1)S(1)}, bf16[2048,128]{1,0:T(8,128)(2,1)S(1)}, f32[192,128]{1,0:T(8,128)S(1)}) custom-call(bf16[192,2048]{1,0:T(8,128)(2,1)} %own_hbm.1, f32[1,2048]{1,0:T(1,128)} %bitcast.13, bf16[2048,512]{1,0:T(8,128)(2,1)} %wk_hbm.1, ...), custom_call_target="tpu_custom_call" | custom-call | flops 1000000000 | bytes 1048576 | tf_op jit(solution)/shard_map/pallas_call | solution.py:52
  10.0 0.0 collective-permute-done.2.two_ref
  10.0 0.0 collective-permute-done.1.one_ref
  10.0 0.0 collective-permute-done.oth_ref
  10.0 0.0 copy-done.1
  10.0 0.0 copy-done.2
  10.0 0.0 copy-done.5
  10.1 0.0 copy-start.3
  10.1 0.0 copy-start.4
  10.1 5.0 %shard_map.137 = (bf16[384,512]{1,0:T(8,128)(2,1)S(1)}, bf16[384,1024]{1,0:T(8,128)(2,1)S(1)}, f32[384,128]{1,0:T(8,128)S(1)}, bf16[512,384]{1,0:T(8,128)(2,1)}, bf16[400,2048]{1,0:T(8,128)(2,1)S(1)}) custom-call(bf16[192,2048]{1,0:T(8,128)(2,1)S(1)} %get-tuple-element.26.own_ref, bf16[192,2048]{1,0:T(8,128)(2,1)S(1)} %collective-permute-done.oth_ref, ...), custom_call_target="tpu_custom_call" | custom-call | flops 3000000000 | bytes 1048576 | tf_op jit(solution)/shard_map/pallas_call | solution.py:52
  15.1 13.4 %all-to-all-start = ((bf16[64,8,384]{2,1,0:T(8,128)(2,1)}), bf16[64,8,384]{2,1,0:T(8,128)(2,1)S(1)}, u32[]{:S(2)}, u32[]{:S(2)}) async-start(bf16[64,8,384]{2,1,0:T(8,128)(2,1)} %bitcast.4), calls=%async_computation | async-start | bytes 786432 | tf_op jit(solution)/shard_map/all_to_all | solution.py:411
  28.5 0.0 copy-done.3
  28.5 0.0 copy-done.4
  28.5 0.0 copy-start
  28.6 7.0 %shard_map.138 = (bf16[384,512]{1,0:T(8,128)(2,1)S(1)}, bf16[400,2048]{1,0:T(8,128)(2,1)S(1)}, f32[384,128]{1,0:T(8,128)S(1)}) custom-call(bf16[400,2048]{1,0:T(8,128)(2,1)S(1)} %get-tuple-element.32.rows_ref, bf16[2048,512]{1,0:T(8,128)(2,1)} %wq_hbm.1, ...), custom_call_target="tpu_custom_call", output_to_operand_aliasing={{0}: (2, {}), {1}: (0, {}), {2}: (4, {})} | custom-call | flops 6000000000 | bytes 1048576 | tf_op jit(solution)/shard_map/pallas_call | solution.py:52
  35.6 0.0 all-to-all-done
  35.6 0.0 copy-done
  35.6 1.6 %shard_map.139 = (bf16[512,384]{1,0:T(8,128)(2,1)S(1)}, bf16[512,2048]{1,0:T(8,128)(2,1)S(1)}) custom-call(bf16[512,384]{1,0:T(8,128)(2,1)S(1)} %bitcast.11, s32[2,64,64]{2,1,0:T(8,128)S(1)} %copy-done, bf16[1024,2048]{1,0:T(8,128)(2,1)} %wout_hbm.3), custom_call_target="tpu_custom_call" | custom-call | flops 100000000 | bytes 1048576 | tf_op jit(solution)/shard_map/pallas_call | solution.py:52
  37.2 13.1 %all_to_all.10 = bf16[64,8,384]{2,1,0:T(8,128)(2,1)S(1)} all-to-all(bf16[64,8,384]{2,1,0:T(8,128)(2,1)S(1)} %bitcast.12), channel_id=1, replica_groups={{84,52,76,82,86,92,116,20,44,50,54,60,68,74,78,80,90,94,108,114,118,124..., dimensions={0} | all-to-all | bytes 786432 | tf_op jit(solution)/shard_map/all_to_all | solution.py:428
  50.3 2.7 %shard_map.140 = (bf16[192,2048]{1,0:T(8,128)(2,1)S(1)}, bf16[512,2048]{1,0:T(8,128)(2,1)S(1)}) custom-call(bf16[384,512]{1,0:T(8,128)(2,1)S(1)} %get-tuple-element.39.query_ref, bf16[400,2048]{1,0:T(8,128)(2,1)S(1)} %get-tuple-element.40.wide_ref, bf16[512,384]{1,0:T(8,128)(2,1)S(1)} %bitcast.9, f32[384,128]{1,0:T(8,128)S(1)} %get-tuple-element.43.stats_ref, ...), custom_call_target="tpu_custom_call" | custom-call | flops 1000000000 | bytes 1048576 | tf_op jit(solution)/shard_map/pallas_call | solution.py:52
  53.1 3.8 %collective-permute-start.3 = (bf16[192,2048]{1,0:T(8,128)(2,1)S(1)}, bf16[192,2048]{1,0:T(8,128)(2,1)S(1)}, u32[]{:S(2)}, u32[]{:S(2)}) collective-permute-start(bf16[192,2048]{1,0:T(8,128)(2,1)S(1)} %get-tuple-element.46), channel_id=1, source_target_pairs={{0,1},{1,0},{2,3},{3,2},{4,5},{5,4},{6,7},{7,6},{8,9},{9,8},{10,11... | collective-permute-start | bytes 2359304 | tf_op jit(solution)/shard_map/ppermute | solution.py:439
  56.8 1.7 %shard_map.141 = f32[192,2048]{1,0:T(8,128)S(1)} custom-call(bf16[384,512]{1,0:T(8,128)(2,1)S(1)} %get-tuple-element.39.query_ref, bf16[400,2048]{1,0:T(8,128)(2,1)S(1)} %get-tuple-element.40.wide_ref, bf16[512,384]{1,0:T(8,128)(2,1)S(1)} %bitcast.10, f32[384,128]{1,0:T(8,128)S(1)} %get-tuple-element.43.stats_ref, ...), custom_call_target="tpu_custom_call" | custom-call | flops 1000000000 | bytes 1048576 | tf_op jit(solution)/shard_map/pallas_call | solution.py:52
  58.5 0.2 collective-permute-done.3
  58.7 1.1 %add_convert_fusion = bf16[192,2048]{1,0:T(8,128)(2,1)} fusion(f32[192,2048]{1,0:T(8,128)S(1)} %shard_map.141, bf16[192,2048]{1,0:T(8,128)(2,1)S(1)} %collective-permute-done.3), kind=kLoop, calls=%fused_computation | loop fusion | flops 1179648 | bytes 3145728 | tf_op jit(solution)/shard_map/convert_element_type | solution.py:443
Async XLA Ops:
  0.0 10.0 %collective-permute-start = (bf16[192,2048]{1,0:T(8,128)(2,1)}, bf16[192,2048]{1,0:T(8,128)(2,1)S(1)}, u32[]{:S(2)}, u32[]{:S(2)}) collective-permute-start(bf16[192,2048]{1,0:T(8,128)(2,1)} %own_hbm.1), channel_id=1, source_target_pairs={{0,1},{1,0},{2,3},{3,2},{4,5},{5,4},{6,7},{7,6},{8,9},{9,8},{10,11... | collective-permute-start | bytes 2359304 | tf_op jit(solution)/shard_map/ppermute | solution.py:375
  2.2 7.8 %collective-permute-start.2 = (bf16[16,2048]{1,0:T(8,128)(2,1)S(1)}, bf16[16,2048]{1,0:T(8,128)(2,1)S(1)}, u32[]{:S(2)}, u32[]{:S(2)}) collective-permute-start(bf16[16,2048]{1,0:T(8,128)(2,1)S(1)} %slice.3), channel_id=1, source_target_pairs={{1,3},{3,5},{5,7},{7,9},{9,11},{11,13},{13,15},{15,17},{17,19},{19... | collective-permute-start | bytes 196616 | tf_op jit(solution)/shard_map/ppermute | solution.py:377
  5.5 4.6 %collective-permute-start.1 = (bf16[16,2048]{1,0:T(8,128)(2,1)S(1)}, bf16[16,2048]{1,0:T(8,128)(2,1)S(1)}, u32[]{:S(2)}, u32[]{:S(2)}) collective-permute-start(bf16[16,2048]{1,0:T(8,128)(2,1)S(1)} %slice.3), channel_id=1, source_target_pairs={{1,2},{3,4},{5,6},{7,8},{9,10},{11,12},{13,14},{15,16},{17,18},{19... | collective-permute-start | bytes 196616 | tf_op jit(solution)/shard_map/ppermute | solution.py:378
  6.8 3.3 %copy-start.1 = (f32[2048]{0:T(1024)S(1)}, f32[2048]{0:T(1024)}, u32[]{:S(2)}) copy-start(f32[2048]{0:T(1024)} %param.15) | copy-start | bytes 24580
  6.8 3.3 %copy-start.2 = (bf16[4,1024]{1,0:T(4,128)(2,1)S(1)}, bf16[4,1024]{1,0:T(4,128)(2,1)}, u32[]{:S(2)}) copy-start(bf16[4,1024]{1,0:T(4,128)(2,1)} %taps_ref.2) | copy-start | bytes 24580
  6.8 3.3 %copy-start.5 = (f32[2,3,4]{2,0,1:T(2,128)S(1)}, f32[2,3,4]{2,0,1:T(2,128)}, u32[]{:S(2)}) copy-start(f32[2,3,4]{2,0,1:T(2,128)} %param.24) | copy-start | bytes 292
  10.1 18.5 %copy-start.3 = (bf16[4,1024]{1,0:T(4,128)(2,1)S(1)}, bf16[4,1024]{1,0:T(4,128)(2,1)}, u32[]{:S(2)}) copy-start(bf16[4,1024]{1,0:T(4,128)(2,1)} %taps_ref.3) | copy-start | bytes 24580
  10.1 18.5 %copy-start.4 = (f32[2048]{0:T(1024)S(1)}, f32[2048]{0:T(1024)}, u32[]{:S(2)}) copy-start(f32[2048]{0:T(1024)} %param.25) | copy-start | bytes 24580
  15.1 20.5 %all-to-all-start = ((bf16[64,8,384]{2,1,0:T(8,128)(2,1)}), bf16[64,8,384]{2,1,0:T(8,128)(2,1)S(1)}, u32[]{:S(2)}, u32[]{:S(2)}) async-start(bf16[64,8,384]{2,1,0:T(8,128)(2,1)} %bitcast.4), calls=%async_computation | async-start | bytes 786432 | tf_op jit(solution)/shard_map/all_to_all | solution.py:411
  28.5 7.1 %copy-start = (s32[2,64,64]{2,1,0:T(8,128)S(1)}, s32[2,64,64]{2,1,0:T(8,128)}, u32[]{:S(2)}) copy-start(s32[2,64,64]{2,1,0:T(8,128)} %constant.2.clone.place_ref) | copy-start | bytes 98308
  53.1 5.7 %collective-permute-start.3 = (bf16[192,2048]{1,0:T(8,128)(2,1)S(1)}, bf16[192,2048]{1,0:T(8,128)(2,1)S(1)}, u32[]{:S(2)}, u32[]{:S(2)}) collective-permute-start(bf16[192,2048]{1,0:T(8,128)(2,1)S(1)} %get-tuple-element.46), channel_id=1, source_target_pairs={{0,1},{1,0},{2,3},{3,2},{4,5},{5,4},{6,7},{7,6},{8,9},{9,8},{10,11... | collective-permute-start | bytes 2359304 | tf_op jit(solution)/shard_map/ppermute | solution.py:439

commit v4 on v3

--- a/solution.py
+++ b/solution.py
@@ -197,8 +197,7 @@
         piece_ref[out, DV:] = extra.astype(BF)
 
 
-def prefix_kernel(piece_ref, place_ref, wout_hbm, out_ref, wout_ref, sems):
-    copies = started(by_rows(wout_hbm.at[pl.ds(0, wout_ref.shape[0])], wout_ref, 4), sems)
+def prefix_kernel(piece_ref, place_ref, out_ref):
     count = piece_ref.shape[0] // 8
     tall = piece_ref.shape[0]
 
@@ -239,15 +238,14 @@
     lane = lane_of((tall, 128))
     out_ref[:, :DV] = state[:, :DV].astype(BF)
     out_ref[:, DV:] = jnp.where((lane >= 1) & (lane < 4), marks, state[:, DV:]).astype(BF)
-    wait_all(copies)
-
-
-def local_kernel(rows_ref, wq_hbm, key_ref, value_ref, logs_ref, wo_hbm, taps_ref, gain_ref,
-                 query_out, wide_out, stats_ref, query_ref, numer_ref, ogate_ref, wq_ref, pre_ref, wo_ref, sems):
-    copies = started(by_rows(wq_hbm, wq_ref, 4) + by_rows(wo_hbm, wo_ref, 8), sems)
+
+
+def local_kernel(rows_ref, wq_hbm, key_ref, value_ref, logs_ref, taps_ref,
+                 query_out, numer_out, stats_ref, query_ref, numer_ref, wq_ref, pre_ref, sems):
+    copies = started(by_rows(wq_hbm, wq_ref, 4), sems)
     tp = lax.axis_index("tp")
     taps = taps_ref[:, pl.ds(pl.multiple_of(tp * (HEADS * DQK), 128), HEADS * DQK)].astype(F32)
-    wait_all(copies[:4])
+    wait_all(copies)
     pre_ref[...] = jnp.dot(rows_ref[...], wq_ref[...], preferred_element_type=F32).astype(BF).astype(F32)
     for h in range(HEADS):
         lanes = slice(h * DQK, (h + 1) * DQK)
@@ -298,18 +296,28 @@
             stats[t] = jnp.where(lane == h, denom, jnp.where(lane == HEADS + h, top, stats[t]))
     for t in range(BLOCKS):
         stats_ref[t * SPAN : (t + 1) * SPAN, :] = stats[t]
-    wait_all(copies[4:])
+    query_out[...] = query_ref[...]
+    numer_out[...] = numer_ref[...]
+
+
+def gate_kernel(rows_ref, wo_hbm, gain_ref, wide_out, wo_ref, ogate_ref, sems):
+    wide = HEADS * DV // 2
+    pairs = []
+    for c in range(2):
+        cols = pl.ds(c * wide, wide)
+        pairs += by_rows(wo_hbm.at[:, cols], wo_ref.at[:, cols], 4)
+    copies = started(pairs, sems)
+    tp = lax.axis_index("tp")
     gain = gain_ref[:, pl.ds(pl.multiple_of(tp * (HEADS * DV), 128), HEADS * DV)]
     for c in range(2):
-        cols = slice(c * HEADS * DV // 2, (c + 1) * HEADS * DV // 2)
+        wait_all(copies[4 * c : 4 * c + 4])
+        cols = slice(c * wide, (c + 1) * wide)
         pre = jnp.dot(rows_ref[pl.ds(TAIL, ROWS), :], wo_ref[:, cols], preferred_element_type=F32).astype(BF).astype(F32)
         ogate_ref[:, cols] = (gain[:, cols] / (1.0 + jnp.exp(-pre))).astype(BF)
-    query_out[...] = query_ref[...]
-    wide_out[0:ROWS, : HEADS * DV] = numer_ref[...]
-    wide_out[0:ROWS, HEADS * DV :] = ogate_ref[...]
-
-
-def hidden_rows(first, query_ref, wide_ref, state_ref, stats_ref, hidden_ref):
+    wide_out[0:ROWS, : HEADS * DV] = ogate_ref[...]
+
+
+def hidden_rows(first, query_ref, wide_ref, state_ref, numer_ref, stats_ref, hidden_ref):
     rows = pl.ds(pl.multiple_of(first, 16), HALF)
     lane = lane_of((HALF, 128))
     stats = stats_ref[rows, :]
@@ -337,27 +345,26 @@
         read = jnp.dot(
             query[:, h * DQK : (h + 1) * DQK], state_ref[h * DQK : (h + 1) * DQK, :DV], preferred_element_type=F32
         )
-        cell = one[:, h : h + 1] * read + two[:, h : h + 1] * wide_ref[rows, wide].astype(F32)
+        cell = one[:, h : h + 1] * read + two[:, h : h + 1] * numer_ref[rows, wide].astype(F32)
         scale = lax.rsqrt(jnp.mean(cell * cell, axis=-1, keepdims=True) + EPS)
-        hidden_ref[:, wide] = (cell * scale * wide_ref[rows, HEADS * DV + h * DV : HEADS * DV + (h + 1) * DV].astype(F32)).astype(BF)
-
-
-def sent_kernel(query_ref, wide_ref, state_ref, stats_ref, upper_ref, wout_hbm, out_ref, lower_ref, hidden_ref, sems):
-    deep = upper_ref.shape[0]
-    copies = started(by_rows(wout_hbm.at[pl.ds(deep, deep)], lower_ref, 4), sems)
+        hidden_ref[:, wide] = (cell * scale * wide_ref[rows, wide].astype(F32)).astype(BF)
+
+
+def sent_kernel(query_ref, wide_ref, state_ref, numer_ref, stats_ref, wout_hbm, out_ref, wout_ref, hidden_ref, sems):
+    deep = HEADS * DV // 2
+    copies = started(by_rows(wout_hbm, wout_ref, 8), sems)
     first = (1 - lax.axis_index("tp")) * HALF
-    hidden_rows(first, query_ref, wide_ref, state_ref, stats_ref, hidden_ref)
-    part = jnp.dot(hidden_ref[:, :deep], upper_ref[...], preferred_element_type=F32)
-    wait_all(copies)
-    out_ref[...] = (part + jnp.dot(hidden_ref[:, deep:], lower_ref[...], preferred_element_type=F32)).astype(BF)
-
-
-def kept_kernel(query_ref, wide_ref, state_ref, stats_ref, upper_ref, lower_ref, out_ref, hidden_ref):
-    deep = upper_ref.shape[0]
+    hidden_rows(first, query_ref, wide_ref, state_ref, numer_ref, stats_ref, hidden_ref)
+    wait_all(copies[:4])
+    part = jnp.dot(hidden_ref[:, :deep], wout_ref[:deep, :], preferred_element_type=F32)
+    wait_all(copies[4:])
+    out_ref[...] = (part + jnp.dot(hidden_ref[:, deep:], wout_ref[deep:, :], preferred_element_type=F32)).astype(BF)
+
+
+def kept_kernel(query_ref, wide_ref, state_ref, numer_ref, stats_ref, wout_ref, out_ref, hidden_ref):
     first = lax.axis_index("tp") * HALF
-    hidden_rows(first, query_ref, wide_ref, state_ref, stats_ref, hidden_ref)
-    part = jnp.dot(hidden_ref[:, :deep], upper_ref[...], preferred_element_type=F32)
-    out_ref[...] = part + jnp.dot(hidden_ref[:, deep:], lower_ref[...], preferred_element_type=F32)
+    hidden_rows(first, query_ref, wide_ref, state_ref, numer_ref, stats_ref, hidden_ref)
+    out_ref[...] = jnp.dot(hidden_ref[...], wout_ref[...], preferred_element_type=F32)
 
 
 def far_first(stretches):
@@ -409,36 +416,44 @@
         flops=3_000_000_000,
     )(own, other, to_first, to_second, gain, wk, wv, wg, gates, conv_key, gate_offset.transpose(1, 0, 2))
     pieces = lax.all_to_all(pieces.reshape(stretches, 8, WIDTH), SP_TP, 0, 0, axis_index_groups=groups, tiled=True)
-    query, wide, stats = call(
+    query, numer, stats = call(
         local_kernel,
-        (key_shape, rows_shape, logs_shape),
+        (key_shape, value_shape, logs_shape),
         (v, v, v),
-        [v, m, v, v, v, m, n, n],
-        [room(key_shape), room(value_shape), room(value_shape), room(w_query), room(pre_shape), room(w_ogate), dma((12,))],
-        flops=6_000_000_000,
-        limit=16,
-        aliases={2: 0, 0: 1, 4: 2},
-    )(rows, w_query, key, value, logs, w_ogate, conv_query, head_gain)
-    pieces, query, wide, stats = lax.optimization_barrier((pieces, query, wide, stats))
+        [v, m, v, v, v, n],
+        [room(key_shape), room(value_shape), room(w_query), room(pre_shape), dma((4,))],
+        flops=4_000_000_000,
+        limit=10,
+        aliases={2: 0, 3: 1, 4: 2},
+    )(rows, w_query, key, value, logs, conv_query)
+    pieces, query, numer, stats = lax.optimization_barrier((pieces, query, numer, stats))
     piece_shape = shape((stretches * 8, WIDTH), BF)
-    half_shape = shape((w_out.shape[0] // 2, width), BF)
-    state, upper = call(
-        prefix_kernel, (piece_shape, half_shape), (n, v), [n, n, m], [dma((4,))], flops=100_000_000
-    )(pieces.reshape(piece_shape.shape), place, w_out)
+    state = call(prefix_kernel, piece_shape, n, [n, n], flops=100_000_000)(pieces.reshape(piece_shape.shape), place)
+    state, rows = lax.optimization_barrier((state, rows))
     state = lax.all_to_all(state.reshape(stretches, 8, WIDTH), SP_TP, 0, 0, axis_index_groups=groups, tiled=True)
     state = state.reshape(HEADS * DQK, WIDTH)
+    wide = call(
+        gate_kernel,
+        rows_shape,
+        v,
+        [v, m, n],
+        [room(w_ogate), room(value_shape), dma((8,))],
+        flops=4_000_000_000,
+        limit=10,
+        aliases={0: 0},
+    )(rows, w_ogate, head_gain)
     hidden = pltpu.VMEM((HALF, HEADS * DV), BF)
-    sent, lower = call(
+    sent, wout = call(
         sent_kernel,
-        (shape((HALF, width), BF), half_shape),
+        (shape((HALF, width), BF), shape(w_out.shape, BF)),
         (n, v),
         [v, v, n, v, v, m],
-        [hidden, dma((4,))],
+        [hidden, dma((8,))],
         flops=1_000_000_000,
-    )(query, wide, state, stats, upper, w_out)
+    )(query, wide, state, numer, stats, w_out)
     got = lax.ppermute(sent, "tp", [(0, 1), (1, 0)])
     kept = call(kept_kernel, shape((HALF, width), F32), n, [v, v, n, v, v, v], [hidden], flops=1_000_000_000)(
-        query, wide, state, stats, upper, lower
+        query, wide, state, numer, stats, wout
     )
     return (kept + got.astype(F32)).astype(BF)
 

time: 60.1 us -> 60.2 us (level)
  blocking collectives: 13.1 us -> 0 us
  starting transfers between devices: 23.1 us -> 33 us
  Pallas kernels: 21.2 us -> 23.1 us
  local copies, waits for them, and re-layouts: 0.88 us -> 2.36 us
    all_to_all x1 -> x0, blocking collectives: 13.1 us -> none  [body(): lax.all_to_all(state.reshape(stretches, 8, WIDTH), SP_TP, 0, 0, axis_inde...]
    all_to_all x0 -> x1, starting transfers between devices: none -> 9.93 us  [body(): lax.all_to_all(state.reshape(stretches, 8, WIDTH), SP_TP, 0, 0, axis_inde...]
    pallas_call x6 -> x7, Pallas kernels: 21.2 us -> 23.1 us  [call(): return lambda *args: run(*map(kept, args, spaces))]
    unnamed x12 -> x16, local copies, waits for them, and re-layouts: 0.04 us -> 1.52 us
  transfers between devices with their start and end apart: 5 -> 6, of which waited for: 1 -> 0; matrix products, arithmetic and copies ran while one was open for 1% -> 1% of each run, Pallas kernels for 20% -> 23%
where the time goes in v4:
time: 60.2 us; the launch traced here: 59.9 us
  starting transfers between devices  33 us (55%)
  Pallas kernels  23.1 us (38%)
  local copies, waits for them, and re-layouts  2.36 us (4%)
  other arithmetic  1.09 us (2%)
    pallas_call x7, Pallas kernels, call(): return lambda *args: run(*map(kept, args, spaces))  23.1 us
    all_to_all x1, starting transfers between devices, body(): lax.all_to_all(pieces.reshape(stretches, 8, WIDTH), SP_TP, 0, 0, axis_ind...  13.4 us
    all_to_all x1, starting transfers between devices, body(): lax.all_to_all(state.reshape(stretches, 8, WIDTH), SP_TP, 0, 0, axis_inde...  9.93 us
    ppermute x1, starting transfers between devices, body(): got = lax.ppermute(sent, 'tp', [(0, 1), (1, 0)])  3.8 us
    ppermute x1, starting transfers between devices, body(): lax.ppermute(last, SP_TP, [(2 * i + 1, 2 * i + 3) for i in range(stretche...  3.22 us
    unnamed x16, local copies, waits for them, and re-layouts  1.52 us
    ppermute x1, starting transfers between devices, body(): other = lax.ppermute(tokens, 'tp', [(0, 1), (1, 0)])  1.38 us
    ppermute x1, starting transfers between devices, body(): lax.ppermute(last, SP_TP, [(2 * i + 1, 2 * i + 2) for i in range(stretche...  1.29 us
  transfers between devices with their start and end apart: 6, of which 0 were waited for; matrix products, arithmetic and copies ran while one was open for 1% of the time, Pallas kernels for 23%

profile of v4, /device:TPU:1, one launch (start us, length us, event | category | flops | bytes accessed | tf_op | source)
XLA Modules:
  0.0 59.9 jit_solution(8235053939123899673)
XLA Ops:
  0.0 1.4 %collective-permute-start = (bf16[192,2048]{1,0:T(8,128)(2,1)}, bf16[192,2048]{1,0:T(8,128)(2,1)S(1)}, u32[]{:S(2)}, u32[]{:S(2)}) collective-permute-start(bf16[192,2048]{1,0:T(8,128)(2,1)} %own_hbm.1), channel_id=1, source_target_pairs={{0,1},{1,0},{2,3},{3,2},{4,5},{5,4},{6,7},{7,6},{8,9},{9,8},{10,11... | collective-permute-start | bytes 2359304 | tf_op jit(solution)/shard_map/ppermute | solution.py:382
  1.4 0.8 %slice.3 = bf16[16,2048]{1,0:T(8,128)(2,1)S(1)} slice(bf16[192,2048]{1,0:T(8,128)(2,1)} %own_hbm.1), slice={[176:192], [0:2048]} | slice | bytes 131072 | tf_op jit(solution)/shard_map/slice | solution.py:383
  2.2 3.2 %collective-permute-start.2 = (bf16[16,2048]{1,0:T(8,128)(2,1)S(1)}, bf16[16,2048]{1,0:T(8,128)(2,1)S(1)}, u32[]{:S(2)}, u32[]{:S(2)}) collective-permute-start(bf16[16,2048]{1,0:T(8,128)(2,1)S(1)} %slice.3), channel_id=1, source_target_pairs={{1,3},{3,5},{5,7},{7,9},{9,11},{11,13},{13,15},{15,17},{17,19},{19... | collective-permute-start | bytes 196616 | tf_op jit(solution)/shard_map/ppermute | solution.py:384
  5.5 1.3 %collective-permute-start.1 = (bf16[16,2048]{1,0:T(8,128)(2,1)S(1)}, bf16[16,2048]{1,0:T(8,128)(2,1)S(1)}, u32[]{:S(2)}, u32[]{:S(2)}) collective-permute-start(bf16[16,2048]{1,0:T(8,128)(2,1)S(1)} %slice.3), channel_id=1, source_target_pairs={{1,2},{3,4},{5,6},{7,8},{9,10},{11,12},{13,14},{15,16},{17,18},{19... | collective-permute-start | bytes 196616 | tf_op jit(solution)/shard_map/ppermute | solution.py:385
  6.8 0.0 copy-start.3
  6.8 0.0 copy-start.4
  6.8 0.0 copy-start.7
  6.8 3.2 %shard_map.136 = (bf16[192,2048]{1,0:T(8,128)(2,1)S(1)}, bf16[2048,512]{1,0:T(8,128)(2,1)S(1)}, bf16[2048,1024]{1,0:T(8,128)(2,1)S(1)}, bf16[2048,128]{1,0:T(8,128)(2,1)S(1)}, f32[192,128]{1,0:T(8,128)S(1)}) custom-call(bf16[192,2048]{1,0:T(8,128)(2,1)} %own_hbm.1, f32[1,2048]{1,0:T(1,128)} %bitcast.14, bf16[2048,512]{1,0:T(8,128)(2,1)} %wk_hbm.1, ...), custom_call_target="tpu_custom_call" | custom-call | flops 1000000000 | bytes 1048576 | tf_op jit(solution)/shard_map/pallas_call | solution.py:52
  10.0 0.0 collective-permute-done.2.two_ref
  10.0 0.0 collective-permute-done.1.one_ref
  10.0 0.0 collective-permute-done.oth_ref
  10.0 0.0 copy-done.3
  10.0 0.0 copy-done.4
  10.0 0.0 copy-done.7
  10.1 0.0 copy-start.5
  10.1 4.2 %shard_map.137 = (bf16[384,512]{1,0:T(8,128)(2,1)S(1)}, bf16[384,1024]{1,0:T(8,128)(2,1)S(1)}, f32[384,128]{1,0:T(8,128)S(1)}, bf16[512,384]{1,0:T(8,128)(2,1)S(1)}, bf16[400,2048]{1,0:T(8,128)(2,1)S(1)}) custom-call(bf16[192,2048]{1,0:T(8,128)(2,1)S(1)} %get-tuple-element.26.own_ref, bf16[192,2048]{1,0:T(8,128)(2,1)S(1)} %collective-permute-done.oth_ref, ...), custom_call_target="tpu_custom_call" | custom-call | flops 3000000000 | bytes 1048576 | tf_op jit(solution)/shard_map/pallas_call | solution.py:52
  14.3 0.0 copy-start.1
  14.3 0.7 %copy-done.1 = bf16[512,384]{1,0:T(8,128)(2,1)} copy-done((bf16[512,384]{1,0:T(8,128)(2,1)}, bf16[512,384]{1,0:T(8,128)(2,1)S(1)}, u32[]{:S(2)}) %copy-start.1) | copy-done | bytes 393240
  15.0 13.4 %all-to-all-start = ((bf16[64,8,384]{2,1,0:T(8,128)(2,1)}), bf16[64,8,384]{2,1,0:T(8,128)(2,1)S(1)}, u32[]{:S(2)}, u32[]{:S(2)}) async-start(bf16[64,8,384]{2,1,0:T(8,128)(2,1)} %bitcast.13), calls=%async_computation | async-start | bytes 786432 | tf_op jit(solution)/shard_map/all_to_all | solution.py:418
  28.5 0.0 copy-done.5
  28.5 0.0 copy-start.2
  28.5 0.0 copy-start.6
  28.5 4.7 %shard_map.138 = (bf16[384,512]{1,0:T(8,128)(2,1)S(1)}, bf16[384,1024]{1,0:T(8,128)(2,1)S(1)}, f32[384,128]{1,0:T(8,128)S(1)}) custom-call(bf16[400,2048]{1,0:T(8,128)(2,1)S(1)} %get-tuple-element.41.rows_ref, bf16[2048,512]{1,0:T(8,128)(2,1)} %wq_hbm.1, ...), custom_call_target="tpu_custom_call", output_to_operand_aliasing={{0}: (2, {}), {1}: (3, {}), {2}: (4, {})} | custom-call | flops 4000000000 | bytes 1048576 | tf_op jit(solution)/shard_map/pallas_call | solution.py:52
  33.2 0.0 all-to-all-done
  33.2 0.0 copy-done.2
  33.2 1.2 %shard_map.139 = bf16[512,384]{1,0:T(8,128)(2,1)S(1)} custom-call(bf16[512,384]{1,0:T(8,128)(2,1)S(1)} %bitcast.11, s32[2,64,64]{2,1,0:T(8,128)S(1)} %copy-done.2), custom_call_target="tpu_custom_call" | custom-call | flops 100000000 | bytes 1048576 | tf_op jit(solution)/shard_map/pallas_call | solution.py:52
  34.4 0.0 copy-start
  34.5 0.7 %copy-done = bf16[512,384]{1,0:T(8,128)(2,1)} copy-done((bf16[512,384]{1,0:T(8,128)(2,1)}, bf16[512,384]{1,0:T(8,128)(2,1)S(1)}, u32[]{:S(2)}) %copy-start) | copy-done | bytes 393240
  35.2 9.9 %all-to-all-start.1 = ((bf16[64,8,384]{2,1,0:T(8,128)(2,1)}), bf16[64,8,384]{2,1,0:T(8,128)(2,1)S(1)}, u32[]{:S(2)}, u32[]{:S(2)}) async-start(bf16[64,8,384]{2,1,0:T(8,128)(2,1)} %bitcast.12), calls=%async_computation.1 | async-start | bytes 786432 | tf_op jit(solution)/shard_map/all_to_all | solution.py:433
  45.1 0.0 copy-done.6
  45.1 3.8 %shard_map.140.wide_ref = bf16[400,2048]{1,0:T(8,128)(2,1)S(1)} custom-call(bf16[400,2048]{1,0:T(8,128)(2,1)S(1)} %get-tuple-element.41.rows_ref, bf16[2048,1024]{1,0:T(8,128)(2,1)} %wo_hbm.1, f32[1,2048]{1,0:T(1,128)S(1)} %bitcast.16), custom_call_target="tpu_custom_call", output_to_operand_aliasing={{}: (0, {})} | custom-call | flops 4000000000 | bytes 1048576 | tf_op jit(solution)/shard_map/pallas_call | solution.py:52
  49.0 0.0 all-to-all-done.1
  49.0 3.9 %shard_map.141 = (bf16[192,2048]{1,0:T(8,128)(2,1)S(1)}, bf16[1024,2048]{1,0:T(8,128)(2,1)S(1)}) custom-call(bf16[384,512]{1,0:T(8,128)(2,1)S(1)} %get-tuple-element.39.query_ref, bf16[400,2048]{1,0:T(8,128)(2,1)S(1)} %shard_map.140.wide_ref, bf16[512,384]{1,0:T(8,128)(2,1)S(1)} %bitcast.9, bf16[384,1024]{1,0:T(8,128)(2,1)S(1)} %get-tuple-element.43.numer_ref, ...), custom_call_target="tpu_custom_call" | custom-call | flops 1000000000 | bytes 1048576 | tf_op jit(solution)/shard_map/pallas_call | solution.py:52
  52.9 3.8 %collective-permute-start.3 = (bf16[192,2048]{1,0:T(8,128)(2,1)S(1)}, bf16[192,2048]{1,0:T(8,128)(2,1)S(1)}, u32[]{:S(2)}, u32[]{:S(2)}) collective-permute-start(bf16[192,2048]{1,0:T(8,128)(2,1)S(1)} %get-tuple-element.46), channel_id=1, source_target_pairs={{0,1},{1,0},{2,3},{3,2},{4,5},{5,4},{6,7},{7,6},{8,9},{9,8},{10,11... | collective-permute-start | bytes 2359304 | tf_op jit(solution)/shard_map/ppermute | solution.py:454
  56.7 2.0 %shard_map.142 = f32[192,2048]{1,0:T(8,128)S(1)} custom-call(bf16[384,512]{1,0:T(8,128)(2,1)S(1)} %get-tuple-element.39.query_ref, bf16[400,2048]{1,0:T(8,128)(2,1)S(1)} %shard_map.140.wide_ref, bf16[512,384]{1,0:T(8,128)(2,1)S(1)} %bitcast.10, bf16[384,1024]{1,0:T(8,128)(2,1)S(1)} %get-tuple-element.43.numer_ref, ...), custom_call_target="tpu_custom_call" | custom-call | flops 1000000000 | bytes 1048576 | tf_op jit(solution)/shard_map/pallas_call | solution.py:52
  58.8 0.0 collective-permute-done.3
  58.8 1.1 %add_convert_fusion = bf16[192,2048]{1,0:T(8,128)(2,1)} fusion(f32[192,2048]{1,0:T(8,128)S(1)} %shard_map.142, bf16[192,2048]{1,0:T(8,128)(2,1)S(1)} %collective-permute-done.3), kind=kLoop, calls=%fused_computation | loop fusion | flops 1179648 | bytes 3145728 | tf_op jit(solution)/shard_map/convert_element_type | solution.py:458
Async XLA Ops:
  0.0 10.0 %collective-permute-start = (bf16[192,2048]{1,0:T(8,128)(2,1)}, bf16[192,2048]{1,0:T(8,128)(2,1)S(1)}, u32[]{:S(2)}, u32[]{:S(2)}) collective-permute-start(bf16[192,2048]{1,0:T(8,128)(2,1)} %own_hbm.1), channel_id=1, source_target_pairs={{0,1},{1,0},{2,3},{3,2},{4,5},{5,4},{6,7},{7,6},{8,9},{9,8},{10,11... | collective-permute-start | bytes 2359304 | tf_op jit(solution)/shard_map/ppermute | solution.py:382
  2.2 7.8 %collective-permute-start.2 = (bf16[16,2048]{1,0:T(8,128)(2,1)S(1)}, bf16[16,2048]{1,0:T(8,128)(2,1)S(1)}, u32[]{:S(2)}, u32[]{:S(2)}) collective-permute-start(bf16[16,2048]{1,0:T(8,128)(2,1)S(1)} %slice.3), channel_id=1, source_target_pairs={{1,3},{3,5},{5,7},{7,9},{9,11},{11,13},{13,15},{15,17},{17,19},{19... | collective-permute-start | bytes 196616 | tf_op jit(solution)/shard_map/ppermute | solution.py:384
  5.5 4.6 %collective-permute-start.1 = (bf16[16,2048]{1,0:T(8,128)(2,1)S(1)}, bf16[16,2048]{1,0:T(8,128)(2,1)S(1)}, u32[]{:S(2)}, u32[]{:S(2)}) collective-permute-start(bf16[16,2048]{1,0:T(8,128)(2,1)S(1)} %slice.3), channel_id=1, source_target_pairs={{1,2},{3,4},{5,6},{7,8},{9,10},{11,12},{13,14},{15,16},{17,18},{19... | collective-permute-start | bytes 196616 | tf_op jit(solution)/shard_map/ppermute | solution.py:385
  6.8 3.3 %copy-start.3 = (f32[2048]{0:T(1024)S(1)}, f32[2048]{0:T(1024)}, u32[]{:S(2)}) copy-start(f32[2048]{0:T(1024)} %param.15) | copy-start | bytes 24580
  6.8 3.3 %copy-start.4 = (bf16[4,1024]{1,0:T(4,128)(2,1)S(1)}, bf16[4,1024]{1,0:T(4,128)(2,1)}, u32[]{:S(2)}) copy-start(bf16[4,1024]{1,0:T(4,128)(2,1)} %taps_ref.2) | copy-start | bytes 24580
  6.8 3.3 %copy-start.7 = (f32[2,3,4]{2,0,1:T(2,128)S(1)}, f32[2,3,4]{2,0,1:T(2,128)}, u32[]{:S(2)}) copy-start(f32[2,3,4]{2,0,1:T(2,128)} %param.24) | copy-start | bytes 292
  10.1 18.4 %copy-start.5 = (bf16[4,1024]{1,0:T(4,128)(2,1)S(1)}, bf16[4,1024]{1,0:T(4,128)(2,1)}, u32[]{:S(2)}) copy-start(bf16[4,1024]{1,0:T(4,128)(2,1)} %taps_ref.3) | copy-start | bytes 24580
  14.3 0.7 %copy-start.1 = (bf16[512,384]{1,0:T(8,128)(2,1)}, bf16[512,384]{1,0:T(8,128)(2,1)S(1)}, u32[]{:S(2)}) copy-start(bf16[512,384]{1,0:T(8,128)(2,1)S(1)} %get-tuple-element.31) | copy-start | bytes 1179652
  15.0 18.2 %all-to-all-start = ((bf16[64,8,384]{2,1,0:T(8,128)(2,1)}), bf16[64,8,384]{2,1,0:T(8,128)(2,1)S(1)}, u32[]{:S(2)}, u32[]{:S(2)}) async-start(bf16[64,8,384]{2,1,0:T(8,128)(2,1)} %bitcast.13), calls=%async_computation | async-start | bytes 786432 | tf_op jit(solution)/shard_map/all_to_all | solution.py:418
  28.5 4.7 %copy-start.2 = (s32[2,64,64]{2,1,0:T(8,128)S(1)}, s32[2,64,64]{2,1,0:T(8,128)}, u32[]{:S(2)}) copy-start(s32[2,64,64]{2,1,0:T(8,128)} %constant.2.clone.place_ref) | copy-start | bytes 98308
  28.5 16.7 %copy-start.6 = (f32[2048]{0:T(1024)S(1)}, f32[2048]{0:T(1024)}, u32[]{:S(2)}) copy-start(f32[2048]{0:T(1024)} %param.25) | copy-start | bytes 24580
  34.4 0.7 %copy-start = (bf16[512,384]{1,0:T(8,128)(2,1)}, bf16[512,384]{1,0:T(8,128)(2,1)S(1)}, u32[]{:S(2)}) copy-start(bf16[512,384]{1,0:T(8,128)(2,1)S(1)} %shard_map.139) | copy-start | bytes 1179652
  35.2 13.8 %all-to-all-start.1 = ((bf16[64,8,384]{2,1,0:T(8,128)(2,1)}), bf16[64,8,384]{2,1,0:T(8,128)(2,1)S(1)}, u32[]{:S(2)}, u32[]{:S(2)}) async-start(bf16[64,8,384]{2,1,0:T(8,128)(2,1)} %bitcast.12), calls=%async_computation.1 | async-start | bytes 786432 | tf_op jit(solution)/shard_map/all_to_all | solution.py:433
  52.9 5.8 %collective-permute-start.3 = (bf16[192,2048]{1,0:T(8,128)(2,1)S(1)}, bf16[192,2048]{1,0:T(8,128)(2,1)S(1)}, u32[]{:S(2)}, u32[]{:S(2)}) collective-permute-start(bf16[192,2048]{1,0:T(8,128)(2,1)S(1)} %get-tuple-element.46), channel_id=1, source_target_pairs={{0,1},{1,0},{2,3},{3,2},{4,5},{5,4},{6,7},{7,6},{8,9},{9,8},{10,11... | collective-permute-start | bytes 2359304 | tf_op jit(solution)/shard_map/ppermute | solution.py:454

commit v5 on v4

--- a/solution.py
+++ b/solution.py
@@ -97,12 +97,14 @@
     return (x * row_scale(x) * gain).astype(BF)
 
 
-def fetch_kernel(own_hbm, gain_hbm, wk_hbm, wv_hbm, wi_hbm, wf_hbm,
-                 rows_ref, wk_ref, wv_ref, wg_ref, gates_ref, own_ref, gain_ref, wi_ref, wf_ref, flat_ref, sems):
+def last_kernel(own_hbm, out_ref, sems):
+    wait_all(started([(own_hbm.at[pl.ds(HALF - TAIL, TAIL)], out_ref)], sems))
+
+
+def fetch_kernel(own_hbm, gain_hbm, wi_hbm, wf_hbm,
+                 rows_ref, wg_ref, gates_ref, own_ref, gain_ref, wi_ref, wf_ref, flat_ref, sems):
     copies = started(
-        [(own_hbm, own_ref), (gain_hbm, gain_ref), (wi_hbm, wi_ref), (wf_hbm, wf_ref)]
-        + by_rows(wk_hbm, wk_ref, 4)
-        + by_rows(wv_hbm, wv_ref, 8),
+        [(own_hbm, own_ref), (gain_hbm, gain_ref), (wi_hbm, wi_ref), (wf_hbm, wf_ref)],
         sems,
     )
     copies[0].wait()
@@ -120,11 +122,10 @@
     for at in range(0, wg_ref.shape[0], 128):
         wg_ref[at : at + 128, :] = flat_ref[:, at : at + 128].T.astype(BF)
     gates_ref[...] = jnp.dot(rows_ref[...], wg_ref[...], preferred_element_type=F32)
-    wait_all(copies[4:])
 
 
 def summary_kernel(own_ref, oth_ref, one_ref, two_ref, gain_ref, wk_ref, wv_ref, wg_ref, gates_ref, taps_ref, offs_ref,
-                   key_ref, value_ref, logs_ref, piece_ref, rows_ref, pre_ref, both_ref):
+                   key_ref, value_ref, logs_ref, piece_out, rows_ref, pre_ref, both_ref, piece_ref, sems):
     tp = lax.axis_index("tp")
     gain = gain_ref[...]
     rows_ref[0:TAIL, :] = normalized(one_ref[...] + two_ref[...], gain)
@@ -178,6 +179,7 @@
             key_ref[rows, lanes] = (mixed_rows(pre_ref, taps, lanes, b * SPAN, SPAN) * DQK**-0.5).astype(BF)
     value_ref[...] = jnp.dot(rows_ref[own, :], wv_ref[...], preferred_element_type=F32).astype(BF)
     ones = jnp.ones((ROWS, 128), BF)
+    copies = []
     dims = (((0,), (0,)), ((), ()))
     for h in range(HEADS):
         lanes = slice(h * DQK, (h + 1) * DQK)
@@ -195,9 +197,13 @@
         out = slice(h * DQK, (h + 1) * DQK)
         piece_ref[out, :DV] = memory.astype(BF)
         piece_ref[out, DV:] = extra.astype(BF)
-
-
-def prefix_kernel(piece_ref, place_ref, out_ref):
+        copy = pltpu.make_async_copy(piece_ref.at[pl.ds(h * DQK, DQK)], piece_out.at[pl.ds(h * DQK, DQK)], sems.at[h])
+        copy.start()
+        copies.append(copy)
+    wait_all(copies)
+
+
+def prefix_kernel(piece_ref, place_ref, out_hbm, out_ref, sems):
     count = piece_ref.shape[0] // 8
     tall = piece_ref.shape[0]
 
@@ -234,10 +240,18 @@
     for n, mark in enumerate(thirds(top)):
         marks = jnp.where(lane == n + 1, mark, marks)
     marks = jnp.dot(spread, marks.astype(BF), preferred_element_type=F32)
-    state = jnp.dot(weight, piece_ref[...], preferred_element_type=F32)
-    lane = lane_of((tall, 128))
-    out_ref[:, :DV] = state[:, :DV].astype(BF)
-    out_ref[:, DV:] = jnp.where((lane >= 1) & (lane < 4), marks, state[:, DV:]).astype(BF)
+    part = tall // 4
+    lane = lane_of((part, 128))
+    copies = []
+    for c in range(4):
+        rows = slice(c * part, (c + 1) * part)
+        state = jnp.dot(weight[rows], piece_ref[...], preferred_element_type=F32)
+        out_ref[rows, :DV] = state[:, :DV].astype(BF)
+        out_ref[rows, DV:] = jnp.where((lane >= 1) & (lane < 4), marks[rows], state[:, DV:]).astype(BF)
+        copy = pltpu.make_async_copy(out_ref.at[pl.ds(c * part, part)], out_hbm.at[pl.ds(c * part, part)], sems.at[c])
+        copy.start()
+        copies.append(copy)
+    wait_all(copies)
 
 
 def local_kernel(rows_ref, wq_hbm, key_ref, value_ref, logs_ref, taps_ref,
@@ -380,7 +394,14 @@
     stretches = lax.axis_size(SP)
     shape = jax.ShapeDtypeStruct
     other = lax.ppermute(tokens, "tp", [(0, 1), (1, 0)])
-    last = tokens[HALF - TAIL :]
+    last = call(
+        last_kernel,
+        jax.ShapeDtypeStruct((TAIL, width), BF),
+        None,
+        [pltpu.HBM],
+        [pltpu.SemaphoreType.DMA((1,))],
+        flops=100_000_000_000,
+    )(tokens)
     to_second = lax.ppermute(last, SP_TP, [(2 * i + 1, 2 * i + 3) for i in range(stretches - 1)])
     to_first = lax.ppermute(last, SP_TP, [(2 * i + 1, 2 * i + 2) for i in range(stretches - 1)])
     gain = norm_gain.reshape(1, -1)
@@ -399,22 +420,22 @@
         return pltpu.VMEM(like.shape, like.dtype)
 
     gates_shape = shape((width, 128), BF), shape((HALF, 128), F32)
-    own, wk, wv, wg, gates = call(
+    own, wg, gates = call(
         fetch_kernel,
-        (shape(tokens.shape, BF), shape(w_key.shape, BF), shape(w_value.shape, BF), *gates_shape),
-        (v, v, v, v, v),
-        [m, m, m, m, m, m],
-        [room(tokens), room(gain), *[pltpu.VMEM((w_igate.shape[1], width), BF)] * 2, pltpu.VMEM((128, width), F32), dma((16,))],
-        flops=1_000_000_000,
-    )(tokens, gain, w_key, w_value, w_igate.T, w_fgate.T)
+        (shape(tokens.shape, BF), *gates_shape),
+        (v, v, v),
+        [m, m, m, m],
+        [room(tokens), room(gain), *[pltpu.VMEM((w_igate.shape[1], width), BF)] * 2, pltpu.VMEM((128, width), F32), dma((4,))],
+        flops=1000000000,
+    )(tokens, gain, w_igate.T, w_fgate.T)
     key, value, logs, pieces, rows = call(
         summary_kernel,
         (key_shape, value_shape, logs_shape, shape((HEADS * DQK, WIDTH), BF), rows_shape),
-        (v, v, v, n, v),
-        [v, n, n, n, n, v, v, v, v, n, n],
-        [room(pre_shape), room(logs_shape)],
+        (v, v, v, m, v),
+        [v, n, n, n, n, n, n, v, v, n, n],
+        [room(pre_shape), room(logs_shape), pltpu.VMEM((HEADS * DQK, WIDTH), BF), dma((HEADS,))],
         flops=3_000_000_000,
-    )(own, other, to_first, to_second, gain, wk, wv, wg, gates, conv_key, gate_offset.transpose(1, 0, 2))
+    )(own, other, to_first, to_second, gain, w_key, w_value, wg, gates, conv_key, gate_offset.transpose(1, 0, 2))
     pieces = lax.all_to_all(pieces.reshape(stretches, 8, WIDTH), SP_TP, 0, 0, axis_index_groups=groups, tiled=True)
     query, numer, stats = call(
         local_kernel,
@@ -428,7 +449,7 @@
     )(rows, w_query, key, value, logs, conv_query)
     pieces, query, numer, stats = lax.optimization_barrier((pieces, query, numer, stats))
     piece_shape = shape((stretches * 8, WIDTH), BF)
-    state = call(prefix_kernel, piece_shape, n, [n, n], flops=100_000_000)(pieces.reshape(piece_shape.shape), place)
+    state = call(prefix_kernel, piece_shape, m, [n, n], [room(piece_shape), dma((4,))], flops=100_000_000)(pieces.reshape(piece_shape.shape), place)
     state, rows = lax.optimization_barrier((state, rows))
     state = lax.all_to_all(state.reshape(stretches, 8, WIDTH), SP_TP, 0, 0, axis_index_groups=groups, tiled=True)
     state = state.reshape(HEADS * DQK, WIDTH)

time: 60.2 us -> 60.6 us (level)
  local copies, waits for them, and re-layouts: 2.36 us -> 0.05 us
  starting transfers between devices: 33 us -> 34.5 us
  Pallas kernels: 23.1 us -> 24.4 us
    unnamed x16, local copies, waits for them, and re-layouts: 1.52 us -> 0.05 us
    pallas_call x7 -> x8, Pallas kernels: 23.1 us -> 24.4 us  [call(): return lambda *args: run(*map(kept, args, spaces))]
    all_to_all x1, starting transfers between devices: 13.4 us -> 14.6 us  [body(): lax.all_to_all(pieces.reshape(stretches, 8, WIDTH), SP_TP, 0, 0, axis_ind...]
    slice x1 -> x0, local copies, waits for them, and re-layouts: 0.84 us -> none  [body(): last = tokens[HALF - TAIL:]]
  transfers between devices with their start and end apart: 6 -> 6, of which waited for: 0 -> 0; matrix products, arithmetic and copies ran while one was open for 1% -> 0% of each run, Pallas kernels for 23% -> 23%
where the time goes in v5:
time: 60.6 us; the launch traced here: 60.3 us
  starting transfers between devices  34.5 us (57%)
  Pallas kernels  24.4 us (40%)
  other arithmetic  1.09 us (2%)
    pallas_call x8, Pallas kernels, call(): return lambda *args: run(*map(kept, args, spaces))  24.4 us
    all_to_all x1, starting transfers between devices, body(): lax.all_to_all(pieces.reshape(stretches, 8, WIDTH), SP_TP, 0, 0, axis_ind...  14.6 us
    all_to_all x1, starting transfers between devices, body(): lax.all_to_all(state.reshape(stretches, 8, WIDTH), SP_TP, 0, 0, axis_inde...  9.94 us
    ppermute x1, starting transfers between devices, body(): got = lax.ppermute(sent, 'tp', [(0, 1), (1, 0)])  3.8 us
    ppermute x1, starting transfers between devices, body(): lax.ppermute(last, SP_TP, [(2 * i + 1, 2 * i + 3) for i in range(stretche...  3.49 us
    ppermute x1, starting transfers between devices, body(): other = lax.ppermute(tokens, 'tp', [(0, 1), (1, 0)])  1.38 us
    ppermute x1, starting transfers between devices, body(): lax.ppermute(last, SP_TP, [(2 * i + 1, 2 * i + 2) for i in range(stretche...  1.29 us
  transfers between devices with their start and end apart: 6, of which 0 were waited for; matrix products, arithmetic and copies ran while one was open for 0% of the time, Pallas kernels for 23%

profile of v5, /device:TPU:1, one launch (start us, length us, event | category | flops | bytes accessed | tf_op | source)
XLA Modules:
  0.0 60.3 jit_solution(10079750178692010296)
XLA Ops:
  0.0 1.4 %collective-permute-start = (bf16[192,2048]{1,0:T(8,128)(2,1)}, bf16[192,2048]{1,0:T(8,128)(2,1)S(1)}, u32[]{:S(2)}, u32[]{:S(2)}) collective-permute-start(bf16[192,2048]{1,0:T(8,128)(2,1)} %own_hbm.3), channel_id=1, source_target_pairs={{0,1},{1,0},{2,3},{3,2},{4,5},{5,4},{6,7},{7,6},{8,9},{9,8},{10,11... | collective-permute-start | bytes 2359304 | tf_op jit(solution)/shard_map/ppermute | solution.py:396
  1.4 0.0 copy-start.1
  1.4 1.0 %shard_map.137 = bf16[16,2048]{1,0:T(8,128)(2,1)S(1)} custom-call(bf16[192,2048]{1,0:T(8,128)(2,1)} %own_hbm.3), custom_call_target="tpu_custom_call" | custom-call | flops 99999997952 | bytes 1048576 | tf_op jit(solution)/shard_map/pallas_call | solution.py:52
  2.4 0.0 copy-start.2
  2.4 0.0 copy-start.3
  2.4 0.0 copy-start.4
  2.4 0.0 copy-start.7
  2.4 3.5 %collective-permute-start.2 = (bf16[16,2048]{1,0:T(8,128)(2,1)S(1)}, bf16[16,2048]{1,0:T(8,128)(2,1)S(1)}, u32[]{:S(2)}, u32[]{:S(2)}) collective-permute-start(bf16[16,2048]{1,0:T(8,128)(2,1)S(1)} %shard_map.137), channel_id=1, source_target_pairs={{1,3},{3,5},{5,7},{7,9},{9,11},{11,13},{13,15},{15,17},{17,19},{19... | collective-permute-start | bytes 196616 | tf_op jit(solution)/shard_map/ppermute | solution.py:405
  5.9 1.3 %collective-permute-start.1 = (bf16[16,2048]{1,0:T(8,128)(2,1)S(1)}, bf16[16,2048]{1,0:T(8,128)(2,1)S(1)}, u32[]{:S(2)}, u32[]{:S(2)}) collective-permute-start(bf16[16,2048]{1,0:T(8,128)(2,1)S(1)} %shard_map.137), channel_id=1, source_target_pairs={{1,2},{3,4},{5,6},{7,8},{9,10},{11,12},{13,14},{15,16},{17,18},{19... | collective-permute-start | bytes 196616 | tf_op jit(solution)/shard_map/ppermute | solution.py:406
  7.2 2.1 %shard_map.136 = (bf16[192,2048]{1,0:T(8,128)(2,1)S(1)}, bf16[2048,128]{1,0:T(8,128)(2,1)S(1)}, f32[192,128]{1,0:T(8,128)S(1)}) custom-call(bf16[192,2048]{1,0:T(8,128)(2,1)} %own_hbm.3, f32[1,2048]{1,0:T(1,128)} %bitcast.12, bf16[8,2048]{1,0:T(8,128)(2,1)} %bitcast.18, bf16[8,2048]{1,0:T(8,128)(2,1)} %bitcast.19), custom_call_target="tpu_custom_call" | custom-call | flops 1000000000 | bytes 1048576 | tf_op jit(solution)/shard_map/pallas_call | solution.py:52
  9.3 0.0 collective-permute-done.2.two_ref
  9.4 0.0 collective-permute-done.1.one_ref
  9.4 0.0 collective-permute-done.oth_ref
  9.4 0.0 copy-done.1
  9.4 0.0 copy-done.2
  9.4 0.0 copy-done.3
  9.4 0.0 copy-done.4
  9.4 0.0 copy-done.7
  9.4 0.0 copy-start.5
  9.4 4.9 %shard_map.138 = (bf16[384,512]{1,0:T(8,128)(2,1)S(1)}, bf16[384,1024]{1,0:T(8,128)(2,1)S(1)}, f32[384,128]{1,0:T(8,128)S(1)}, bf16[512,384]{1,0:T(8,128)(2,1)}, bf16[400,2048]{1,0:T(8,128)(2,1)S(1)}) custom-call(bf16[192,2048]{1,0:T(8,128)(2,1)S(1)} %get-tuple-element.24.own_ref, bf16[192,2048]{1,0:T(8,128)(2,1)S(1)} %collective-permute-done.oth_ref, ...), custom_call_target="tpu_custom_call" | custom-call | flops 3000000000 | bytes 1048576 | tf_op jit(solution)/shard_map/pallas_call | solution.py:52
  14.4 14.6 %all-to-all-start = ((bf16[64,8,384]{2,1,0:T(8,128)(2,1)}), bf16[64,8,384]{2,1,0:T(8,128)(2,1)S(1)}, u32[]{:S(2)}, u32[]{:S(2)}) async-start(bf16[64,8,384]{2,1,0:T(8,128)(2,1)} %bitcast.17), calls=%async_computation | async-start | bytes 786432 | tf_op jit(solution)/shard_map/all_to_all | solution.py:439
  28.9 0.0 copy-done.5
  28.9 0.0 copy-start
  28.9 0.0 copy-start.6
  29.0 4.7 %shard_map.139 = (bf16[384,512]{1,0:T(8,128)(2,1)S(1)}, bf16[384,1024]{1,0:T(8,128)(2,1)S(1)}, f32[384,128]{1,0:T(8,128)S(1)}) custom-call(bf16[400,2048]{1,0:T(8,128)(2,1)S(1)} %get-tuple-element.37.rows_ref, bf16[2048,512]{1,0:T(8,128)(2,1)} %wq_hbm.1, ...), custom_call_target="tpu_custom_call", output_to_operand_aliasing={{0}: (2, {}), {1}: (3, {}), {2}: (4, {})} | custom-call | flops 4000000000 | bytes 1048576 | tf_op jit(solution)/shard_map/pallas_call | solution.py:52
  33.7 0.0 all-to-all-done
  33.7 0.0 copy-done
  33.7 1.9 %shard_map.140 = bf16[512,384]{1,0:T(8,128)(2,1)} custom-call(bf16[512,384]{1,0:T(8,128)(2,1)S(1)} %bitcast.11, s32[2,64,64]{2,1,0:T(8,128)S(1)} %copy-done), custom_call_target="tpu_custom_call" | custom-call | flops 100000000 | bytes 1048576 | tf_op jit(solution)/shard_map/pallas_call | solution.py:52
  35.6 9.9 %all-to-all-start.1 = ((bf16[64,8,384]{2,1,0:T(8,128)(2,1)}), bf16[64,8,384]{2,1,0:T(8,128)(2,1)S(1)}, u32[]{:S(2)}, u32[]{:S(2)}) async-start(bf16[64,8,384]{2,1,0:T(8,128)(2,1)} %bitcast.16), calls=%async_computation.1 | async-start | bytes 786432 | tf_op jit(solution)/shard_map/all_to_all | solution.py:454
  45.5 0.0 copy-done.6
  45.6 3.8 %shard_map.141.wide_ref = bf16[400,2048]{1,0:T(8,128)(2,1)S(1)} custom-call(bf16[400,2048]{1,0:T(8,128)(2,1)S(1)} %get-tuple-element.37.rows_ref, bf16[2048,1024]{1,0:T(8,128)(2,1)} %wo_hbm.1, f32[1,2048]{1,0:T(1,128)S(1)} %bitcast.14), custom_call_target="tpu_custom_call", output_to_operand_aliasing={{}: (0, {})} | custom-call | flops 4000000000 | bytes 1048576 | tf_op jit(solution)/shard_map/pallas_call | solution.py:52
  49.4 0.0 all-to-all-done.1
  49.4 3.9 %shard_map.142 = (bf16[192,2048]{1,0:T(8,128)(2,1)S(1)}, bf16[1024,2048]{1,0:T(8,128)(2,1)S(1)}) custom-call(bf16[384,512]{1,0:T(8,128)(2,1)S(1)} %get-tuple-element.35.query_ref, bf16[400,2048]{1,0:T(8,128)(2,1)S(1)} %shard_map.141.wide_ref, bf16[512,384]{1,0:T(8,128)(2,1)S(1)} %bitcast.9, bf16[384,1024]{1,0:T(8,128)(2,1)S(1)} %get-tuple-element.39.numer_ref, ...), custom_call_target="tpu_custom_call" | custom-call | flops 1000000000 | bytes 1048576 | tf_op jit(solution)/shard_map/pallas_call | solution.py:52
  53.4 3.8 %collective-permute-start.3 = (bf16[192,2048]{1,0:T(8,128)(2,1)S(1)}, bf16[192,2048]{1,0:T(8,128)(2,1)S(1)}, u32[]{:S(2)}, u32[]{:S(2)}) collective-permute-start(bf16[192,2048]{1,0:T(8,128)(2,1)S(1)} %get-tuple-element.42), channel_id=1, source_target_pairs={{0,1},{1,0},{2,3},{3,2},{4,5},{5,4},{6,7},{7,6},{8,9},{9,8},{10,11... | collective-permute-start | bytes 2359304 | tf_op jit(solution)/shard_map/ppermute | solution.py:475
  57.2 2.0 %shard_map.143 = f32[192,2048]{1,0:T(8,128)S(1)} custom-call(bf16[384,512]{1,0:T(8,128)(2,1)S(1)} %get-tuple-element.35.query_ref, bf16[400,2048]{1,0:T(8,128)(2,1)S(1)} %shard_map.141.wide_ref, bf16[512,384]{1,0:T(8,128)(2,1)S(1)} %bitcast.10, bf16[384,1024]{1,0:T(8,128)(2,1)S(1)} %get-tuple-element.39.numer_ref, ...), custom_call_target="tpu_custom_call" | custom-call | flops 1000000000 | bytes 1048576 | tf_op jit(solution)/shard_map/pallas_call | solution.py:52
  59.2 0.0 collective-permute-done.3
  59.2 1.1 %add_convert_fusion = bf16[192,2048]{1,0:T(8,128)(2,1)} fusion(f32[192,2048]{1,0:T(8,128)S(1)} %shard_map.143, bf16[192,2048]{1,0:T(8,128)(2,1)S(1)} %collective-permute-done.3), kind=kLoop, calls=%fused_computation | loop fusion | flops 1179648 | bytes 3145728 | tf_op jit(solution)/shard_map/convert_element_type | solution.py:479
Async XLA Ops:
  0.0 9.4 %collective-permute-start = (bf16[192,2048]{1,0:T(8,128)(2,1)}, bf16[192,2048]{1,0:T(8,128)(2,1)S(1)}, u32[]{:S(2)}, u32[]{:S(2)}) collective-permute-start(bf16[192,2048]{1,0:T(8,128)(2,1)} %own_hbm.3), channel_id=1, source_target_pairs={{0,1},{1,0},{2,3},{3,2},{4,5},{5,4},{6,7},{7,6},{8,9},{9,8},{10,11... | collective-permute-start | bytes 2359304 | tf_op jit(solution)/shard_map/ppermute | solution.py:396
  1.4 8.0 %copy-start.1 = (bf16[2048,1024]{1,0:T(8,128)(2,1)S(1)}, bf16[2048,1024]{1,0:T(8,128)(2,1)}, u32[]{:S(2)}) copy-start(bf16[2048,1024]{1,0:T(8,128)(2,1)} %wv_ref.1) | copy-start | bytes 12582916
  2.4 7.0 %copy-start.2 = (bf16[2048,512]{1,0:T(8,128)(2,1)S(1)}, bf16[2048,512]{1,0:T(8,128)(2,1)}, u32[]{:S(2)}) copy-start(bf16[2048,512]{1,0:T(8,128)(2,1)} %wk_ref.1) | copy-start | bytes 6291460
  2.4 7.0 %copy-start.3 = (f32[2048]{0:T(1024)S(1)}, f32[2048]{0:T(1024)}, u32[]{:S(2)}) copy-start(f32[2048]{0:T(1024)} %param.15) | copy-start | bytes 24580
  2.4 7.0 %copy-start.4 = (bf16[4,1024]{1,0:T(4,128)(2,1)S(1)}, bf16[4,1024]{1,0:T(4,128)(2,1)}, u32[]{:S(2)}) copy-start(bf16[4,1024]{1,0:T(4,128)(2,1)} %taps_ref.2) | copy-start | bytes 24580
  2.4 7.0 %copy-start.7 = (f32[2,3,4]{2,0,1:T(2,128)S(1)}, f32[2,3,4]{2,0,1:T(2,128)}, u32[]{:S(2)}) copy-start(f32[2,3,4]{2,0,1:T(2,128)} %param.24) | copy-start | bytes 292
  2.4 6.9 %collective-permute-start.2 = (bf16[16,2048]{1,0:T(8,128)(2,1)S(1)}, bf16[16,2048]{1,0:T(8,128)(2,1)S(1)}, u32[]{:S(2)}, u32[]{:S(2)}) collective-permute-start(bf16[16,2048]{1,0:T(8,128)(2,1)S(1)} %shard_map.137), channel_id=1, source_target_pairs={{1,3},{3,5},{5,7},{7,9},{9,11},{11,13},{13,15},{15,17},{17,19},{19... | collective-permute-start | bytes 196616 | tf_op jit(solution)/shard_map/ppermute | solution.py:405
  5.9 3.4 %collective-permute-start.1 = (bf16[16,2048]{1,0:T(8,128)(2,1)S(1)}, bf16[16,2048]{1,0:T(8,128)(2,1)S(1)}, u32[]{:S(2)}, u32[]{:S(2)}) collective-permute-start(bf16[16,2048]{1,0:T(8,128)(2,1)S(1)} %shard_map.137), channel_id=1, source_target_pairs={{1,2},{3,4},{5,6},{7,8},{9,10},{11,12},{13,14},{15,16},{17,18},{19... | collective-permute-start | bytes 196616 | tf_op jit(solution)/shard_map/ppermute | solution.py:406
  9.4 19.5 %copy-start.5 = (bf16[4,1024]{1,0:T(4,128)(2,1)S(1)}, bf16[4,1024]{1,0:T(4,128)(2,1)}, u32[]{:S(2)}) copy-start(bf16[4,1024]{1,0:T(4,128)(2,1)} %taps_ref.3) | copy-start | bytes 24580
  14.4 19.3 %all-to-all-start = ((bf16[64,8,384]{2,1,0:T(8,128)(2,1)}), bf16[64,8,384]{2,1,0:T(8,128)(2,1)S(1)}, u32[]{:S(2)}, u32[]{:S(2)}) async-start(bf16[64,8,384]{2,1,0:T(8,128)(2,1)} %bitcast.17), calls=%async_computation | async-start | bytes 786432 | tf_op jit(solution)/shard_map/all_to_all | solution.py:439
  28.9 4.7 %copy-start = (s32[2,64,64]{2,1,0:T(8,128)S(1)}, s32[2,64,64]{2,1,0:T(8,128)}, u32[]{:S(2)}) copy-start(s32[2,64,64]{2,1,0:T(8,128)} %constant.2.clone.place_ref) | copy-start | bytes 98308
  28.9 16.6 %copy-start.6 = (f32[2048]{0:T(1024)S(1)}, f32[2048]{0:T(1024)}, u32[]{:S(2)}) copy-start(f32[2048]{0:T(1024)} %param.25) | copy-start | bytes 24580
  35.6 13.8 %all-to-all-start.1 = ((bf16[64,8,384]{2,1,0:T(8,128)(2,1)}), bf16[64,8,384]{2,1,0:T(8,128)(2,1)S(1)}, u32[]{:S(2)}, u32[]{:S(2)}) async-start(bf16[64,8,384]{2,1,0:T(8,128)(2,1)} %bitcast.16), calls=%async_computation.1 | async-start | bytes 786432 | tf_op jit(solution)/shard_map/all_to_all | solution.py:454
  53.4 5.8 %collective-permute-start.3 = (bf16[192,2048]{1,0:T(8,128)(2,1)S(1)}, bf16[192,2048]{1,0:T(8,128)(2,1)S(1)}, u32[]{:S(2)}, u32[]{:S(2)}) collective-permute-start(bf16[192,2048]{1,0:T(8,128)(2,1)S(1)} %get-tuple-element.42), channel_id=1, source_target_pairs={{0,1},{1,0},{2,3},{3,2},{4,5},{5,4},{6,7},{7,6},{8,9},{9,8},{10,11... | collective-permute-start | bytes 2359304 | tf_op jit(solution)/shard_map/ppermute | solution.py:475

commit v6 on v3

--- a/solution.py
+++ b/solution.py
@@ -97,14 +97,9 @@
     return (x * row_scale(x) * gain).astype(BF)
 
 
-def fetch_kernel(own_hbm, gain_hbm, wk_hbm, wv_hbm, wi_hbm, wf_hbm,
-                 rows_ref, wk_ref, wv_ref, wg_ref, gates_ref, own_ref, gain_ref, wi_ref, wf_ref, flat_ref, sems):
-    copies = started(
-        [(own_hbm, own_ref), (gain_hbm, gain_ref), (wi_hbm, wi_ref), (wf_hbm, wf_ref)]
-        + by_rows(wk_hbm, wk_ref, 4)
-        + by_rows(wv_hbm, wv_ref, 8),
-        sems,
-    )
+def fetch_kernel(own_hbm, gain_hbm, wi_hbm, wf_hbm,
+                 rows_ref, wg_ref, gates_ref, own_ref, gain_ref, wi_ref, wf_ref, flat_ref, sems):
+    copies = started([(own_hbm, own_ref), (gain_hbm, gain_ref), (wi_hbm, wi_ref), (wf_hbm, wf_ref)], sems)
     copies[0].wait()
     parts = [slice(at, at + 48) for at in range(0, HALF, 48)]
     scales = [row_scale(own_ref[part, :].astype(F32)) for part in parts]
@@ -120,29 +115,38 @@
     for at in range(0, wg_ref.shape[0], 128):
         wg_ref[at : at + 128, :] = flat_ref[:, at : at + 128].T.astype(BF)
     gates_ref[...] = jnp.dot(rows_ref[...], wg_ref[...], preferred_element_type=F32)
-    wait_all(copies[4:])
-
-
-def summary_kernel(own_ref, oth_ref, one_ref, two_ref, gain_ref, wk_ref, wv_ref, wg_ref, gates_ref, taps_ref, offs_ref,
-                   key_ref, value_ref, logs_ref, piece_ref, rows_ref, pre_ref, both_ref):
+
+
+def spread_kernel(own_ref, oth_ref, gain_ref, rows_ref, tail_ref):
     tp = lax.axis_index("tp")
     gain = gain_ref[...]
-    rows_ref[0:TAIL, :] = normalized(one_ref[...] + two_ref[...], gain)
-    mine = pl.multiple_of(TAIL + tp * HALF, 16)
-    rows_ref[pl.ds(mine, HALF), :] = own_ref[...]
+    rows_ref[0:TAIL, :] = jnp.zeros((TAIL, rows_ref.shape[1]), BF)
+    rows_ref[pl.ds(pl.multiple_of(TAIL + tp * HALF, 16), HALF), :] = own_ref[...]
     for part in range(HALF // 48):
         to = pl.multiple_of(TAIL + (1 - tp) * HALF + part * 48, 16)
         rows_ref[pl.ds(to, 48), :] = normalized(oth_ref[part * 48 : part * 48 + 48, :], gain)
+    tail_ref[...] = rows_ref[ROWS : ROWS + TAIL, :]
+
+
+def project_kernel(rows_ref, wk_ref, wv_ref, wg_ref, gates_ref, pre_ref, value_ref, both_ref):
+    tp = lax.axis_index("tp")
     own = pl.ds(TAIL, ROWS)
-    theirs = pl.multiple_of((1 - tp) * HALF, 8)
     both_ref[pl.ds(pl.multiple_of(tp * HALF, 8), HALF), :] = gates_ref[...]
-    both_ref[pl.ds(theirs, HALF), :] = jnp.dot(
+    both_ref[pl.ds(pl.multiple_of((1 - tp) * HALF, 8), HALF), :] = jnp.dot(
         rows_ref[pl.ds(pl.multiple_of(TAIL + (1 - tp) * HALF, 16), HALF), :], wg_ref[...], preferred_element_type=F32
     )
+    pre_ref[...] = jnp.dot(rows_ref[own, :], wk_ref[...], preferred_element_type=F32).astype(BF).astype(F32)
+    value_ref[...] = jnp.dot(rows_ref[own, :], wv_ref[...], preferred_element_type=F32).astype(BF)
+
+
+def summary_kernel(rows_ref, tail_ref, wk_ref, own_pre_ref, value_ref, both_ref, taps_ref, offs_ref,
+                   rows_out, key_ref, logs_ref, piece_out, pre_ref, piece_ref, sems):
+    tp = lax.axis_index("tp")
+    rows_out[0:TAIL, :] = tail_ref[...]
+    pre_ref[0:TAIL, :] = jnp.dot(tail_ref[...], wk_ref[...], preferred_element_type=F32).astype(BF).astype(F32)
+    pre_ref[TAIL : TAIL + ROWS, :] = own_pre_ref[...]
     gates = both_ref[...]
     gates = jnp.where(tp == 0, gates, pltpu.roll(gates, 128 - HEADS, 1))
-    pre_ref[...] = jnp.dot(rows_ref[...], wk_ref[...], preferred_element_type=F32).astype(BF).astype(F32)
-
     lane = lane_of((SPAN, 128))
     tri = (lax.broadcasted_iota(jnp.int32, (SPAN, SPAN), 0) >= lax.broadcasted_iota(jnp.int32, (SPAN, SPAN), 1)).astype(F32)
     gate, inside, totals = [], [], []
@@ -176,8 +180,8 @@
         for b in range(BLOCKS):
             rows = slice(b * SPAN, (b + 1) * SPAN)
             key_ref[rows, lanes] = (mixed_rows(pre_ref, taps, lanes, b * SPAN, SPAN) * DQK**-0.5).astype(BF)
-    value_ref[...] = jnp.dot(rows_ref[own, :], wv_ref[...], preferred_element_type=F32).astype(BF)
     ones = jnp.ones((ROWS, 128), BF)
+    copies = []
     dims = (((0,), (0,)), ((), ()))
     for h in range(HEADS):
         lanes = slice(h * DQK, (h + 1) * DQK)
@@ -195,6 +199,10 @@
         out = slice(h * DQK, (h + 1) * DQK)
         piece_ref[out, :DV] = memory.astype(BF)
         piece_ref[out, DV:] = extra.astype(BF)
+        copy = pltpu.make_async_copy(piece_ref.at[pl.ds(h * DQK, DQK)], piece_out.at[pl.ds(h * DQK, DQK)], sems.at[h])
+        copy.start()
+        copies.append(copy)
+    wait_all(copies)
 
 
 def prefix_kernel(piece_ref, place_ref, wout_hbm, out_ref, wout_ref, sems):
@@ -373,9 +381,6 @@
     stretches = lax.axis_size(SP)
     shape = jax.ShapeDtypeStruct
     other = lax.ppermute(tokens, "tp", [(0, 1), (1, 0)])
-    last = tokens[HALF - TAIL :]
-    to_second = lax.ppermute(last, SP_TP, [(2 * i + 1, 2 * i + 3) for i in range(stretches - 1)])
-    to_first = lax.ppermute(last, SP_TP, [(2 * i + 1, 2 * i + 2) for i in range(stretches - 1)])
     gain = norm_gain.reshape(1, -1)
     head_gain = head_gain.reshape(1, -1)
     order = far_first(stretches)
@@ -392,22 +397,33 @@
         return pltpu.VMEM(like.shape, like.dtype)
 
     gates_shape = shape((width, 128), BF), shape((HALF, 128), F32)
-    own, wk, wv, wg, gates = call(
+    own, wg, gates = call(
         fetch_kernel,
-        (shape(tokens.shape, BF), shape(w_key.shape, BF), shape(w_value.shape, BF), *gates_shape),
-        (v, v, v, v, v),
-        [m, m, m, m, m, m],
-        [room(tokens), room(gain), *[pltpu.VMEM((w_igate.shape[1], width), BF)] * 2, pltpu.VMEM((128, width), F32), dma((16,))],
+        (shape(tokens.shape, BF), *gates_shape),
+        (v, v, v),
+        [m, m, m, m],
+        [room(tokens), room(gain), *[pltpu.VMEM((w_igate.shape[1], width), BF)] * 2, pltpu.VMEM((128, width), F32), dma((4,))],
+        flops=100_000_000_000,
+    )(tokens, gain, w_igate.T, w_fgate.T)
+    rows, last = call(spread_kernel, (rows_shape, shape((TAIL, width), BF)), (v, n), [v, n, n], flops=100_000_000)(own, other, gain)
+    tail = lax.ppermute(last, SP, [(i, i + 1) for i in range(stretches - 1)])
+    own_pre_shape = shape((ROWS, HEADS * DQK), F32)
+    own_pre, value, both = call(
+        project_kernel,
+        (own_pre_shape, value_shape, logs_shape),
+        (v, v, v),
+        [v, n, n, v, v],
+        flops=3_000_000_000,
+    )(rows, w_key, w_value, wg, gates)
+    rows, key, logs, pieces = call(
+        summary_kernel,
+        (rows_shape, key_shape, logs_shape, shape((HEADS * DQK, WIDTH), BF)),
+        (v, v, v, m),
+        [v, n, n, v, v, v, n, n],
+        [room(pre_shape), pltpu.VMEM((HEADS * DQK, WIDTH), BF), dma((HEADS,))],
         flops=1_000_000_000,
-    )(tokens, gain, w_key, w_value, w_igate.T, w_fgate.T)
-    key, value, logs, pieces, rows = call(
-        summary_kernel,
-        (key_shape, value_shape, logs_shape, shape((HEADS * DQK, WIDTH), BF), rows_shape),
-        (v, v, v, n, v),
-        [v, n, n, n, n, v, v, v, v, n, n],
-        [room(pre_shape), room(logs_shape)],
-        flops=3_000_000_000,
-    )(own, other, to_first, to_second, gain, wk, wv, wg, gates, conv_key, gate_offset.transpose(1, 0, 2))
+        aliases={0: 0},
+    )(rows, tail, w_key, own_pre, value, both, conv_key, gate_offset.transpose(1, 0, 2))
     pieces = lax.all_to_all(pieces.reshape(stretches, 8, WIDTH), SP_TP, 0, 0, axis_index_groups=groups, tiled=True)
     query, wide, stats = call(
         local_kernel,

time: 60.1 us -> 59.2 us (0.985)
  local copies, waits for them, and re-layouts: 0.88 us -> 0.04 us
    all_to_all x1, starting transfers between devices: 13.4 us -> 15.5 us  [body(): lax.all_to_all(pieces.reshape(stretches, 8, WIDTH), SP_TP, 0, 0, axis_ind...]
    ppermute x2 -> x1, starting transfers between devices: 4.51 us -> 3.23 us  [body(): tail = lax.ppermute(last, SP, [(i, i + 1) for i in range(stretches - 1)])]
    ppermute x1, starting transfers between devices: 3.75 us -> 2.8 us  [body(): got = lax.ppermute(sent, 'tp', [(0, 1), (1, 0)])]
    slice x1 -> x0, local copies, waits for them, and re-layouts: 0.84 us -> none  [body(): last = tokens[HALF - TAIL:]]
    pallas_call x6 -> x8, Pallas kernels: 21.2 us -> 21.2 us  [call(): return lambda *args: run(*map(kept, args, spaces))]
  transfers between devices with their start and end apart: 5 -> 4, of which waited for: 1 -> 1; matrix products, arithmetic and copies ran while one was open for 1% -> 0% of each run, Pallas kernels for 20% -> 23%
where the time goes in v6:
time: 59.2 us; the launch traced here: 59 us
  starting transfers between devices  22.9 us (39%)
  Pallas kernels  21.2 us (36%)
  blocking collectives  13.3 us (22%)
  other arithmetic  1.09 us (2%)
    pallas_call x8, Pallas kernels, call(): return lambda *args: run(*map(kept, args, spaces))  21.2 us
    all_to_all x1, starting transfers between devices, body(): lax.all_to_all(pieces.reshape(stretches, 8, WIDTH), SP_TP, 0, 0, axis_ind...  15.5 us
    all_to_all x1, blocking collectives, body(): lax.all_to_all(state.reshape(stretches, 8, WIDTH), SP_TP, 0, 0, axis_inde...  13.3 us
    ppermute x1, starting transfers between devices, body(): tail = lax.ppermute(last, SP, [(i, i + 1) for i in range(stretches - 1)])  3.23 us
    ppermute x1, starting transfers between devices, body(): got = lax.ppermute(sent, 'tp', [(0, 1), (1, 0)])  2.8 us
    ppermute x1, starting transfers between devices, body(): other = lax.ppermute(tokens, 'tp', [(0, 1), (1, 0)])  1.38 us
  transfers between devices with their start and end apart: 4, of which 1 were waited for; matrix products, arithmetic and copies ran while one was open for 0% of the time, Pallas kernels for 23%

profile of v6, /device:TPU:1, one launch (start us, length us, event | category | flops | bytes accessed | tf_op | source)
XLA Modules:
  0.0 59.0 jit_solution(13845485003524288054)
XLA Ops:
  0.0 1.4 %collective-permute-start = (bf16[192,2048]{1,0:T(8,128)(2,1)}, bf16[192,2048]{1,0:T(8,128)(2,1)S(1)}, u32[]{:S(2)}, u32[]{:S(2)}) collective-permute-start(bf16[192,2048]{1,0:T(8,128)(2,1)} %own_hbm.1), channel_id=1, source_target_pairs={{0,1},{1,0},{2,3},{3,2},{4,5},{5,4},{6,7},{7,6},{8,9},{9,8},{10,11... | collective-permute-start | bytes 2359304 | tf_op jit(solution)/shard_map/ppermute | solution.py:383
  1.4 0.0 copy-start.2
  1.4 0.0 copy-start
  1.4 0.0 copy-start.5
  1.4 2.2 %shard_map.136 = (bf16[192,2048]{1,0:T(8,128)(2,1)S(1)}, bf16[2048,128]{1,0:T(8,128)(2,1)S(1)}, f32[192,128]{1,0:T(8,128)S(1)}) custom-call(bf16[192,2048]{1,0:T(8,128)(2,1)} %own_hbm.1, f32[1,2048]{1,0:T(1,128)} %bitcast.13, bf16[8,2048]{1,0:T(8,128)(2,1)} %bitcast.18, bf16[8,2048]{1,0:T(8,128)(2,1)} %bitcast.19), custom_call_target="tpu_custom_call" | custom-call | flops 99999997952 | bytes 1048576 | tf_op jit(solution)/shard_map/pallas_call | solution.py:52
  3.6 0.0 collective-permute-done.oth_ref
  3.7 0.0 copy-done.2
  3.7 0.4 shard_map.137
  4.1 3.2 %collective-permute-start.1 = (bf16[16,2048]{1,0:T(8,128)(2,1)S(1)}, bf16[16,2048]{1,0:T(8,128)(2,1)S(1)}, u32[]{:S(2)}, u32[]{:S(2)}) collective-permute-start(bf16[16,2048]{1,0:T(8,128)(2,1)S(1)} %get-tuple-element.30), channel_id=1, source_target_pairs={{0,2},{2,4},{4,6},{6,8},{8,10},{10,12},{12,14},{14,16},{16,18},{18... | collective-permute-start | bytes 196616 | tf_op jit(solution)/shard_map/ppermute | solution.py:409
  7.3 0.0 copy-done
  7.3 0.0 copy-done.5
  7.3 0.0 copy-start.3
  7.4 0.0 copy-start.4
  7.4 2.8 %shard_map.138 = (f32[384,512]{1,0:T(8,128)S(1)}, bf16[384,1024]{1,0:T(8,128)(2,1)S(1)}, f32[384,128]{1,0:T(8,128)S(1)}) custom-call(bf16[400,2048]{1,0:T(8,128)(2,1)S(1)} %get-tuple-element.29.rows_ref, bf16[2048,512]{1,0:T(8,128)(2,1)S(1)} %copy-done, bf16[2048,1024]{1,0:T(8,128)(2,1)S(1)} %copy-done.5, bf16[2048,128]{1,0:T(8,128)(2,1)S(1)} %get-tuple-element.31.wg_ref, ...), custom_call_target="tpu_custom_call" | custom-call | flops 3000000000 | bytes 1048576 | tf_op jit(solution)/shard_map/pallas_call | solution.py:52
  10.2 0.0 collective-permute-done.1.tail_ref
  10.2 0.0 copy-done.3
  10.2 0.0 copy-done.4
  10.2 0.0 copy-start.6
  10.2 0.0 copy-start.7
  10.2 2.7 %shard_map.139 = (bf16[400,2048]{1,0:T(8,128)(2,1)S(1)}, bf16[384,512]{1,0:T(8,128)(2,1)S(1)}, f32[384,128]{1,0:T(8,128)S(1)}, bf16[512,384]{1,0:T(8,128)(2,1)}) custom-call(bf16[400,2048]{1,0:T(8,128)(2,1)S(1)} %get-tuple-element.29.rows_ref, bf16[16,2048]{1,0:T(8,128)(2,1)S(1)} %collective-permute-done.1.tail_ref, ...), custom_call_target="tpu_custom_call", output_to_operand_aliasing={{0}: (0, {})} | custom-call | flops 1000000000 | bytes 1048576 | tf_op jit(solution)/shard_map/pallas_call | solution.py:52
  13.0 15.5 %all-to-all-start = ((bf16[64,8,384]{2,1,0:T(8,128)(2,1)}), bf16[64,8,384]{2,1,0:T(8,128)(2,1)S(1)}, u32[]{:S(2)}, u32[]{:S(2)}) async-start(bf16[64,8,384]{2,1,0:T(8,128)(2,1)} %bitcast.17), calls=%async_computation | async-start | bytes 786432 | tf_op jit(solution)/shard_map/all_to_all | solution.py:427
  28.4 0.0 copy-done.6
  28.4 0.0 copy-done.7
  28.5 0.0 copy-start.1
  28.5 7.0 %shard_map.140 = (bf16[384,512]{1,0:T(8,128)(2,1)S(1)}, bf16[400,2048]{1,0:T(8,128)(2,1)S(1)}, f32[384,128]{1,0:T(8,128)S(1)}) custom-call(bf16[400,2048]{1,0:T(8,128)(2,1)S(1)} %get-tuple-element.37.rows_ref, bf16[2048,512]{1,0:T(8,128)(2,1)} %wq_hbm.1, ...), custom_call_target="tpu_custom_call", output_to_operand_aliasing={{0}: (2, {}), {1}: (0, {}), {2}: (4, {})} | custom-call | flops 6000000000 | bytes 1048576 | tf_op jit(solution)/shard_map/pallas_call | solution.py:52
  35.5 0.0 all-to-all-done
  35.5 0.0 copy-done.1
  35.5 1.6 %shard_map.141 = (bf16[512,384]{1,0:T(8,128)(2,1)S(1)}, bf16[512,2048]{1,0:T(8,128)(2,1)S(1)}) custom-call(bf16[512,384]{1,0:T(8,128)(2,1)S(1)} %bitcast.11, s32[2,64,64]{2,1,0:T(8,128)S(1)} %copy-done.1, bf16[1024,2048]{1,0:T(8,128)(2,1)} %wout_hbm.3), custom_call_target="tpu_custom_call" | custom-call | flops 100000000 | bytes 1048576 | tf_op jit(solution)/shard_map/pallas_call | solution.py:52
  37.1 13.3 %all_to_all.10 = bf16[64,8,384]{2,1,0:T(8,128)(2,1)S(1)} all-to-all(bf16[64,8,384]{2,1,0:T(8,128)(2,1)S(1)} %bitcast.12), channel_id=1, replica_groups={{84,52,76,82,86,92,116,20,44,50,54,60,68,74,78,80,90,94,108,114,118,124..., dimensions={0} | all-to-all | bytes 786432 | tf_op jit(solution)/shard_map/all_to_all | solution.py:444
  50.4 2.7 %shard_map.142 = (bf16[192,2048]{1,0:T(8,128)(2,1)S(1)}, bf16[512,2048]{1,0:T(8,128)(2,1)S(1)}) custom-call(bf16[384,512]{1,0:T(8,128)(2,1)S(1)} %get-tuple-element.43.query_ref, bf16[400,2048]{1,0:T(8,128)(2,1)S(1)} %get-tuple-element.44.wide_ref, bf16[512,384]{1,0:T(8,128)(2,1)S(1)} %bitcast.9, f32[384,128]{1,0:T(8,128)S(1)} %get-tuple-element.47.stats_ref, ...), custom_call_target="tpu_custom_call" | custom-call | flops 1000000000 | bytes 1048576 | tf_op jit(solution)/shard_map/pallas_call | solution.py:52
  53.2 2.8 %collective-permute-start.2 = (bf16[192,2048]{1,0:T(8,128)(2,1)S(1)}, bf16[192,2048]{1,0:T(8,128)(2,1)S(1)}, u32[]{:S(2)}, u32[]{:S(2)}) collective-permute-start(bf16[192,2048]{1,0:T(8,128)(2,1)S(1)} %get-tuple-element.50), channel_id=1, source_target_pairs={{0,1},{1,0},{2,3},{3,2},{4,5},{5,4},{6,7},{7,6},{8,9},{9,8},{10,11... | collective-permute-start | bytes 2359304 | tf_op jit(solution)/shard_map/ppermute | solution.py:455
  56.0 1.7 %shard_map.143 = f32[192,2048]{1,0:T(8,128)S(1)} custom-call(bf16[384,512]{1,0:T(8,128)(2,1)S(1)} %get-tuple-element.43.query_ref, bf16[400,2048]{1,0:T(8,128)(2,1)S(1)} %get-tuple-element.44.wide_ref, bf16[512,384]{1,0:T(8,128)(2,1)S(1)} %bitcast.10, f32[384,128]{1,0:T(8,128)S(1)} %get-tuple-element.47.stats_ref, ...), custom_call_target="tpu_custom_call" | custom-call | flops 1000000000 | bytes 1048576 | tf_op jit(solution)/shard_map/pallas_call | solution.py:52
  57.6 0.2 collective-permute-done.2
  57.9 1.1 %add_convert_fusion = bf16[192,2048]{1,0:T(8,128)(2,1)} fusion(f32[192,2048]{1,0:T(8,128)S(1)} %shard_map.143, bf16[192,2048]{1,0:T(8,128)(2,1)S(1)} %collective-permute-done.2), kind=kLoop, calls=%fused_computation | loop fusion | flops 1179648 | bytes 3145728 | tf_op jit(solution)/shard_map/convert_element_type | solution.py:459
Async XLA Ops:
  0.0 3.6 %collective-permute-start = (bf16[192,2048]{1,0:T(8,128)(2,1)}, bf16[192,2048]{1,0:T(8,128)(2,1)S(1)}, u32[]{:S(2)}, u32[]{:S(2)}) collective-permute-start(bf16[192,2048]{1,0:T(8,128)(2,1)} %own_hbm.1), channel_id=1, source_target_pairs={{0,1},{1,0},{2,3},{3,2},{4,5},{5,4},{6,7},{7,6},{8,9},{9,8},{10,11... | collective-permute-start | bytes 2359304 | tf_op jit(solution)/shard_map/ppermute | solution.py:383
  1.4 2.3 %copy-start.2 = (f32[2048]{0:T(1024)S(1)}, f32[2048]{0:T(1024)}, u32[]{:S(2)}) copy-start(f32[2048]{0:T(1024)} %param.15) | copy-start | bytes 24580
  1.4 5.9 %copy-start = (bf16[2048,512]{1,0:T(8,128)(2,1)S(1)}, bf16[2048,512]{1,0:T(8,128)(2,1)}, u32[]{:S(2)}) copy-start(bf16[2048,512]{1,0:T(8,128)(2,1)} %wk_ref.3) | copy-start | bytes 6291460
  1.4 5.9 %copy-start.5 = (bf16[2048,1024]{1,0:T(8,128)(2,1)S(1)}, bf16[2048,1024]{1,0:T(8,128)(2,1)}, u32[]{:S(2)}) copy-start(bf16[2048,1024]{1,0:T(8,128)(2,1)} %wv_ref.1) | copy-start | bytes 12582916
  4.1 6.1 %collective-permute-start.1 = (bf16[16,2048]{1,0:T(8,128)(2,1)S(1)}, bf16[16,2048]{1,0:T(8,128)(2,1)S(1)}, u32[]{:S(2)}, u32[]{:S(2)}) collective-permute-start(bf16[16,2048]{1,0:T(8,128)(2,1)S(1)} %get-tuple-element.30), channel_id=1, source_target_pairs={{0,2},{2,4},{4,6},{6,8},{8,10},{10,12},{12,14},{14,16},{16,18},{18... | collective-permute-start | bytes 196616 | tf_op jit(solution)/shard_map/ppermute | solution.py:409
  7.3 2.8 %copy-start.3 = (bf16[4,1024]{1,0:T(4,128)(2,1)S(1)}, bf16[4,1024]{1,0:T(4,128)(2,1)}, u32[]{:S(2)}) copy-start(bf16[4,1024]{1,0:T(4,128)(2,1)} %taps_ref.2) | copy-start | bytes 24580
  7.4 2.8 %copy-start.4 = (f32[2,3,4]{2,0,1:T(2,128)S(1)}, f32[2,3,4]{2,0,1:T(2,128)}, u32[]{:S(2)}) copy-start(f32[2,3,4]{2,0,1:T(2,128)} %param.24) | copy-start | bytes 292
  10.2 18.2 %copy-start.6 = (bf16[4,1024]{1,0:T(4,128)(2,1)S(1)}, bf16[4,1024]{1,0:T(4,128)(2,1)}, u32[]{:S(2)}) copy-start(bf16[4,1024]{1,0:T(4,128)(2,1)} %taps_ref.3) | copy-start | bytes 24580
  10.2 18.2 %copy-start.7 = (f32[2048]{0:T(1024)S(1)}, f32[2048]{0:T(1024)}, u32[]{:S(2)}) copy-start(f32[2048]{0:T(1024)} %param.25) | copy-start | bytes 24580
  13.0 22.5 %all-to-all-start = ((bf16[64,8,384]{2,1,0:T(8,128)(2,1)}), bf16[64,8,384]{2,1,0:T(8,128)(2,1)S(1)}, u32[]{:S(2)}, u32[]{:S(2)}) async-start(bf16[64,8,384]{2,1,0:T(8,128)(2,1)} %bitcast.17), calls=%async_computation | async-start | bytes 786432 | tf_op jit(solution)/shard_map/all_to_all | solution.py:427
  28.5 7.1 %copy-start.1 = (s32[2,64,64]{2,1,0:T(8,128)S(1)}, s32[2,64,64]{2,1,0:T(8,128)}, u32[]{:S(2)}) copy-start(s32[2,64,64]{2,1,0:T(8,128)} %constant.2.clone.place_ref) | copy-start | bytes 98308
  53.2 4.7 %collective-permute-start.2 = (bf16[192,2048]{1,0:T(8,128)(2,1)S(1)}, bf16[192,2048]{1,0:T(8,128)(2,1)S(1)}, u32[]{:S(2)}, u32[]{:S(2)}) collective-permute-start(bf16[192,2048]{1,0:T(8,128)(2,1)S(1)} %get-tuple-element.50), channel_id=1, source_target_pairs={{0,1},{1,0},{2,3},{3,2},{4,5},{5,4},{6,7},{7,6},{8,9},{9,8},{10,11... | collective-permute-start | bytes 2359304 | tf_op jit(solution)/shard_map/ppermute | solution.py:455

commit v7 on v6

--- a/solution.py
+++ b/solution.py
@@ -205,8 +205,7 @@
     wait_all(copies)
 
 
-def prefix_kernel(piece_ref, place_ref, wout_hbm, out_ref, wout_ref, sems):
-    copies = started(by_rows(wout_hbm.at[pl.ds(0, wout_ref.shape[0])], wout_ref, 4), sems)
+def prefix_kernel(piece_ref, place_ref, out_ref):
     count = piece_ref.shape[0] // 8
     tall = piece_ref.shape[0]
 
@@ -247,21 +246,13 @@
     lane = lane_of((tall, 128))
     out_ref[:, :DV] = state[:, :DV].astype(BF)
     out_ref[:, DV:] = jnp.where((lane >= 1) & (lane < 4), marks, state[:, DV:]).astype(BF)
-    wait_all(copies)
 
 
 def local_kernel(rows_ref, wq_hbm, key_ref, value_ref, logs_ref, wo_hbm, taps_ref, gain_ref,
-                 query_out, wide_out, stats_ref, query_ref, numer_ref, ogate_ref, wq_ref, pre_ref, wo_ref, sems):
+                 query_out, wide_out, stats_ref, query_ref, numer_ref, ogate_ref, wq_ref, pre_ref, wo_ref, weight_ref, sems):
     copies = started(by_rows(wq_hbm, wq_ref, 4) + by_rows(wo_hbm, wo_ref, 8), sems)
     tp = lax.axis_index("tp")
     taps = taps_ref[:, pl.ds(pl.multiple_of(tp * (HEADS * DQK), 128), HEADS * DQK)].astype(F32)
-    wait_all(copies[:4])
-    pre_ref[...] = jnp.dot(rows_ref[...], wq_ref[...], preferred_element_type=F32).astype(BF).astype(F32)
-    for h in range(HEADS):
-        lanes = slice(h * DQK, (h + 1) * DQK)
-        for b in range(BLOCKS):
-            rows = slice(b * SPAN, (b + 1) * SPAN)
-            query_ref[rows, lanes] = mixed_rows(pre_ref, taps, lanes, b * SPAN, SPAN).astype(BF)
     lane = lane_of((SPAN, 128))
     cols = [logs_ref[b * SPAN : (b + 1) * SPAN, :] for b in range(BLOCKS)]
     flat = [c.T for c in cols]
@@ -296,14 +287,30 @@
             for x in logs:
                 peak = jnp.max(x, axis=1, keepdims=True)
                 top = peak if top is None else jnp.maximum(top, peak)
-            weight = jnp.concatenate([jnp.exp(x - top) for x in logs], axis=1)
+            for s, x in enumerate(logs):
+                weight_ref[h * ROWS + t * SPAN : h * ROWS + (t + 1) * SPAN, s * SPAN : (s + 1) * SPAN] = jnp.exp(x - top)
+            stats[t] = jnp.where(lane == HEADS + h, top, stats[t])
+    wait_all(copies[:4])
+    pre_ref[...] = jnp.dot(rows_ref[...], wq_ref[...], preferred_element_type=F32).astype(BF).astype(F32)
+    for h in range(HEADS):
+        lanes = slice(h * DQK, (h + 1) * DQK)
+        for b in range(BLOCKS):
+            rows = slice(b * SPAN, (b + 1) * SPAN)
+            query_ref[rows, lanes] = mixed_rows(pre_ref, taps, lanes, b * SPAN, SPAN).astype(BF)
+    for h in range(HEADS):
+        head = slice(h * DQK, (h + 1) * DQK)
+        wide = slice(h * DV, (h + 1) * DV)
+        for t in range(BLOCKS):
+            rows = slice(t * SPAN, (t + 1) * SPAN)
+            seen = (t + 1) * SPAN
+            weight = weight_ref[h * ROWS + t * SPAN : h * ROWS + (t + 1) * SPAN, :seen]
             scores = (
                 lax.dot_general(query_ref[rows, head], key_ref[:seen, head], nt, preferred_element_type=F32) * weight
             )
             denom = jnp.sum(scores, axis=1, keepdims=True)
             numer = jnp.dot(scores.astype(BF), value_ref[:seen, wide], preferred_element_type=F32)
             numer_ref[rows, wide] = numer.astype(BF)
-            stats[t] = jnp.where(lane == h, denom, jnp.where(lane == HEADS + h, top, stats[t]))
+            stats[t] = jnp.where(lane == h, denom, stats[t])
     for t in range(BLOCKS):
         stats_ref[t * SPAN : (t + 1) * SPAN, :] = stats[t]
     wait_all(copies[4:])
@@ -350,22 +357,16 @@
         hidden_ref[:, wide] = (cell * scale * wide_ref[rows, HEADS * DV + h * DV : HEADS * DV + (h + 1) * DV].astype(F32)).astype(BF)
 
 
-def sent_kernel(query_ref, wide_ref, state_ref, stats_ref, upper_ref, wout_hbm, out_ref, lower_ref, hidden_ref, sems):
-    deep = upper_ref.shape[0]
-    copies = started(by_rows(wout_hbm.at[pl.ds(deep, deep)], lower_ref, 4), sems)
+def sent_kernel(query_ref, wide_ref, state_ref, stats_ref, wout_ref, out_ref, hidden_ref):
     first = (1 - lax.axis_index("tp")) * HALF
     hidden_rows(first, query_ref, wide_ref, state_ref, stats_ref, hidden_ref)
-    part = jnp.dot(hidden_ref[:, :deep], upper_ref[...], preferred_element_type=F32)
-    wait_all(copies)
-    out_ref[...] = (part + jnp.dot(hidden_ref[:, deep:], lower_ref[...], preferred_element_type=F32)).astype(BF)
-
-
-def kept_kernel(query_ref, wide_ref, state_ref, stats_ref, upper_ref, lower_ref, out_ref, hidden_ref):
-    deep = upper_ref.shape[0]
+    out_ref[...] = jnp.dot(hidden_ref[...], wout_ref[...], preferred_element_type=F32).astype(BF)
+
+
+def kept_kernel(query_ref, wide_ref, state_ref, stats_ref, wout_ref, out_ref, hidden_ref):
     first = lax.axis_index("tp") * HALF
     hidden_rows(first, query_ref, wide_ref, state_ref, stats_ref, hidden_ref)
-    part = jnp.dot(hidden_ref[:, :deep], upper_ref[...], preferred_element_type=F32)
-    out_ref[...] = part + jnp.dot(hidden_ref[:, deep:], lower_ref[...], preferred_element_type=F32)
+    out_ref[...] = jnp.dot(hidden_ref[...], wout_ref[...], preferred_element_type=F32)
 
 
 def far_first(stretches):
@@ -430,31 +431,23 @@
         (key_shape, rows_shape, logs_shape),
         (v, v, v),
         [v, m, v, v, v, m, n, n],
-        [room(key_shape), room(value_shape), room(value_shape), room(w_query), room(pre_shape), room(w_ogate), dma((12,))],
+        [room(key_shape), room(value_shape), room(value_shape), room(w_query), room(pre_shape), room(w_ogate), pltpu.VMEM((HEADS * ROWS, ROWS), F32), dma((12,))],
         flops=6_000_000_000,
         limit=16,
         aliases={2: 0, 0: 1, 4: 2},
     )(rows, w_query, key, value, logs, w_ogate, conv_query, head_gain)
     pieces, query, wide, stats = lax.optimization_barrier((pieces, query, wide, stats))
     piece_shape = shape((stretches * 8, WIDTH), BF)
-    half_shape = shape((w_out.shape[0] // 2, width), BF)
-    state, upper = call(
-        prefix_kernel, (piece_shape, half_shape), (n, v), [n, n, m], [dma((4,))], flops=100_000_000
-    )(pieces.reshape(piece_shape.shape), place, w_out)
+    state = call(prefix_kernel, piece_shape, n, [n, n], flops=100_000_000_000)(pieces.reshape(piece_shape.shape), place)
     state = lax.all_to_all(state.reshape(stretches, 8, WIDTH), SP_TP, 0, 0, axis_index_groups=groups, tiled=True)
     state = state.reshape(HEADS * DQK, WIDTH)
     hidden = pltpu.VMEM((HALF, HEADS * DV), BF)
-    sent, lower = call(
-        sent_kernel,
-        (shape((HALF, width), BF), half_shape),
-        (n, v),
-        [v, v, n, v, v, m],
-        [hidden, dma((4,))],
-        flops=1_000_000_000,
-    )(query, wide, state, stats, upper, w_out)
+    sent = call(sent_kernel, shape((HALF, width), BF), n, [v, v, n, v, n], [hidden], flops=1_000_000_000)(
+        query, wide, state, stats, w_out
+    )
     got = lax.ppermute(sent, "tp", [(0, 1), (1, 0)])
-    kept = call(kept_kernel, shape((HALF, width), F32), n, [v, v, n, v, v, v], [hidden], flops=1_000_000_000)(
-        query, wide, state, stats, upper, lower
+    kept = call(kept_kernel, shape((HALF, width), F32), n, [v, v, n, v, n], [hidden], flops=1_000_000_000)(
+        query, wide, state, stats, w_out
     )
     return (kept + got.astype(F32)).astype(BF)
 

time: 59.2 us -> 58.3 us (0.985)
  Pallas kernels: 21.2 us -> 20.6 us
    pallas_call x8, Pallas kernels: 21.2 us -> 20.6 us  [call(): return lambda *args: run(*map(kept, args, spaces))]
  transfers between devices with their start and end apart: 4 -> 4, of which waited for: 1 -> 0; matrix products, arithmetic and copies ran while one was open for 0% -> 0% of each run, Pallas kernels for 23% -> 24%
where the time goes in v7:
time: 58.3 us; the launch traced here: 58.1 us
  starting transfers between devices  22.9 us (39%)
  Pallas kernels  20.6 us (35%)
  blocking collectives  13.3 us (23%)
  other arithmetic  1.09 us (2%)
    pallas_call x8, Pallas kernels, call(): return lambda *args: run(*map(kept, args, spaces))  20.6 us
    all_to_all x1, starting transfers between devices, body(): lax.all_to_all(pieces.reshape(stretches, 8, WIDTH), SP_TP, 0, 0, axis_ind...  15.5 us
    all_to_all x1, blocking collectives, body(): lax.all_to_all(state.reshape(stretches, 8, WIDTH), SP_TP, 0, 0, axis_inde...  13.3 us
    ppermute x1, starting transfers between devices, body(): tail = lax.ppermute(last, SP, [(i, i + 1) for i in range(stretches - 1)])  3.23 us
    ppermute x1, starting transfers between devices, body(): got = lax.ppermute(sent, 'tp', [(0, 1), (1, 0)])  2.8 us
    ppermute x1, starting transfers between devices, body(): other = lax.ppermute(tokens, 'tp', [(0, 1), (1, 0)])  1.38 us
  transfers between devices with their start and end apart: 4, of which 0 were waited for; matrix products, arithmetic and copies ran while one was open for 0% of the time, Pallas kernels for 24%

profile of v7, /device:TPU:1, one launch (start us, length us, event | category | flops | bytes accessed | tf_op | source)
XLA Modules:
  0.0 58.1 jit_solution(4675637449873890236)
XLA Ops:
  0.0 1.4 %collective-permute-start = (bf16[192,2048]{1,0:T(8,128)(2,1)}, bf16[192,2048]{1,0:T(8,128)(2,1)S(1)}, u32[]{:S(2)}, u32[]{:S(2)}) collective-permute-start(bf16[192,2048]{1,0:T(8,128)(2,1)} %own_hbm.1), channel_id=1, source_target_pairs={{0,1},{1,0},{2,3},{3,2},{4,5},{5,4},{6,7},{7,6},{8,9},{9,8},{10,11... | collective-permute-start | bytes 2359304 | tf_op jit(solution)/shard_map/ppermute | solution.py:384
  1.4 0.0 copy-start.2
  1.4 0.0 copy-start.1
  1.4 0.0 copy-start.5
  1.4 2.2 %shard_map.136 = (bf16[192,2048]{1,0:T(8,128)(2,1)S(1)}, bf16[2048,128]{1,0:T(8,128)(2,1)S(1)}, f32[192,128]{1,0:T(8,128)S(1)}) custom-call(bf16[192,2048]{1,0:T(8,128)(2,1)} %own_hbm.1, f32[1,2048]{1,0:T(1,128)} %bitcast.13, bf16[8,2048]{1,0:T(8,128)(2,1)} %bitcast.18, bf16[8,2048]{1,0:T(8,128)(2,1)} %bitcast.19), custom_call_target="tpu_custom_call" | custom-call | flops 99999997952 | bytes 1048576 | tf_op jit(solution)/shard_map/pallas_call | solution.py:52
  3.6 0.0 collective-permute-done.oth_ref
  3.7 0.0 copy-done.2
  3.7 0.4 shard_map.137
  4.1 3.2 %collective-permute-start.1 = (bf16[16,2048]{1,0:T(8,128)(2,1)S(1)}, bf16[16,2048]{1,0:T(8,128)(2,1)S(1)}, u32[]{:S(2)}, u32[]{:S(2)}) collective-permute-start(bf16[16,2048]{1,0:T(8,128)(2,1)S(1)} %get-tuple-element.26), channel_id=1, source_target_pairs={{0,2},{2,4},{4,6},{6,8},{8,10},{10,12},{12,14},{14,16},{16,18},{18... | collective-permute-start | bytes 196616 | tf_op jit(solution)/shard_map/ppermute | solution.py:410
  7.3 0.0 copy-done.1
  7.3 0.0 copy-done.5
  7.3 0.0 copy-start.3
  7.4 0.0 copy-start.4
  7.4 2.8 %shard_map.138 = (f32[384,512]{1,0:T(8,128)S(1)}, bf16[384,1024]{1,0:T(8,128)(2,1)S(1)}, f32[384,128]{1,0:T(8,128)S(1)}) custom-call(bf16[400,2048]{1,0:T(8,128)(2,1)S(1)} %get-tuple-element.25.rows_ref, bf16[2048,512]{1,0:T(8,128)(2,1)S(1)} %copy-done.1, bf16[2048,1024]{1,0:T(8,128)(2,1)S(1)} %copy-done.5, bf16[2048,128]{1,0:T(8,128)(2,1)S(1)} %get-tuple-element.27.wg_ref, ...), custom_call_target="tpu_custom_call" | custom-call | flops 3000000000 | bytes 1048576 | tf_op jit(solution)/shard_map/pallas_call | solution.py:52
  10.2 0.0 collective-permute-done.1.tail_ref
  10.2 0.0 copy-done.3
  10.2 0.0 copy-done.4
  10.2 0.0 copy-start.6
  10.2 0.0 copy-start.7
  10.2 2.7 %shard_map.139 = (bf16[400,2048]{1,0:T(8,128)(2,1)S(1)}, bf16[384,512]{1,0:T(8,128)(2,1)S(1)}, f32[384,128]{1,0:T(8,128)S(1)}, bf16[512,384]{1,0:T(8,128)(2,1)}) custom-call(bf16[400,2048]{1,0:T(8,128)(2,1)S(1)} %get-tuple-element.25.rows_ref, bf16[16,2048]{1,0:T(8,128)(2,1)S(1)} %collective-permute-done.1.tail_ref, ...), custom_call_target="tpu_custom_call", output_to_operand_aliasing={{0}: (0, {})} | custom-call | flops 1000000000 | bytes 1048576 | tf_op jit(solution)/shard_map/pallas_call | solution.py:52
  13.0 15.5 %all-to-all-start = ((bf16[64,8,384]{2,1,0:T(8,128)(2,1)}), bf16[64,8,384]{2,1,0:T(8,128)(2,1)S(1)}, u32[]{:S(2)}, u32[]{:S(2)}) async-start(bf16[64,8,384]{2,1,0:T(8,128)(2,1)} %bitcast.17), calls=%async_computation | async-start | bytes 786432 | tf_op jit(solution)/shard_map/all_to_all | solution.py:428
  28.4 0.0 copy-done.6
  28.4 0.0 copy-done.7
  28.5 0.0 copy-start.8
  28.5 7.1 %shard_map.140 = (bf16[384,512]{1,0:T(8,128)(2,1)S(1)}, bf16[400,2048]{1,0:T(8,128)(2,1)S(1)}, f32[384,128]{1,0:T(8,128)S(1)}) custom-call(bf16[400,2048]{1,0:T(8,128)(2,1)S(1)} %get-tuple-element.33.rows_ref, bf16[2048,512]{1,0:T(8,128)(2,1)} %wq_hbm.1, ...), custom_call_target="tpu_custom_call", output_to_operand_aliasing={{0}: (2, {}), {1}: (0, {}), {2}: (4, {})} | custom-call | flops 6000000000 | bytes 1048576 | tf_op jit(solution)/shard_map/pallas_call | solution.py:52
  35.6 0.0 all-to-all-done
  35.6 0.0 copy-done.8
  35.6 0.0 copy-start
  35.6 1.2 %shard_map.141 = bf16[512,384]{1,0:T(8,128)(2,1)S(1)} custom-call(bf16[512,384]{1,0:T(8,128)(2,1)S(1)} %bitcast.11, s32[2,64,64]{2,1,0:T(8,128)S(1)} %copy-done.8), custom_call_target="tpu_custom_call" | custom-call | flops 99999997952 | bytes 1048576 | tf_op jit(solution)/shard_map/pallas_call | solution.py:52
  36.8 13.3 %all_to_all.10 = bf16[64,8,384]{2,1,0:T(8,128)(2,1)S(1)} all-to-all(bf16[64,8,384]{2,1,0:T(8,128)(2,1)S(1)} %bitcast.12), channel_id=1, replica_groups={{84,52,76,82,86,92,116,20,44,50,54,60,68,74,78,80,90,94,108,114,118,124..., dimensions={0} | all-to-all | bytes 786432 | tf_op jit(solution)/shard_map/all_to_all | solution.py:442
  50.1 0.0 copy-done
  50.1 2.0 %shard_map.143 = bf16[192,2048]{1,0:T(8,128)(2,1)S(1)} custom-call(bf16[384,512]{1,0:T(8,128)(2,1)S(1)} %get-tuple-element.39.query_ref, bf16[400,2048]{1,0:T(8,128)(2,1)S(1)} %get-tuple-element.40.wide_ref, bf16[512,384]{1,0:T(8,128)(2,1)S(1)} %bitcast.9, f32[384,128]{1,0:T(8,128)S(1)} %get-tuple-element.42.stats_ref, bf16[1024,2048]{1,0:T(8,128)(2,1)S(1)} %copy-done), custom_call_target="tpu_custom_call" | custom-call | flops 1000000000 | bytes 1048576 | tf_op jit(solution)/shard_map/pallas_call | solution.py:52
  52.2 2.8 %collective-permute-start.2 = (bf16[192,2048]{1,0:T(8,128)(2,1)S(1)}, bf16[192,2048]{1,0:T(8,128)(2,1)S(1)}, u32[]{:S(2)}, u32[]{:S(2)}) collective-permute-start(bf16[192,2048]{1,0:T(8,128)(2,1)S(1)} %shard_map.143), channel_id=1, source_target_pairs={{0,1},{1,0},{2,3},{3,2},{4,5},{5,4},{6,7},{7,6},{8,9},{9,8},{10,11... | collective-permute-start | bytes 2359304 | tf_op jit(solution)/shard_map/ppermute | solution.py:448
  55.0 2.0 %shard_map.142 = f32[192,2048]{1,0:T(8,128)S(1)} custom-call(bf16[384,512]{1,0:T(8,128)(2,1)S(1)} %get-tuple-element.39.query_ref, bf16[400,2048]{1,0:T(8,128)(2,1)S(1)} %get-tuple-element.40.wide_ref, bf16[512,384]{1,0:T(8,128)(2,1)S(1)} %bitcast.10, f32[384,128]{1,0:T(8,128)S(1)} %get-tuple-element.42.stats_ref, bf16[1024,2048]{1,0:T(8,128)(2,1)S(1)} %copy-done), custom_call_target="tpu_custom_call" | custom-call | flops 1000000000 | bytes 1048576 | tf_op jit(solution)/shard_map/pallas_call | solution.py:52
  57.0 0.0 collective-permute-done.2
  57.0 1.1 %add_convert_fusion = bf16[192,2048]{1,0:T(8,128)(2,1)} fusion(f32[192,2048]{1,0:T(8,128)S(1)} %shard_map.142, bf16[192,2048]{1,0:T(8,128)(2,1)S(1)} %collective-permute-done.2), kind=kLoop, calls=%fused_computation | loop fusion | flops 1179648 | bytes 3145728 | tf_op jit(solution)/shard_map/convert_element_type | solution.py:452
Async XLA Ops:
  0.0 3.6 %collective-permute-start = (bf16[192,2048]{1,0:T(8,128)(2,1)}, bf16[192,2048]{1,0:T(8,128)(2,1)S(1)}, u32[]{:S(2)}, u32[]{:S(2)}) collective-permute-start(bf16[192,2048]{1,0:T(8,128)(2,1)} %own_hbm.1), channel_id=1, source_target_pairs={{0,1},{1,0},{2,3},{3,2},{4,5},{5,4},{6,7},{7,6},{8,9},{9,8},{10,11... | collective-permute-start | bytes 2359304 | tf_op jit(solution)/shard_map/ppermute | solution.py:384
  1.4 2.3 %copy-start.2 = (f32[2048]{0:T(1024)S(1)}, f32[2048]{0:T(1024)}, u32[]{:S(2)}) copy-start(f32[2048]{0:T(1024)} %param.15) | copy-start | bytes 24580
  1.4 5.9 %copy-start.1 = (bf16[2048,512]{1,0:T(8,128)(2,1)S(1)}, bf16[2048,512]{1,0:T(8,128)(2,1)}, u32[]{:S(2)}) copy-start(bf16[2048,512]{1,0:T(8,128)(2,1)} %wk_ref.3) | copy-start | bytes 6291460
  1.4 5.9 %copy-start.5 = (bf16[2048,1024]{1,0:T(8,128)(2,1)S(1)}, bf16[2048,1024]{1,0:T(8,128)(2,1)}, u32[]{:S(2)}) copy-start(bf16[2048,1024]{1,0:T(8,128)(2,1)} %wv_ref.1) | copy-start | bytes 12582916
  4.1 6.1 %collective-permute-start.1 = (bf16[16,2048]{1,0:T(8,128)(2,1)S(1)}, bf16[16,2048]{1,0:T(8,128)(2,1)S(1)}, u32[]{:S(2)}, u32[]{:S(2)}) collective-permute-start(bf16[16,2048]{1,0:T(8,128)(2,1)S(1)} %get-tuple-element.26), channel_id=1, source_target_pairs={{0,2},{2,4},{4,6},{6,8},{8,10},{10,12},{12,14},{14,16},{16,18},{18... | collective-permute-start | bytes 196616 | tf_op jit(solution)/shard_map/ppermute | solution.py:410
  7.3 2.8 %copy-start.3 = (bf16[4,1024]{1,0:T(4,128)(2,1)S(1)}, bf16[4,1024]{1,0:T(4,128)(2,1)}, u32[]{:S(2)}) copy-start(bf16[4,1024]{1,0:T(4,128)(2,1)} %taps_ref.2) | copy-start | bytes 24580
  7.4 2.8 %copy-start.4 = (f32[2,3,4]{2,0,1:T(2,128)S(1)}, f32[2,3,4]{2,0,1:T(2,128)}, u32[]{:S(2)}) copy-start(f32[2,3,4]{2,0,1:T(2,128)} %param.24) | copy-start | bytes 292
  10.2 18.3 %copy-start.6 = (bf16[4,1024]{1,0:T(4,128)(2,1)S(1)}, bf16[4,1024]{1,0:T(4,128)(2,1)}, u32[]{:S(2)}) copy-start(bf16[4,1024]{1,0:T(4,128)(2,1)} %taps_ref.3) | copy-start | bytes 24580
  10.2 18.3 %copy-start.7 = (f32[2048]{0:T(1024)S(1)}, f32[2048]{0:T(1024)}, u32[]{:S(2)}) copy-start(f32[2048]{0:T(1024)} %param.25) | copy-start | bytes 24580
  13.0 22.6 %all-to-all-start = ((bf16[64,8,384]{2,1,0:T(8,128)(2,1)}), bf16[64,8,384]{2,1,0:T(8,128)(2,1)S(1)}, u32[]{:S(2)}, u32[]{:S(2)}) async-start(bf16[64,8,384]{2,1,0:T(8,128)(2,1)} %bitcast.17), calls=%async_computation | async-start | bytes 786432 | tf_op jit(solution)/shard_map/all_to_all | solution.py:428
  28.5 7.1 %copy-start.8 = (s32[2,64,64]{2,1,0:T(8,128)S(1)}, s32[2,64,64]{2,1,0:T(8,128)}, u32[]{:S(2)}) copy-start(s32[2,64,64]{2,1,0:T(8,128)} %constant.2.clone.place_ref) | copy-start | bytes 98308
  35.6 14.5 %copy-start = (bf16[1024,2048]{1,0:T(8,128)(2,1)S(1)}, bf16[1024,2048]{1,0:T(8,128)(2,1)}, u32[]{:S(2)}) copy-start(bf16[1024,2048]{1,0:T(8,128)(2,1)} %wout_ref.3) | copy-start | bytes 12582916
  52.2 4.8 %collective-permute-start.2 = (bf16[192,2048]{1,0:T(8,128)(2,1)S(1)}, bf16[192,2048]{1,0:T(8,128)(2,1)S(1)}, u32[]{:S(2)}, u32[]{:S(2)}) collective-permute-start(bf16[192,2048]{1,0:T(8,128)(2,1)S(1)} %shard_map.143), channel_id=1, source_target_pairs={{0,1},{1,0},{2,3},{3,2},{4,5},{5,4},{6,7},{7,6},{8,9},{9,8},{10,11... | collective-permute-start | bytes 2359304 | tf_op jit(solution)/shard_map/ppermute | solution.py:448

commit v8 on v7

--- a/solution.py
+++ b/solution.py
@@ -142,8 +142,9 @@
 def summary_kernel(rows_ref, tail_ref, wk_ref, own_pre_ref, value_ref, both_ref, taps_ref, offs_ref,
                    rows_out, key_ref, logs_ref, piece_out, pre_ref, piece_ref, sems):
     tp = lax.axis_index("tp")
-    rows_out[0:TAIL, :] = tail_ref[...]
-    pre_ref[0:TAIL, :] = jnp.dot(tail_ref[...], wk_ref[...], preferred_element_type=F32).astype(BF).astype(F32)
+    later = sum(lax.axis_index(axis) for axis in SP) > 0
+    rows_out[0:TAIL, :] = jnp.where(later, tail_ref[...], jnp.zeros_like(tail_ref))
+    pre_ref[0:TAIL, :] = jnp.dot(rows_out[0:TAIL, :], wk_ref[...], preferred_element_type=F32).astype(BF).astype(F32)
     pre_ref[TAIL : TAIL + ROWS, :] = own_pre_ref[...]
     gates = both_ref[...]
     gates = jnp.where(tp == 0, gates, pltpu.roll(gates, 128 - HEADS, 1))
@@ -407,7 +408,7 @@
         flops=100_000_000_000,
     )(tokens, gain, w_igate.T, w_fgate.T)
     rows, last = call(spread_kernel, (rows_shape, shape((TAIL, width), BF)), (v, n), [v, n, n], flops=100_000_000)(own, other, gain)
-    tail = lax.ppermute(last, SP, [(i, i + 1) for i in range(stretches - 1)])
+    tail = lax.ppermute(last, SP, [(i, (i + 1) % stretches) for i in range(stretches)])
     own_pre_shape = shape((ROWS, HEADS * DQK), F32)
     own_pre, value, both = call(
         project_kernel,

time: 58.3 us -> 57.3 us (0.983)
  starting transfers between devices: 22.9 us -> 15.2 us
  waiting for transfers between devices: 0.01 us -> 6.64 us
    ppermute x1, waiting for transfers between devices: 0.01 us -> 6.64 us  [body(): lax.ppermute(last, SP, [(i, (i + 1) % stretches) for i in range(stretches)])]
    all_to_all x1, starting transfers between devices: 15.5 us -> 9.94 us  [body(): lax.all_to_all(pieces.reshape(stretches, 8, WIDTH), SP_TP, 0, 0, axis_ind...]
    ppermute x1, starting transfers between devices: 3.23 us -> 1.39 us  [body(): lax.ppermute(last, SP, [(i, (i + 1) % stretches) for i in range(stretches)])]
  transfers between devices with their start and end apart: 4 -> 4, of which waited for: 0 -> 1; matrix products, arithmetic and copies ran while one was open for 0% -> 0% of each run, Pallas kernels for 24% -> 25%
where the time goes in v8:
time: 57.3 us; the launch traced here: 57.1 us
  Pallas kernels  20.6 us (36%)
  starting transfers between devices  15.2 us (27%)
  blocking collectives  13.4 us (23%)
  waiting for transfers between devices  6.64 us (12%)
  other arithmetic  1.09 us (2%)
    pallas_call x8, Pallas kernels, call(): return lambda *args: run(*map(kept, args, spaces))  20.6 us
    all_to_all x1, blocking collectives, body(): lax.all_to_all(state.reshape(stretches, 8, WIDTH), SP_TP, 0, 0, axis_inde...  13.4 us
    all_to_all x1, starting transfers between devices, body(): lax.all_to_all(pieces.reshape(stretches, 8, WIDTH), SP_TP, 0, 0, axis_ind...  9.94 us
    ppermute x1, waiting for transfers between devices, body(): lax.ppermute(last, SP, [(i, (i + 1) % stretches) for i in range(stretches)])  6.64 us
    ppermute x1, starting transfers between devices, body(): got = lax.ppermute(sent, 'tp', [(0, 1), (1, 0)])  2.49 us
    ppermute x1, starting transfers between devices, body(): lax.ppermute(last, SP, [(i, (i + 1) % stretches) for i in range(stretches)])  1.39 us
    ppermute x1, starting transfers between devices, body(): other = lax.ppermute(tokens, 'tp', [(0, 1), (1, 0)])  1.38 us
  transfers between devices with their start and end apart: 4, of which 1 were waited for; matrix products, arithmetic and copies ran while one was open for 0% of the time, Pallas kernels for 25%

profile of v8, /device:TPU:1, one launch (start us, length us, event | category | flops | bytes accessed | tf_op | source)
XLA Modules:
  0.0 57.1 jit_solution(5723517123816453232)
XLA Ops:
  0.0 1.4 %collective-permute-start = (bf16[192,2048]{1,0:T(8,128)(2,1)}, bf16[192,2048]{1,0:T(8,128)(2,1)S(1)}, u32[]{:S(2)}, u32[]{:S(2)}) collective-permute-start(bf16[192,2048]{1,0:T(8,128)(2,1)} %own_hbm.1), channel_id=1, source_target_pairs={{0,1},{1,0},{2,3},{3,2},{4,5},{5,4},{6,7},{7,6},{8,9},{9,8},{10,11... | collective-permute-start | bytes 2359304 | tf_op jit(solution)/shard_map/ppermute | solution.py:385
  1.4 0.0 copy-start.2
  1.4 0.0 copy-start.1
  1.4 0.0 copy-start.5
  1.4 2.2 %shard_map.136 = (bf16[192,2048]{1,0:T(8,128)(2,1)S(1)}, bf16[2048,128]{1,0:T(8,128)(2,1)S(1)}, f32[192,128]{1,0:T(8,128)S(1)}) custom-call(bf16[192,2048]{1,0:T(8,128)(2,1)} %own_hbm.1, f32[1,2048]{1,0:T(1,128)} %bitcast.13, bf16[8,2048]{1,0:T(8,128)(2,1)} %bitcast.18, bf16[8,2048]{1,0:T(8,128)(2,1)} %bitcast.19), custom_call_target="tpu_custom_call" | custom-call | flops 99999997952 | bytes 1048576 | tf_op jit(solution)/shard_map/pallas_call | solution.py:52
  3.6 0.0 collective-permute-done.oth_ref
  3.7 0.0 copy-done.2
  3.7 0.4 shard_map.137
  4.1 1.4 %collective-permute-start.1 = (bf16[16,2048]{1,0:T(8,128)(2,1)S(1)}, bf16[16,2048]{1,0:T(8,128)(2,1)S(1)}, u32[]{:S(2)}, u32[]{:S(2)}) collective-permute-start(bf16[16,2048]{1,0:T(8,128)(2,1)S(1)} %get-tuple-element.26), channel_id=1, source_target_pairs={{0,2},{2,4},{4,6},{6,8},{8,10},{10,12},{12,14},{14,16},{16,18},{18... | collective-permute-start | bytes 196616 | tf_op jit(solution)/shard_map/ppermute | solution.py:411
  5.5 0.0 copy-done.1
  5.5 0.0 copy-done.5
  5.5 0.0 copy-start.3
  5.5 0.0 copy-start.4
  5.5 2.8 %shard_map.138 = (f32[384,512]{1,0:T(8,128)S(1)}, bf16[384,1024]{1,0:T(8,128)(2,1)S(1)}, f32[384,128]{1,0:T(8,128)S(1)}) custom-call(bf16[400,2048]{1,0:T(8,128)(2,1)S(1)} %get-tuple-element.25.rows_ref, bf16[2048,512]{1,0:T(8,128)(2,1)S(1)} %copy-done.1, bf16[2048,1024]{1,0:T(8,128)(2,1)S(1)} %copy-done.5, bf16[2048,128]{1,0:T(8,128)(2,1)S(1)} %get-tuple-element.27.wg_ref, ...), custom_call_target="tpu_custom_call" | custom-call | flops 3000000000 | bytes 1048576 | tf_op jit(solution)/shard_map/pallas_call | solution.py:52
  8.3 6.6 %collective-permute-done.1.tail_ref = bf16[16,2048]{1,0:T(8,128)(2,1)S(1)} collective-permute-done((bf16[16,2048]{1,0:T(8,128)(2,1)S(1)}, bf16[16,2048]{1,0:T(8,128)(2,1)S(1)}, u32[]{:S(2)}, u32[]{:S(2)}) %collective-permute-start.1) | collective-permute-done | bytes 65568 | tf_op jit(solution)/shard_map/ppermute | solution.py:411
  14.9 0.0 copy-done.3
  14.9 0.0 copy-done.4
  14.9 0.0 copy-start.6
  14.9 0.0 copy-start.7
  14.9 2.8 %shard_map.139 = (bf16[400,2048]{1,0:T(8,128)(2,1)S(1)}, bf16[384,512]{1,0:T(8,128)(2,1)S(1)}, f32[384,128]{1,0:T(8,128)S(1)}, bf16[512,384]{1,0:T(8,128)(2,1)}) custom-call(bf16[400,2048]{1,0:T(8,128)(2,1)S(1)} %get-tuple-element.25.rows_ref, bf16[16,2048]{1,0:T(8,128)(2,1)S(1)} %collective-permute-done.1.tail_ref, ...), custom_call_target="tpu_custom_call", output_to_operand_aliasing={{0}: (0, {})} | custom-call | flops 1000000000 | bytes 1048576 | tf_op jit(solution)/shard_map/pallas_call | solution.py:52
  17.7 9.9 %all-to-all-start = ((bf16[64,8,384]{2,1,0:T(8,128)(2,1)}), bf16[64,8,384]{2,1,0:T(8,128)(2,1)S(1)}, u32[]{:S(2)}, u32[]{:S(2)}) async-start(bf16[64,8,384]{2,1,0:T(8,128)(2,1)} %bitcast.17), calls=%async_computation | async-start | bytes 786432 | tf_op jit(solution)/shard_map/all_to_all | solution.py:429
  27.7 0.0 copy-done.6
  27.7 0.0 copy-done.7
  27.7 0.0 copy-start.8
  27.7 7.1 %shard_map.140 = (bf16[384,512]{1,0:T(8,128)(2,1)S(1)}, bf16[400,2048]{1,0:T(8,128)(2,1)S(1)}, f32[384,128]{1,0:T(8,128)S(1)}) custom-call(bf16[400,2048]{1,0:T(8,128)(2,1)S(1)} %get-tuple-element.33.rows_ref, bf16[2048,512]{1,0:T(8,128)(2,1)} %wq_hbm.1, ...), custom_call_target="tpu_custom_call", output_to_operand_aliasing={{0}: (2, {}), {1}: (0, {}), {2}: (4, {})} | custom-call | flops 6000000000 | bytes 1048576 | tf_op jit(solution)/shard_map/pallas_call | solution.py:52
  34.8 0.0 all-to-all-done
  34.8 0.0 copy-done.8
  34.8 0.0 copy-start
  34.8 1.2 %shard_map.141 = bf16[512,384]{1,0:T(8,128)(2,1)S(1)} custom-call(bf16[512,384]{1,0:T(8,128)(2,1)S(1)} %bitcast.11, s32[2,64,64]{2,1,0:T(8,128)S(1)} %copy-done.8), custom_call_target="tpu_custom_call" | custom-call | flops 99999997952 | bytes 1048576 | tf_op jit(solution)/shard_map/pallas_call | solution.py:52
  36.1 13.4 %all_to_all.10 = bf16[64,8,384]{2,1,0:T(8,128)(2,1)S(1)} all-to-all(bf16[64,8,384]{2,1,0:T(8,128)(2,1)S(1)} %bitcast.12), channel_id=1, replica_groups={{84,52,76,82,86,92,116,20,44,50,54,60,68,74,78,80,90,94,108,114,118,124..., dimensions={0} | all-to-all | bytes 786432 | tf_op jit(solution)/shard_map/all_to_all | solution.py:443
  49.4 0.0 copy-done
  49.4 2.0 %shard_map.143 = bf16[192,2048]{1,0:T(8,128)(2,1)S(1)} custom-call(bf16[384,512]{1,0:T(8,128)(2,1)S(1)} %get-tuple-element.39.query_ref, bf16[400,2048]{1,0:T(8,128)(2,1)S(1)} %get-tuple-element.40.wide_ref, bf16[512,384]{1,0:T(8,128)(2,1)S(1)} %bitcast.9, f32[384,128]{1,0:T(8,128)S(1)} %get-tuple-element.42.stats_ref, bf16[1024,2048]{1,0:T(8,128)(2,1)S(1)} %copy-done), custom_call_target="tpu_custom_call" | custom-call | flops 1000000000 | bytes 1048576 | tf_op jit(solution)/shard_map/pallas_call | solution.py:52
  51.5 2.5 %collective-permute-start.2 = (bf16[192,2048]{1,0:T(8,128)(2,1)S(1)}, bf16[192,2048]{1,0:T(8,128)(2,1)S(1)}, u32[]{:S(2)}, u32[]{:S(2)}) collective-permute-start(bf16[192,2048]{1,0:T(8,128)(2,1)S(1)} %shard_map.143), channel_id=1, source_target_pairs={{0,1},{1,0},{2,3},{3,2},{4,5},{5,4},{6,7},{7,6},{8,9},{9,8},{10,11... | collective-permute-start | bytes 2359304 | tf_op jit(solution)/shard_map/ppermute | solution.py:449
  53.9 2.0 %shard_map.142 = f32[192,2048]{1,0:T(8,128)S(1)} custom-call(bf16[384,512]{1,0:T(8,128)(2,1)S(1)} %get-tuple-element.39.query_ref, bf16[400,2048]{1,0:T(8,128)(2,1)S(1)} %get-tuple-element.40.wide_ref, bf16[512,384]{1,0:T(8,128)(2,1)S(1)} %bitcast.10, f32[384,128]{1,0:T(8,128)S(1)} %get-tuple-element.42.stats_ref, bf16[1024,2048]{1,0:T(8,128)(2,1)S(1)} %copy-done), custom_call_target="tpu_custom_call" | custom-call | flops 1000000000 | bytes 1048576 | tf_op jit(solution)/shard_map/pallas_call | solution.py:52
  56.0 0.0 collective-permute-done.2
  56.0 1.1 %add_convert_fusion = bf16[192,2048]{1,0:T(8,128)(2,1)} fusion(f32[192,2048]{1,0:T(8,128)S(1)} %shard_map.142, bf16[192,2048]{1,0:T(8,128)(2,1)S(1)} %collective-permute-done.2), kind=kLoop, calls=%fused_computation | loop fusion | flops 1179648 | bytes 3145728 | tf_op jit(solution)/shard_map/convert_element_type | solution.py:453
Async XLA Ops:
  0.0 3.6 %collective-permute-start = (bf16[192,2048]{1,0:T(8,128)(2,1)}, bf16[192,2048]{1,0:T(8,128)(2,1)S(1)}, u32[]{:S(2)}, u32[]{:S(2)}) collective-permute-start(bf16[192,2048]{1,0:T(8,128)(2,1)} %own_hbm.1), channel_id=1, source_target_pairs={{0,1},{1,0},{2,3},{3,2},{4,5},{5,4},{6,7},{7,6},{8,9},{9,8},{10,11... | collective-permute-start | bytes 2359304 | tf_op jit(solution)/shard_map/ppermute | solution.py:385
  1.4 2.3 %copy-start.2 = (f32[2048]{0:T(1024)S(1)}, f32[2048]{0:T(1024)}, u32[]{:S(2)}) copy-start(f32[2048]{0:T(1024)} %param.15) | copy-start | bytes 24580
  1.4 4.1 %copy-start.1 = (bf16[2048,512]{1,0:T(8,128)(2,1)S(1)}, bf16[2048,512]{1,0:T(8,128)(2,1)}, u32[]{:S(2)}) copy-start(bf16[2048,512]{1,0:T(8,128)(2,1)} %wk_ref.3) | copy-start | bytes 6291460
  1.4 4.1 %copy-start.5 = (bf16[2048,1024]{1,0:T(8,128)(2,1)S(1)}, bf16[2048,1024]{1,0:T(8,128)(2,1)}, u32[]{:S(2)}) copy-start(bf16[2048,1024]{1,0:T(8,128)(2,1)} %wv_ref.1) | copy-start | bytes 12582916
  4.1 10.8 %collective-permute-start.1 = (bf16[16,2048]{1,0:T(8,128)(2,1)S(1)}, bf16[16,2048]{1,0:T(8,128)(2,1)S(1)}, u32[]{:S(2)}, u32[]{:S(2)}) collective-permute-start(bf16[16,2048]{1,0:T(8,128)(2,1)S(1)} %get-tuple-element.26), channel_id=1, source_target_pairs={{0,2},{2,4},{4,6},{6,8},{8,10},{10,12},{12,14},{14,16},{16,18},{18... | collective-permute-start | bytes 196616 | tf_op jit(solution)/shard_map/ppermute | solution.py:411
  5.5 9.4 %copy-start.3 = (bf16[4,1024]{1,0:T(4,128)(2,1)S(1)}, bf16[4,1024]{1,0:T(4,128)(2,1)}, u32[]{:S(2)}) copy-start(bf16[4,1024]{1,0:T(4,128)(2,1)} %taps_ref.2) | copy-start | bytes 24580
  5.5 9.4 %copy-start.4 = (f32[2,3,4]{2,0,1:T(2,128)S(1)}, f32[2,3,4]{2,0,1:T(2,128)}, u32[]{:S(2)}) copy-start(f32[2,3,4]{2,0,1:T(2,128)} %param.24) | copy-start | bytes 292
  14.9 12.7 %copy-start.6 = (bf16[4,1024]{1,0:T(4,128)(2,1)S(1)}, bf16[4,1024]{1,0:T(4,128)(2,1)}, u32[]{:S(2)}) copy-start(bf16[4,1024]{1,0:T(4,128)(2,1)} %taps_ref.3) | copy-start | bytes 24580
  14.9 12.7 %copy-start.7 = (f32[2048]{0:T(1024)S(1)}, f32[2048]{0:T(1024)}, u32[]{:S(2)}) copy-start(f32[2048]{0:T(1024)} %param.25) | copy-start | bytes 24580
  17.7 17.1 %all-to-all-start = ((bf16[64,8,384]{2,1,0:T(8,128)(2,1)}), bf16[64,8,384]{2,1,0:T(8,128)(2,1)S(1)}, u32[]{:S(2)}, u32[]{:S(2)}) async-start(bf16[64,8,384]{2,1,0:T(8,128)(2,1)} %bitcast.17), calls=%async_computation | async-start | bytes 786432 | tf_op jit(solution)/shard_map/all_to_all | solution.py:429
  27.7 7.1 %copy-start.8 = (s32[2,64,64]{2,1,0:T(8,128)S(1)}, s32[2,64,64]{2,1,0:T(8,128)}, u32[]{:S(2)}) copy-start(s32[2,64,64]{2,1,0:T(8,128)} %constant.2.clone.place_ref) | copy-start | bytes 98308
  34.8 14.6 %copy-start = (bf16[1024,2048]{1,0:T(8,128)(2,1)S(1)}, bf16[1024,2048]{1,0:T(8,128)(2,1)}, u32[]{:S(2)}) copy-start(bf16[1024,2048]{1,0:T(8,128)(2,1)} %wout_ref.3) | copy-start | bytes 12582916
  51.5 4.5 %collective-permute-start.2 = (bf16[192,2048]{1,0:T(8,128)(2,1)S(1)}, bf16[192,2048]{1,0:T(8,128)(2,1)S(1)}, u32[]{:S(2)}, u32[]{:S(2)}) collective-permute-start(bf16[192,2048]{1,0:T(8,128)(2,1)S(1)} %shard_map.143), channel_id=1, source_target_pairs={{0,1},{1,0},{2,3},{3,2},{4,5},{5,4},{6,7},{7,6},{8,9},{9,8},{10,11... | collective-permute-start | bytes 2359304 | tf_op jit(solution)/shard_map/ppermute | solution.py:449

commit v9 on v8

--- a/solution.py
+++ b/solution.py
@@ -291,8 +291,15 @@
             for s, x in enumerate(logs):
                 weight_ref[h * ROWS + t * SPAN : h * ROWS + (t + 1) * SPAN, s * SPAN : (s + 1) * SPAN] = jnp.exp(x - top)
             stats[t] = jnp.where(lane == HEADS + h, top, stats[t])
-    wait_all(copies[:4])
-    pre_ref[...] = jnp.dot(rows_ref[...], wq_ref[...], preferred_element_type=F32).astype(BF).astype(F32)
+    deep = wq_ref.shape[0] // 4
+    for c in range(4):
+        copies[c].wait()
+        depth = slice(c * deep, (c + 1) * deep)
+        part = jnp.dot(rows_ref[:, depth], wq_ref[depth, :], preferred_element_type=F32)
+        if c < 3:
+            pre_ref[...] = part if c == 0 else pre_ref[...] + part
+        else:
+            pre_ref[...] = (pre_ref[...] + part).astype(BF).astype(F32)
     for h in range(HEADS):
         lanes = slice(h * DQK, (h + 1) * DQK)
         for b in range(BLOCKS):
@@ -373,7 +380,7 @@
 def far_first(stretches):
     at = np.arange(stretches)
     hops = sum(np.minimum(c, 4 - c) for c in (at // 16, at // 4 % 4, at % 4))
-    return np.lexsort((at, -hops))
+    return np.lexsort((-at, -hops))
 
 
 def body(

time: 57.3 us -> 57.2 us (level)
  no operation moved by 1% of the time
where the time goes in v9:
time: 57.2 us; the launch traced here: 57 us
  Pallas kernels  20.6 us (36%)
  starting transfers between devices  15.1 us (26%)
  blocking collectives  13.4 us (23%)
  waiting for transfers between devices  6.64 us (12%)
  other arithmetic  1.09 us (2%)
    pallas_call x8, Pallas kernels, call(): return lambda *args: run(*map(kept, args, spaces))  20.6 us
    all_to_all x1, blocking collectives, body(): lax.all_to_all(state.reshape(stretches, 8, WIDTH), SP_TP, 0, 0, axis_inde...  13.4 us
    all_to_all x1, starting transfers between devices, body(): lax.all_to_all(pieces.reshape(stretches, 8, WIDTH), SP_TP, 0, 0, axis_ind...  9.94 us
    ppermute x1, waiting for transfers between devices, body(): lax.ppermute(last, SP, [(i, (i + 1) % stretches) for i in range(stretches)])  6.64 us
    ppermute x1, starting transfers between devices, body(): got = lax.ppermute(sent, 'tp', [(0, 1), (1, 0)])  2.36 us
    ppermute x1, starting transfers between devices, body(): lax.ppermute(last, SP, [(i, (i + 1) % stretches) for i in range(stretches)])  1.39 us
    ppermute x1, starting transfers between devices, body(): other = lax.ppermute(tokens, 'tp', [(0, 1), (1, 0)])  1.38 us
  transfers between devices with their start and end apart: 4, of which 1 were waited for; matrix products, arithmetic and copies ran while one was open for 0% of the time, Pallas kernels for 25%

profile of v9, /device:TPU:1, one launch (start us, length us, event | category | flops | bytes accessed | tf_op | source)
XLA Modules:
  0.0 57.0 jit_solution(2181774890238569836)
XLA Ops:
  0.0 1.4 %collective-permute-start = (bf16[192,2048]{1,0:T(8,128)(2,1)}, bf16[192,2048]{1,0:T(8,128)(2,1)S(1)}, u32[]{:S(2)}, u32[]{:S(2)}) collective-permute-start(bf16[192,2048]{1,0:T(8,128)(2,1)} %own_hbm.1), channel_id=1, source_target_pairs={{0,1},{1,0},{2,3},{3,2},{4,5},{5,4},{6,7},{7,6},{8,9},{9,8},{10,11... | collective-permute-start | bytes 2359304 | tf_op jit(solution)/shard_map/ppermute | solution.py:392
  1.4 0.0 copy-start.2
  1.4 0.0 copy-start.1
  1.4 0.0 copy-start.5
  1.4 2.2 %shard_map.136 = (bf16[192,2048]{1,0:T(8,128)(2,1)S(1)}, bf16[2048,128]{1,0:T(8,128)(2,1)S(1)}, f32[192,128]{1,0:T(8,128)S(1)}) custom-call(bf16[192,2048]{1,0:T(8,128)(2,1)} %own_hbm.1, f32[1,2048]{1,0:T(1,128)} %bitcast.13, bf16[8,2048]{1,0:T(8,128)(2,1)} %bitcast.18, bf16[8,2048]{1,0:T(8,128)(2,1)} %bitcast.19), custom_call_target="tpu_custom_call" | custom-call | flops 99999997952 | bytes 1048576 | tf_op jit(solution)/shard_map/pallas_call | solution.py:52
  3.6 0.0 collective-permute-done.oth_ref
  3.7 0.0 copy-done.2
  3.7 0.4 shard_map.137
  4.1 1.4 %collective-permute-start.1 = (bf16[16,2048]{1,0:T(8,128)(2,1)S(1)}, bf16[16,2048]{1,0:T(8,128)(2,1)S(1)}, u32[]{:S(2)}, u32[]{:S(2)}) collective-permute-start(bf16[16,2048]{1,0:T(8,128)(2,1)S(1)} %get-tuple-element.26), channel_id=1, source_target_pairs={{0,2},{2,4},{4,6},{6,8},{8,10},{10,12},{12,14},{14,16},{16,18},{18... | collective-permute-start | bytes 196616 | tf_op jit(solution)/shard_map/ppermute | solution.py:418
  5.5 0.0 copy-done.1
  5.5 0.0 copy-done.5
  5.5 0.0 copy-start.3
  5.5 0.0 copy-start.4
  5.5 2.8 %shard_map.138 = (f32[384,512]{1,0:T(8,128)S(1)}, bf16[384,1024]{1,0:T(8,128)(2,1)S(1)}, f32[384,128]{1,0:T(8,128)S(1)}) custom-call(bf16[400,2048]{1,0:T(8,128)(2,1)S(1)} %get-tuple-element.25.rows_ref, bf16[2048,512]{1,0:T(8,128)(2,1)S(1)} %copy-done.1, bf16[2048,1024]{1,0:T(8,128)(2,1)S(1)} %copy-done.5, bf16[2048,128]{1,0:T(8,128)(2,1)S(1)} %get-tuple-element.27.wg_ref, ...), custom_call_target="tpu_custom_call" | custom-call | flops 3000000000 | bytes 1048576 | tf_op jit(solution)/shard_map/pallas_call | solution.py:52
  8.3 6.6 %collective-permute-done.1.tail_ref = bf16[16,2048]{1,0:T(8,128)(2,1)S(1)} collective-permute-done((bf16[16,2048]{1,0:T(8,128)(2,1)S(1)}, bf16[16,2048]{1,0:T(8,128)(2,1)S(1)}, u32[]{:S(2)}, u32[]{:S(2)}) %collective-permute-start.1) | collective-permute-done | bytes 65568 | tf_op jit(solution)/shard_map/ppermute | solution.py:418
  14.9 0.0 copy-done.3
  14.9 0.0 copy-done.4
  14.9 0.0 copy-start.6
  14.9 0.0 copy-start.7
  14.9 2.8 %shard_map.139 = (bf16[400,2048]{1,0:T(8,128)(2,1)S(1)}, bf16[384,512]{1,0:T(8,128)(2,1)S(1)}, f32[384,128]{1,0:T(8,128)S(1)}, bf16[512,384]{1,0:T(8,128)(2,1)}) custom-call(bf16[400,2048]{1,0:T(8,128)(2,1)S(1)} %get-tuple-element.25.rows_ref, bf16[16,2048]{1,0:T(8,128)(2,1)S(1)} %collective-permute-done.1.tail_ref, ...), custom_call_target="tpu_custom_call", output_to_operand_aliasing={{0}: (0, {})} | custom-call | flops 1000000000 | bytes 1048576 | tf_op jit(solution)/shard_map/pallas_call | solution.py:52
  17.7 9.9 %all-to-all-start = ((bf16[64,8,384]{2,1,0:T(8,128)(2,1)}), bf16[64,8,384]{2,1,0:T(8,128)(2,1)S(1)}, u32[]{:S(2)}, u32[]{:S(2)}) async-start(bf16[64,8,384]{2,1,0:T(8,128)(2,1)} %bitcast.17), calls=%async_computation | async-start | bytes 786432 | tf_op jit(solution)/shard_map/all_to_all | solution.py:436
  27.7 0.0 copy-done.6
  27.7 0.0 copy-done.7
  27.7 0.0 copy-start.8
  27.7 7.1 %shard_map.140 = (bf16[384,512]{1,0:T(8,128)(2,1)S(1)}, bf16[400,2048]{1,0:T(8,128)(2,1)S(1)}, f32[384,128]{1,0:T(8,128)S(1)}) custom-call(bf16[400,2048]{1,0:T(8,128)(2,1)S(1)} %get-tuple-element.33.rows_ref, bf16[2048,512]{1,0:T(8,128)(2,1)} %wq_hbm.1, ...), custom_call_target="tpu_custom_call", output_to_operand_aliasing={{0}: (2, {}), {1}: (0, {}), {2}: (4, {})} | custom-call | flops 6000000000 | bytes 1048576 | tf_op jit(solution)/shard_map/pallas_call | solution.py:52
  34.8 0.0 all-to-all-done
  34.8 0.0 copy-done.8
  34.9 0.0 copy-start
  34.9 1.2 %shard_map.141 = bf16[512,384]{1,0:T(8,128)(2,1)S(1)} custom-call(bf16[512,384]{1,0:T(8,128)(2,1)S(1)} %bitcast.11, s32[2,64,64]{2,1,0:T(8,128)S(1)} %copy-done.8), custom_call_target="tpu_custom_call" | custom-call | flops 99999997952 | bytes 1048576 | tf_op jit(solution)/shard_map/pallas_call | solution.py:52
  36.1 13.4 %all_to_all.10 = bf16[64,8,384]{2,1,0:T(8,128)(2,1)S(1)} all-to-all(bf16[64,8,384]{2,1,0:T(8,128)(2,1)S(1)} %bitcast.12), channel_id=1, replica_groups={{84,116,92,86,82,76,52,124,118,114,108,94,90,80,78,74,68,60,54,50,44,20..., dimensions={0} | all-to-all | bytes 786432 | tf_op jit(solution)/shard_map/all_to_all | solution.py:450
  49.5 0.0 copy-done
  49.5 2.0 %shard_map.143 = bf16[192,2048]{1,0:T(8,128)(2,1)S(1)} custom-call(bf16[384,512]{1,0:T(8,128)(2,1)S(1)} %get-tuple-element.39.query_ref, bf16[400,2048]{1,0:T(8,128)(2,1)S(1)} %get-tuple-element.40.wide_ref, bf16[512,384]{1,0:T(8,128)(2,1)S(1)} %bitcast.9, f32[384,128]{1,0:T(8,128)S(1)} %get-tuple-element.42.stats_ref, bf16[1024,2048]{1,0:T(8,128)(2,1)S(1)} %copy-done), custom_call_target="tpu_custom_call" | custom-call | flops 1000000000 | bytes 1048576 | tf_op jit(solution)/shard_map/pallas_call | solution.py:52
  51.5 2.4 %collective-permute-start.2 = (bf16[192,2048]{1,0:T(8,128)(2,1)S(1)}, bf16[192,2048]{1,0:T(8,128)(2,1)S(1)}, u32[]{:S(2)}, u32[]{:S(2)}) collective-permute-start(bf16[192,2048]{1,0:T(8,128)(2,1)S(1)} %shard_map.143), channel_id=1, source_target_pairs={{0,1},{1,0},{2,3},{3,2},{4,5},{5,4},{6,7},{7,6},{8,9},{9,8},{10,11... | collective-permute-start | bytes 2359304 | tf_op jit(solution)/shard_map/ppermute | solution.py:456
  53.8 2.0 %shard_map.142 = f32[192,2048]{1,0:T(8,128)S(1)} custom-call(bf16[384,512]{1,0:T(8,128)(2,1)S(1)} %get-tuple-element.39.query_ref, bf16[400,2048]{1,0:T(8,128)(2,1)S(1)} %get-tuple-element.40.wide_ref, bf16[512,384]{1,0:T(8,128)(2,1)S(1)} %bitcast.10, f32[384,128]{1,0:T(8,128)S(1)} %get-tuple-element.42.stats_ref, bf16[1024,2048]{1,0:T(8,128)(2,1)S(1)} %copy-done), custom_call_target="tpu_custom_call" | custom-call | flops 1000000000 | bytes 1048576 | tf_op jit(solution)/shard_map/pallas_call | solution.py:52
  55.9 0.0 collective-permute-done.2
  55.9 1.1 %add_convert_fusion = bf16[192,2048]{1,0:T(8,128)(2,1)} fusion(f32[192,2048]{1,0:T(8,128)S(1)} %shard_map.142, bf16[192,2048]{1,0:T(8,128)(2,1)S(1)} %collective-permute-done.2), kind=kLoop, calls=%fused_computation | loop fusion | flops 1179648 | bytes 3145728 | tf_op jit(solution)/shard_map/convert_element_type | solution.py:460
Async XLA Ops:
  0.0 3.6 %collective-permute-start = (bf16[192,2048]{1,0:T(8,128)(2,1)}, bf16[192,2048]{1,0:T(8,128)(2,1)S(1)}, u32[]{:S(2)}, u32[]{:S(2)}) collective-permute-start(bf16[192,2048]{1,0:T(8,128)(2,1)} %own_hbm.1), channel_id=1, source_target_pairs={{0,1},{1,0},{2,3},{3,2},{4,5},{5,4},{6,7},{7,6},{8,9},{9,8},{10,11... | collective-permute-start | bytes 2359304 | tf_op jit(solution)/shard_map/ppermute | solution.py:392
  1.4 2.3 %copy-start.2 = (f32[2048]{0:T(1024)S(1)}, f32[2048]{0:T(1024)}, u32[]{:S(2)}) copy-start(f32[2048]{0:T(1024)} %param.15) | copy-start | bytes 24580
  1.4 4.1 %copy-start.1 = (bf16[2048,512]{1,0:T(8,128)(2,1)S(1)}, bf16[2048,512]{1,0:T(8,128)(2,1)}, u32[]{:S(2)}) copy-start(bf16[2048,512]{1,0:T(8,128)(2,1)} %wk_ref.3) | copy-start | bytes 6291460
  1.4 4.1 %copy-start.5 = (bf16[2048,1024]{1,0:T(8,128)(2,1)S(1)}, bf16[2048,1024]{1,0:T(8,128)(2,1)}, u32[]{:S(2)}) copy-start(bf16[2048,1024]{1,0:T(8,128)(2,1)} %wv_ref.1) | copy-start | bytes 12582916
  4.1 10.8 %collective-permute-start.1 = (bf16[16,2048]{1,0:T(8,128)(2,1)S(1)}, bf16[16,2048]{1,0:T(8,128)(2,1)S(1)}, u32[]{:S(2)}, u32[]{:S(2)}) collective-permute-start(bf16[16,2048]{1,0:T(8,128)(2,1)S(1)} %get-tuple-element.26), channel_id=1, source_target_pairs={{0,2},{2,4},{4,6},{6,8},{8,10},{10,12},{12,14},{14,16},{16,18},{18... | collective-permute-start | bytes 196616 | tf_op jit(solution)/shard_map/ppermute | solution.py:418
  5.5 9.4 %copy-start.3 = (bf16[4,1024]{1,0:T(4,128)(2,1)S(1)}, bf16[4,1024]{1,0:T(4,128)(2,1)}, u32[]{:S(2)}) copy-start(bf16[4,1024]{1,0:T(4,128)(2,1)} %taps_ref.2) | copy-start | bytes 24580
  5.5 9.4 %copy-start.4 = (f32[2,3,4]{2,0,1:T(2,128)S(1)}, f32[2,3,4]{2,0,1:T(2,128)}, u32[]{:S(2)}) copy-start(f32[2,3,4]{2,0,1:T(2,128)} %param.24) | copy-start | bytes 292
  14.9 12.7 %copy-start.6 = (bf16[4,1024]{1,0:T(4,128)(2,1)S(1)}, bf16[4,1024]{1,0:T(4,128)(2,1)}, u32[]{:S(2)}) copy-start(bf16[4,1024]{1,0:T(4,128)(2,1)} %taps_ref.3) | copy-start | bytes 24580
  14.9 12.7 %copy-start.7 = (f32[2048]{0:T(1024)S(1)}, f32[2048]{0:T(1024)}, u32[]{:S(2)}) copy-start(f32[2048]{0:T(1024)} %param.25) | copy-start | bytes 24580
  17.7 17.1 %all-to-all-start = ((bf16[64,8,384]{2,1,0:T(8,128)(2,1)}), bf16[64,8,384]{2,1,0:T(8,128)(2,1)S(1)}, u32[]{:S(2)}, u32[]{:S(2)}) async-start(bf16[64,8,384]{2,1,0:T(8,128)(2,1)} %bitcast.17), calls=%async_computation | async-start | bytes 786432 | tf_op jit(solution)/shard_map/all_to_all | solution.py:436
  27.7 7.2 %copy-start.8 = (s32[2,64,64]{2,1,0:T(8,128)S(1)}, s32[2,64,64]{2,1,0:T(8,128)}, u32[]{:S(2)}) copy-start(s32[2,64,64]{2,1,0:T(8,128)} %constant.2.clone.place_ref) | copy-start | bytes 98308
  34.9 14.6 %copy-start = (bf16[1024,2048]{1,0:T(8,128)(2,1)S(1)}, bf16[1024,2048]{1,0:T(8,128)(2,1)}, u32[]{:S(2)}) copy-start(bf16[1024,2048]{1,0:T(8,128)(2,1)} %wout_ref.3) | copy-start | bytes 12582916
  51.5 4.4 %collective-permute-start.2 = (bf16[192,2048]{1,0:T(8,128)(2,1)S(1)}, bf16[192,2048]{1,0:T(8,128)(2,1)S(1)}, u32[]{:S(2)}, u32[]{:S(2)}) collective-permute-start(bf16[192,2048]{1,0:T(8,128)(2,1)S(1)} %shard_map.143), channel_id=1, source_target_pairs={{0,1},{1,0},{2,3},{3,2},{4,5},{5,4},{6,7},{7,6},{8,9},{9,8},{10,11... | collective-permute-start | bytes 2359304 | tf_op jit(solution)/shard_map/ppermute | solution.py:456
